TPU v7x, 128 devices: a whole 4x4x4 slice. The times are simulated.
128 devices in a mesh: sp: 16 (over z, x), tp: 8 (over y, core).
Axes of the slice: x: 4, y: 4, z: 4, core: 2. Of those that a mesh axis runs over, the one named last changes fastest.
Arguments:
- tokens: bfloat16 [16384, 4096], P('sp'), may hold values from -6 to 6
- input_norm_scale: bfloat16 [4096], replicated, may hold values from 0.099609375 to 1.8984375
- mean_input_weight: bfloat16 [4096, 2048], P('sp', 'tp'), may hold values from -0.09375 to 0.09375
- query_matrix: bfloat16 [4096, 2048], P('sp', 'tp'), may hold values from -0.09375 to 0.09375
- key_matrix: bfloat16 [4096, 2048], P('sp', 'tp'), may hold values from -0.09375 to 0.09375
- value_matrix: bfloat16 [4096, 2048], P('sp', 'tp'), may hold values from -0.09375 to 0.09375
- strength_weight: bfloat16 [4096, 16], P('sp', 'tp'), may hold values from -0.09375 to 0.09375
- decay_input_weight: bfloat16 [4096, 16], P('sp', 'tp'), may hold values from -0.25 to 0.25
- causal_filter_weight: bfloat16 [4, 3, 2048], replicated, may hold values from -3 to 3
- head_decay_logrates: float32 [16], replicated, may hold values from -13.2 to -2.9
- decay_input_shift: float32 [16], replicated, may hold values from -1 to 1
- strength_shift: float32 [16], replicated, may hold values from -5 to -3
- decay_spike: float32 [16384, 16], P('sp', 'tp'), may hold values from -1.3 to 0
- head_norm_scale: bfloat16 [128], replicated, may hold values from 0.099609375 to 1.8984375
- group_mixing_weight: bfloat16 [16, 128, 128], replicated, may hold values from -0.5 to 0.5
- mean_channel_scale: bfloat16 [2048], replicated, may hold values from 0.099609375 to 1.8984375
- mean_output_weight: bfloat16 [2048, 4096], P('tp', 'sp'), may hold values from -0.09375 to 0.09375
- delta_output_weight: bfloat16 [2048, 4096], P('tp', 'sp'), may hold values from -0.09375 to 0.09375
Outputs:
- mixed_out: bfloat16 [16384, 4096], P(('sp', 'tp'))
All inputs are finite; a program needn't handle non-finite values.
Results may differ from a plain program's by a relative error of at most 0.015.
Values may be sent and summed in bfloat16 or wider, within the bound.
A program may use at most 128 MiB of HBM per device.

v0:
```python
import jax
import jax.numpy as jnp
from jax import lax
from jax.sharding import Mesh
from jax.sharding import PartitionSpec as P

GROUP_DIM = 128
HEAD_DIM = 128
CONV = 4
BLOCK = 64
SP = ("sp_0", "sp_1")
SP_TP = ("sp_0", "sp_1", "tp")


EPSILON = 1e-06


def side_by_side(arrays, axis, dim, along):
    widths = [a.shape[along] for a in arrays]
    both = jnp.concatenate(arrays, axis=along)
    result = lax.all_gather(both, axis, axis=dim, tiled=True)
    return tuple(jnp.split(result, [sum(widths[:k]) for k in range(1, len(widths))], axis=along))


def shifted_2(block, axis, distance):
    devices = range(lax.axis_size(axis))
    route = [(i - distance, i) for i in devices if i - distance in devices]
    return lax.ppermute(block, axis, route)


def neutral_like(shard, identity):
    return jax.tree.map(
        lambda a, e: jnp.broadcast_to(jnp.asarray(e, a.dtype), a.shape), shard, identity
    )


def prefix_by_axis(shard, axes, combine, identity):
    before = start = neutral_like(shard, identity)
    so_far = shard
    for axis in reversed(axes):
        devices, mine = (lax.axis_size(axis), lax.axis_index(axis))
        pieces = jax.tree.map(
            lambda part, kind: lax.all_gather(part.astype(kind), axis),
            so_far,
            (jnp.bfloat16, jnp.bfloat16),
        )
        inside, so_far = (start, start)
        for k in range(devices):
            passed = k < mine
            so_far = combine(
                so_far, jax.tree.map(lambda part, own: part[k].astype(own.dtype), pieces, shard)
            )
            inside = jax.tree.map(lambda new, old: jnp.where(passed, new, old), so_far, inside)
        before = combine(inside, before)
    return before


def scale_rows(values, gain_vec):
    squares = jnp.mean(values * values, axis=-1, keepdims=True)
    return values * lax.rsqrt(squares + EPSILON) * gain_vec.astype(jnp.float32)


def unit_rows(values):
    return values * lax.rsqrt(jnp.sum(values * values, axis=-1, keepdims=True) + EPSILON)


def causal_taps(extended, taps, rows_out):
    tap_sum = jnp.zeros((rows_out, taps.shape[1]), jnp.float32)
    for tap_index in range(taps.shape[0]):
        tap_sum = tap_sum + taps[tap_index] * extended[tap_index : tap_index + rows_out]
    return jax.nn.silu(tap_sum)


def pool_means(previous, current, group_ids, positions):
    pool_reach = 15
    rows_out = current.shape[0]
    extended = jnp.concatenate([previous, current], axis=0).astype(jnp.float32)
    window_size = jnp.left_shift(jnp.int32(2), group_ids % 4)
    windowed = jnp.zeros(current.shape, jnp.float32)
    for lag_rows in range(pool_reach + 1):
        shifted = extended[pool_reach - lag_rows : pool_reach - lag_rows + rows_out]
        windowed = windowed + jnp.where(lag_rows < window_size[None, :], shifted, 0.0)
    counts = jnp.minimum(positions[:, None] + 1, window_size[None, :]).astype(jnp.float32)
    return (windowed / counts - extended[pool_reach:]).astype(jnp.bfloat16)


def unit_lower_solve(strict_part, right_side):
    power = strict_part
    solved = right_side - jnp.einsum("nhij,nhjd->nhid", power, right_side)
    for square_index in range((BLOCK - 1).bit_length() - 1):
        power = jnp.einsum("nhij,nhjk->nhik", power, power)
        solved = solved + jnp.einsum("nhij,nhjd->nhid", power, solved)
    return solved


def block_terms(query, keys, values, decay_logarithm, beta):
    blocks = keys.shape[0] // BLOCK

    def to_blocks(tensor):
        return jnp.swapaxes(tensor.reshape((blocks, BLOCK) + tensor.shape[1:]), 1, 2)

    query_b = to_blocks(query)
    keys_b = to_blocks(keys)
    values_b = to_blocks(values)
    decay_b = to_blocks(decay_logarithm)
    beta_b = to_blocks(beta)
    cumulative = jnp.cumsum(decay_b, axis=-1)
    positions = jnp.arange(BLOCK)
    causal = positions[:, None] >= positions[None, :]
    strict = positions[:, None] > positions[None, :]
    spread = cumulative[..., :, None] - cumulative[..., None, :]
    weights = jnp.where(causal, jnp.exp(jnp.where(causal, spread, 0.0)), 0.0)
    keys_beta = keys_b * beta_b[..., None]
    values_beta = values_b * beta_b[..., None]
    intersection = jnp.einsum("nhid,nhjd->nhij", keys_beta, keys_b)
    strict_part = jnp.where(strict, intersection * weights, 0.0)
    right_side = jnp.concatenate([values_beta, keys_beta * jnp.exp(cumulative)[..., None]], axis=-1)
    solved = unit_lower_solve(strict_part, right_side)
    value_depth = values.shape[-1]
    update = solved[..., :value_depth]
    project = solved[..., value_depth:]
    scores = jnp.einsum("nhid,nhjd->nhij", query_b, keys_b) * weights
    query_dec = query_b * jnp.exp(cumulative)[..., None]
    keys_dec = keys_b * jnp.exp(cumulative[..., -1:] - cumulative)[..., None]
    carry_decay = jnp.exp(cumulative[..., -1])
    return (scores, query_dec, keys_dec, update, project, carry_decay)


def run_blocks(state, terms):

    def advance(carried, inputs):
        scores, query_dec, keys_dec, update, project, carry_decay = inputs
        fresh = update - jnp.einsum("hcd,hde->hce", project, carried)
        output = jnp.einsum("hcd,hde->hce", query_dec, carried)
        output = output + jnp.einsum("hij,hje->hie", scores, fresh)
        carried = carried * carry_decay[:, None, None] + jnp.einsum("hcd,hce->hde", keys_dec, fresh)
        return (carried, output)

    final_state, outputs = lax.scan(advance, state, terms)
    return outputs


def apply_map(step_map, target):
    return jnp.einsum("hde,hef->hdf", step_map, target)


def block_maps(terms, head_count, head_depth):
    scores, query_dec, keys_dec, update, project, carry_decay = terms
    identity = jnp.eye(head_depth, dtype=jnp.float32)
    step_maps = carry_decay[..., None, None] * identity - jnp.einsum(
        "nhcd,nhce->nhde", keys_dec, project
    )
    injects = jnp.einsum("nhcd,nhce->nhde", keys_dec, update)

    def compose(carried, inputs):
        step_map, inject = inputs
        return ((apply_map(step_map, carried[0]), apply_map(step_map, carried[1]) + inject), None)

    start_maps = (
        jnp.broadcast_to(identity, (head_count, head_depth, head_depth)),
        jnp.zeros((head_count, head_depth, head_depth), jnp.float32),
    )
    composed, unused = lax.scan(compose, start_maps, (step_maps, injects))
    return composed


def per_device(
    tokens,
    input_norm_scale,
    mean_input_weight,
    query_matrix,
    key_matrix,
    value_matrix,
    strength_weight,
    decay_input_weight,
    causal_filter_weight,
    head_decay_logrates,
    decay_input_shift,
    strength_shift,
    decay_spike,
    head_norm_scale,
    group_mixing_weight,
    mean_channel_scale,
    mean_output_weight,
    delta_output_weight,
):
    tok_rows = tokens.shape[0]
    pool_cols = mean_input_weight.shape[1]
    delta_cols = query_matrix.shape[1]
    head_count = strength_weight.shape[1]
    head_depth = delta_cols // head_count
    groups_dev = pool_cols // GROUP_DIM
    tp_index = lax.axis_index("tp")
    sp_index = lax.axis_index(SP)
    normed = scale_rows(tokens.astype(jnp.float32), input_norm_scale).astype(jnp.bfloat16)
    pieces = side_by_side(
        (
            mean_input_weight,
            query_matrix,
            key_matrix,
            value_matrix,
            strength_weight,
            decay_input_weight,
        ),
        SP,
        0,
        1,
    )
    wide_part = jnp.concatenate(pieces[:4], axis=1)
    narrow_part = jnp.concatenate(pieces[4:], axis=1)
    wide_sum = jnp.dot(normed, wide_part, preferred_element_type=jnp.float32)
    narrow_sum = jnp.dot(normed, narrow_part, preferred_element_type=jnp.float32)
    pool_raw = wide_sum[:, :pool_cols].astype(jnp.bfloat16)
    qkv_raw = wide_sum[:, pool_cols:].astype(jnp.bfloat16)
    beta_raw = narrow_sum[:, :head_count].astype(jnp.bfloat16)
    decay_unshaped = narrow_sum[:, head_count:].astype(jnp.bfloat16)
    pool_reach = 15
    conv_reach = CONV - 1
    previous_pool, previous_qkv = shifted_2(
        (pool_raw[tok_rows - pool_reach :], qkv_raw[tok_rows - conv_reach :]), SP, 1
    )
    conv_local = (
        lax.dynamic_slice_in_dim(causal_filter_weight, tp_index * delta_cols, delta_cols, 2)
        .reshape(CONV, 3 * delta_cols)
        .astype(jnp.float32)
    )
    extended_qkv = jnp.concatenate([previous_qkv, qkv_raw], axis=0).astype(jnp.float32)
    convolved = causal_taps(extended_qkv, conv_local, tok_rows)
    query = unit_rows(
        convolved[:, :delta_cols].reshape(tok_rows, head_count, head_depth)
    ) * HEAD_DIM ** (-0.5)
    keys = unit_rows(
        convolved[:, delta_cols : 2 * delta_cols].reshape(tok_rows, head_count, head_depth)
    )
    values = convolved[:, 2 * delta_cols :].reshape(tok_rows, head_count, head_depth)
    rate_logarithm = lax.dynamic_slice_in_dim(
        head_decay_logrates, tp_index * head_count, head_count
    )
    shift_amounts = lax.dynamic_slice_in_dim(decay_input_shift, tp_index * head_count, head_count)
    strength_offsets = lax.dynamic_slice_in_dim(strength_shift, tp_index * head_count, head_count)
    beta = jax.nn.sigmoid(beta_raw.astype(jnp.float32) + strength_offsets)
    decay_logarithm = (
        -jnp.exp(rate_logarithm)
        * jax.nn.softplus(decay_unshaped.astype(jnp.float32) + shift_amounts)
        + decay_spike
    )
    terms = block_terms(query, keys, values, decay_logarithm, beta)
    transfer_map, offset_map = block_maps(terms, head_count, head_depth)

    def combine_maps(earlier, later):
        return (apply_map(later[0], earlier[0]), apply_map(later[0], earlier[1]) + later[1])

    identity_stack = jnp.broadcast_to(jnp.eye(head_depth, dtype=jnp.float32), transfer_map.shape)
    prefix = prefix_by_axis(
        (transfer_map, offset_map), SP, combine_maps, (identity_stack, jnp.zeros_like(offset_map))
    )
    incoming = prefix[1]
    outputs = run_blocks(incoming, terms)
    delta_rows = jnp.swapaxes(outputs, 1, 2).reshape(tok_rows, head_count, head_depth)
    delta_mixed = (
        scale_rows(delta_rows, head_norm_scale).astype(jnp.bfloat16).reshape(tok_rows, delta_cols)
    )
    group_ids = tp_index * groups_dev + jnp.arange(pool_cols) // GROUP_DIM
    positions = sp_index * tok_rows + jnp.arange(tok_rows)
    pool_diff = pool_means(previous_pool, pool_raw, group_ids, positions)
    local_mix = lax.dynamic_slice_in_dim(group_mixing_weight, tp_index * groups_dev, groups_dev, 0)
    pooled = jnp.einsum(
        "tgc,gcd->tgd",
        pool_diff.reshape(tok_rows, groups_dev, GROUP_DIM),
        local_mix,
        preferred_element_type=jnp.float32,
    )
    pool_scale = lax.dynamic_slice_in_dim(mean_channel_scale, tp_index * pool_cols, pool_cols)
    pool_mixed = (pooled.reshape(tok_rows, pool_cols) * pool_scale.astype(jnp.float32)).astype(
        jnp.bfloat16
    )
    mixed = jnp.concatenate([pool_mixed, delta_mixed], axis=1)
    pool_weight_rows, delta_weight_rows = side_by_side(
        (mean_output_weight, delta_output_weight), SP, 1, 0
    )
    out_weight = jnp.concatenate([pool_weight_rows, delta_weight_rows], axis=0)
    return lax.psum_scatter(
        jnp.dot(mixed, out_weight, preferred_element_type=jnp.float32).astype(jnp.bfloat16),
        "tp",
        scatter_dimension=0,
        tiled=True,
    )


def solution(mesh):
    finer = Mesh(mesh.devices.reshape(4, 4, mesh.shape["tp"]), ("sp_0", "sp_1", "tp"))
    in_specs = (
        P(SP, None),
        P(),
        P(SP, "tp"),
        P(SP, "tp"),
        P(SP, "tp"),
        P(SP, "tp"),
        P(SP, "tp"),
        P(SP, "tp"),
        P(),
        P(),
        P(),
        P(),
        P(SP, "tp"),
        P(),
        P(),
        P(),
        P("tp", SP),
        P("tp", SP),
    )
    out_specs = P(SP_TP, None)
    return jax.shard_map(
        per_device, mesh=finer, in_specs=in_specs, out_specs=out_specs, check_vma=False
    )
```

profile of v0, /device:TPU:1, one launch (start us, length us, event | category | flops | bytes accessed | tf_op | source)
XLA Modules:
  0.0 373.8 jit_solution(8501153216190759372)
XLA Ops:
  20.1 5.2 %fusion.27 = f32[1024]{0:T(1024)S(1)} fusion(bf16[1024,4096]{1,0:T(8,128)(2,1)} %param.22), kind=kLoop, calls=%fused_computation.34 | loop fusion | flops 12581888 | bytes 8392704 | tf_op jit(solution)/shard_map/reduce_sum | solution.py:59
  28.5 60.5 %all-gather.7.cloned.1.call-done = bf16[4096,1028]{1,0:T(8,128)(2,1)} async-done(((bf16[256,1028]{1,0:T(8,128)(2,1)}), bf16[4096,1028]{1,0:T(8,128)(2,1)}) %all-gather.7.cloned.1.call-update) | async-done | bytes 8421392 | tf_op jit(solution)/shard_map/all_gather | solution.py:21
  89.0 6.0 %fusion.65 = bf16[1024,4]{0,1:T(4,128)(2,1)S(1)} fusion(bf16[1024,4096]{1,0:T(8,128)(2,1)} %param.22, f32[4096]{0:T(1024)S(1)} %convert_element_type.138, f32[1024]{0:T(1024)S(1)} %add_rsqrt_fusion.2, bf16[4096,1028]{1,0:T(8,128)(2,1)} %all-gather.7.cloned.1.call-done), kind=kOutput, calls=%fused_computation.81 | convolution fusion | flops 50335744 | bytes 9465856 | tf_op jit(solution)/shard_map/dot_general | solution.py:212
  95.2 13.8 %fusion.38 = bf16[1024,1024]{1,0:T(8,128)(2,1)S(1)} fusion(bf16[4096,1028]{1,0:T(8,128)(2,1)} %all-gather.7.cloned.1.call-done, bf16[1024,4096]{1,0:T(8,128)(2,1)} %param.22, f32[4096]{0:T(1024)S(1)} %convert_element_type.138, f32[1024]{0:T(1024)S(1)} %add_rsqrt_fusion.2), kind=kOutput, calls=%fused_computation.51 | convolution fusion | flops 8607760384 | bytes 18894848 | tf_op jit(solution)/shard_map/dot_general | solution.py:211
  109.0 3.1 collective-permute-start.1
  115.7 3.3 collective-permute-start
  119.3 1.9 divide_multiply_fusion
  121.2 2.2 slice_multiply_fusion.4
  127.3 2.1 mul.268
  132.6 2.8 reshape_reshape.3
  138.5 2.1 bitcast_multiply_fusion.2
  145.9 3.1 convolution_add_fusion.5
  149.0 4.7 %convolution_add_fusion.4 = f32[16,2,64,256]{3,2,1,0:T(8,128)} fusion(bf16[16,2,64,64]{3,2,1,0:T(8,128)(2,1)} %copy-done.6, f32[16,2,64,256]{3,2,1,0:T(8,128)} %convolution_add_fusion.5, bf16[16,2,64,64]{3,2,1,0:T(8,128)(2,1)} %copy-done.5), kind=kOutput, calls=%fused_computation.54 | convolution fusion | flops 135266304 | bytes 4718592 | tf_op jit(solution)/shard_map/nhij,nhjd->nhid/dot_general | solution.py:92
  153.7 3.1 convolution_add_fusion.3
  159.4 1.9 fusion.155
  162.9 34.3 %while.26 = (s32[]{:T(128)}, bf16[2,128,128]{2,1,0:T(8,128)(2,1)S(1)}, bf16[2,128,128]{2,1,0:T(8,128)(2,1)S(1)}, bf16[16,2,128,128]{3,2,1,0:T(8,128)(2,1)}, f32[...) while((s32[]{:T(128)}, bf16[2,128,128]{2,1,0:T(8,128)(2,1)S(1)}, ...), condition=%wide.region_4.5_spmd.clone, body=%wide.region_3.4_spmd.clone.sunk | while | flops 16875524 | bytes 788055 | solution.py:163
  197.2 9.9 %all-gather = bf16[8,128,128]{2,1,0:T(8,128)(2,1)S(1)} all-gather(bf16[2,128,128]{2,1,0:T(8,128)(2,1)S(1)} %get-tuple-element.80), channel_id=2, replica_groups=mesh['sp_0'=4,'sp_1'=4,'tp'=8] {'sp_1'}, dimensions={0}, use_global_device_ids=true | all-gather | bytes 327680 | tf_op jit(solution)/shard_map/all_gather | solution.py:43
  207.2 9.5 %all-gather.2 = bf16[8,128,128]{2,1,0:T(8,128)(2,1)S(1)} all-gather(bf16[2,128,128]{2,1,0:T(8,128)(2,1)S(1)} %get-tuple-element.81), channel_id=4, replica_groups=mesh['sp_0'=4,'sp_1'=4,'tp'=8] {'sp_1'}, dimensions={0}, use_global_device_ids=true | all-gather | bytes 327680 | tf_op jit(solution)/shard_map/all_gather | solution.py:43
  217.5 9.4 %all-gather.3 = bf16[8,128,128]{2,1,0:T(8,128)(2,1)S(1)} all-gather(bf16[2,128,128]{2,1,0:T(8,128)(2,1)S(1)} %convolution_add_fusion.9), channel_id=5, replica_groups=mesh['sp_0'=4,'sp_1'=4,'tp'=8] {'sp_0'}, dimensions={0}, use_global_device_ids=true | all-gather | bytes 327680 | tf_op jit(solution)/shard_map/all_gather | solution.py:43
  227.6 10.3 %all-gather.1 = bf16[8,128,128]{2,1,0:T(8,128)(2,1)S(1)} all-gather(bf16[2,128,128]{2,1,0:T(8,128)(2,1)S(1)} %fusion.165), channel_id=3, replica_groups=mesh['sp_0'=4,'sp_1'=4,'tp'=8] {'sp_0'}, dimensions={0}, use_global_device_ids=true | all-gather | bytes 327680 | tf_op jit(solution)/shard_map/all_gather | solution.py:43
  242.1 47.9 %while.25 = (s32[]{:T(128)}, f32[2,128,128]{2,1,0:T(8,128)S(1)}, f32[16,2,64,128]{3,2,1,0:T(8,128)S(1)}, f32[16,2]{1,0:T(8,128)S(1)}, bf16[16,2,64,128]{3,2,1,0:...) while((s32[]{:T(128)}, f32[2,128,128]{2,1,0:T(8,128)S(1)}, ...), condition=%wide.region_7.8_spmd, body=%wide.region_6.7_spmd.sunk | while | flops 14794754 | bytes 1019005 | solution.py:139
  293.4 3.0 fusion.97
  296.9 9.0 %convolution_convert_fusion = bf16[1024,4096]{1,0:T(8,128)(2,1)} fusion(bf16[512,4096]{1,0:T(8,128)(2,1)} %all-gather.9.cloned.1.call-done, bf16[1024,256]{1,0:T(8,128)(2,1)S(1)} %fusion.69, bf16[1024,256]{1,0:T(8,128)(2,1)S(1)} %multiply_convert_fusion), kind=kOutput, calls=%fused_computation.39 | convolution fusion | flops 4301258752 | bytes 13631488 | tf_op jit(solution)/shard_map/dot_general | solution.py:283
  305.9 61.4 %reduce-scatter.2.cloned.1.call-done = bf16[128,4096]{1,0:T(8,128)(2,1)} async-done(((bf16[1024,4096]{1,0:T(8,128)(2,1)}), bf16[128,4096]{1,0:T(8,128)(2,1)}) %reduce-scatter.2.cloned.1.call-update) | async-done | bytes 1048592 | tf_op jit(solution)/shard_map/reduce_scatter | solution.py:282
  (324 shorter events, 130.2 us)
Async XLA Ops:
  6.5 286.7 %copy-start = (bf16[16,128,128]{2,1,0:T(8,128)(2,1)S(1)}, bf16[16,128,128]{2,1,0:T(8,128)(2,1)}, u32[]{:S(2)}) copy-start(bf16[16,128,128]{2,1,0:T(8,128)(2,1)} %param.36) | copy-start | bytes 1572868
  6.5 82.5 %all-gather.7.cloned.1.call-start = ((), (), s32[]{:S(2)}) async-start(), calls=%async_computation.1 | async-start | bytes 10027008 | tf_op jit(solution)/shard_map/all_gather | solution.py:21
  10.1 286.7 %all-gather.9.cloned.1.call-start = ((), (), s32[]{:S(2)}) async-start(), calls=%async_computation.2 | async-start | bytes 4456448 | tf_op jit(solution)/shard_map/all_gather | solution.py:21
  11.9 355.4 %reduce-scatter.2.cloned.1.call-start = ((), (), s32[]{:S(2)}) async-start(), calls=%async_computation.3 | async-start | bytes 9437184 | tf_op jit(solution)/shard_map/reduce_scatter | solution.py:282
  20.0 6.0 %copy-start.20 = (bf16[128]{0:T(256)(128)(2,1)S(1)}, bf16[128]{0:T(256)(128)(2,1)}, u32[]{:S(2)}) copy-start(bf16[128]{0:T(256)(128)(2,1)} %param.35) | copy-start | bytes 772
  28.5 66.5 %copy-start.16 = (f32[1024,2]{0,1:T(2,128)S(1)}, f32[1024,2]{0,1:T(2,128)}, u32[]{:S(2)}) copy-start(f32[1024,2]{0,1:T(2,128)} %param.34) | copy-start | bytes 24580
  109.0 3.8 %copy-start.11 = (bf16[1024,1024]{1,0:T(8,128)(2,1)}, bf16[1024,1024]{1,0:T(8,128)(2,1)S(1)}, u32[]{:S(2)}) copy-start(bf16[1024,1024]{1,0:T(8,128)(2,1)S(1)} %fusion.38) | copy-start | bytes 6291460
  109.0 10.0 %collective-permute-start.1 = (bf16[3,768]{1,0:T(4,128)(2,1)S(1)}, bf16[3,768]{1,0:T(4,128)(2,1)S(1)}, u32[]{:S(2)}, u32[]{:S(2)}) collective-permute-start(bf16[3,768]{1,0:T(4,128)(2,1)S(1)} %slice.260), channel_id=1, source_target_pairs={{0,8},{8,16},{16,24},{24,32},{32,40},{40,48},{48,56},{56,64},{64,7... | collective-permute-start | bytes 13832 | tf_op jit(solution)/shard_map/ppermute | solution.py:28
  112.9 2.1 copy-start.12
  115.7 177.3 %collective-permute-start = (bf16[15,256]{1,0:T(8,128)(2,1)}, bf16[15,256]{1,0:T(8,128)(2,1)S(1)}, u32[]{:S(2)}, u32[]{:S(2)}) collective-permute-start(bf16[15,256]{1,0:T(8,128)(2,1)} %slice.239), channel_id=1, source_target_pairs={{0,8},{8,16},{16,24},{24,32},{32,40},{40,48},{48,56},{56,64},{64,7... | collective-permute-start | bytes 23048 | tf_op jit(solution)/shard_map/ppermute | solution.py:28
  127.3 9.5 %copy-start.2 = (f32[16,64,2,128]{3,2,1,0:T(2,128)}, f32[16,64,2,128]{3,2,1,0:T(2,128)S(1)}, u32[]{:S(2)}) copy-start(f32[16,64,2,128]{3,2,1,0:T(2,128)S(1)} %reshape.236) | copy-start | bytes 3145732
  135.4 3.2 copy-start.10
  138.5 2.1 copy-start.3
  142.3 3.6 copy-start.8
  149.0 4.7 %copy-start.7 = (bf16[16,2,64,64]{3,2,1,0:T(8,128)(2,1)S(1)}, bf16[16,2,64,64]{3,2,1,0:T(8,128)(2,1)}, u32[]{:S(2)}) copy-start(bf16[16,2,64,64]{3,2,1,0:T(8,128)(2,1)} %fusion.162) | copy-start | bytes 786436
  156.8 4.5 %copy-start.1 = (f32[16,2,64,256]{3,2,1,0:T(8,128)}, f32[16,2,64,256]{3,2,1,0:T(8,128)S(1)}, u32[]{:S(2)}) copy-start(f32[16,2,64,256]{3,2,1,0:T(8,128)S(1)} %convolution_add_fusion.3) | copy-start | bytes 6291460
  156.8 2.0 copy-start.4
  207.2 34.9 %slice-start = ((f32[16,2,64,256]{3,2,1,0:T(8,128)}), f32[16,2,64,128]{3,2,1,0:T(8,128)S(1)}, s32[]{:S(2)}) async-start(f32[16,2,64,256]{3,2,1,0:T(8,128)} %copy-done.1), calls=%async_computation.4 | async-start | bytes 2097152 | tf_op jit(solution)/shard_map/slice | solution.py:120
  207.2 34.9 %copy-start.9 = (f32[16,2,64,128]{3,2,1,0:T(8,128)S(1)}, f32[16,2,64,128]{3,2,1,0:T(8,128)}, u32[]{:S(2)}) copy-start(f32[16,2,64,128]{3,2,1,0:T(8,128)} %custom-call.1) | copy-start | bytes 3145732
  217.3 9.7 %copy-start.13 = (bf16[2,128,128]{2,1,0:T(8,128)(2,1)}, bf16[2,128,128]{2,1,0:T(8,128)(2,1)S(1)}, u32[]{:S(2)}) copy-start(bf16[2,128,128]{2,1,0:T(8,128)(2,1)S(1)} %convolution_add_fusion.10) | copy-start | bytes 196612
  227.1 10.8 %copy-start.15 = (bf16[2,128,128]{2,1,0:T(8,128)(2,1)}, bf16[2,128,128]{2,1,0:T(8,128)(2,1)S(1)}, u32[]{:S(2)}) copy-start(bf16[2,128,128]{2,1,0:T(8,128)(2,1)S(1)} %fusion.164) | copy-start | bytes 196612
  289.9 2.9 copy-start.19
  290.6 2.5 slice-start.1
  293.4 3.4 copy-start.18
  (21 other events, 34.3 us)
Sparse Core Ops, SparseCore 0:
  10.3 78.7 all-gather.6
  91.1 55.3 all-gather.8
  306.0 61.2 reduce-scatter.1
where the time goes:
time: 379 us; the launch traced here: 374 us
  matrix products  137 us (36%)
  waiting for transfers between devices  122 us (32%)
  blocking collectives  39.1 us (10%)
  other arithmetic  28.5 us (8%)
  local copies, waits for them, and re-layouts  25.1 us (7%)
  between operations  14 us (4%)
  starting transfers between devices  6.45 us (2%)
    reduce_scatter x1, waiting for transfers between devices, per_device(): lax.psum_scatter(jnp.dot(mixed, out_weight, preferred_element_type=jnp.fl...  61.4 us
    all_gather x2, waiting for transfers between devices, side_by_side(): result = lax.all_gather(both, axis, axis=dim, tiled=True)  60.6 us
    all_gather x4, blocking collectives, prefix_by_axis(): lax.all_gather(part.astype(kind), axis)  39.1 us
    dot_general x46, matrix products, apply_map(): return jnp.einsum('hde,hef->hdf', step_map, target)  38.9 us
    dot_general x16, matrix products, advance(): fresh = update - jnp.einsum('hcd,hde->hce', project, carried)  14.4 us
    dot_general x16, matrix products, advance(): output = jnp.einsum('hcd,hde->hce', query_dec, carried)  14.4 us
    dot_general x16, matrix products, advance(): output = output + jnp.einsum('hij,hje->hie', scores, fresh)  14.2 us
    dot_general x1, matrix products, per_device(): wide_sum = jnp.dot(normed, wide_part, preferred_element_type=jnp.float32)  13.8 us
  transfers between devices with their start and end apart: 5, of which 2 were waited for; matrix products, arithmetic and copies ran while one was open for 47% of the time, Pallas kernels for 0%

commit v1 on v0

v1 whole, which is shorter than its diff:
```python
import jax
import jax.numpy as jnp
from jax import lax
from jax.experimental import pallas as pl
from jax.experimental.pallas import tpu as pltpu
from jax.sharding import Mesh
from jax.sharding import PartitionSpec as P

GROUP_DIM = 128
HEAD_DIM = 128
CONV = 4
CHUNK = 256
HALO = 16
EPSILON = 1e-06
SP = ("sp_0", "sp_1")
SP_TP = ("sp_0", "sp_1", "tp")
MESH_ID = pl.DeviceIdType.MESH
F32 = jnp.float32
BF16 = jnp.bfloat16
VMEM_LIMIT = 60 * 1024 * 1024


def dot(a, b):
    return jnp.dot(a, b, preferred_element_type=F32)


def dot_nt(a, b):
    return lax.dot_general(a, b, (((1,), (1,)), ((), ())), preferred_element_type=F32)


def dot_tn(a, b):
    return lax.dot_general(a, b, (((0,), (0,)), ((), ())), preferred_element_type=F32)


def unit_rows(values):
    return values * lax.rsqrt(jnp.sum(values * values, axis=-1, keepdims=True) + EPSILON)


def fill_masks(masks_ref):
    rows = lax.broadcasted_iota(jnp.int32, (CHUNK, CHUNK), 0)
    cols = lax.broadcasted_iota(jnp.int32, (CHUNK, CHUNK), 1)
    apart = jnp.bitwise_xor(rows, cols)
    for level in range(masks_ref.shape[0]):
        inside = (rows > cols) & (apart >= 2**level) & (apart < 2 ** (level + 1))
        masks_ref[level] = jnp.where(inside, 1.0, 0.0).astype(BF16)


def fill_gates(beta, decay, grow_ref, gcol_ref, bcol_ref):
    lane = lax.broadcasted_iota(jnp.int32, decay.shape, 1)
    total = decay
    step = 1
    while step < CHUNK:
        total = total + jnp.where(lane >= step, pltpu.roll(total, step, 1), 0.0)
        step *= 2
    for row in range(decay.shape[0]):
        grow_ref[row] = jnp.broadcast_to(total[row : row + 1], (8, CHUNK))
        gcol_ref[row] = jnp.broadcast_to(total[row : row + 1], (128, CHUNK)).T
        bcol_ref[row] = jnp.broadcast_to(beta[row : row + 1], (128, CHUNK)).T


def conv_rows(raw_ref, taps_ref, start, part):
    lanes = slice(part * 128, part * 128 + 128)
    rows = raw_ref[pl.ds(pl.multiple_of(start + HALO - 8, 8), CHUNK + 8), lanes]
    mixed = taps_ref[CONV - 1 : CONV, lanes] * rows[8:]
    for back in range(1, CONV):
        tap = taps_ref[CONV - 1 - back : CONV - back, lanes]
        mixed = mixed + tap * pltpu.roll(rows, back, 0)[8:]
    return mixed / (1.0 + jnp.exp(-mixed))


def delta_chunk(chunk, heads, chunks, raw_ref, taps_ref, grow_ref, gcol_ref, bcol_ref, masks_ref,
                map_ref, from_state_ref, local_ref):
    start = chunk * CHUNK
    rows = lax.broadcasted_iota(jnp.int32, (CHUNK, CHUNK), 0)
    cols = lax.broadcasted_iota(jnp.int32, (CHUNK, CHUNK), 1)
    work = []
    for head in range(heads):
        row = head * chunks + chunk
        query = unit_rows(conv_rows(raw_ref, taps_ref, start, head)) * HEAD_DIM ** (-0.5)
        key = unit_rows(conv_rows(raw_ref, taps_ref, start, heads + head))
        value = conv_rows(raw_ref, taps_ref, start, 2 * heads + head)
        gcol, bcol, grow = gcol_ref[row], bcol_ref[row], grow_ref[row][0:1]
        key_b = key.astype(BF16)
        both = jnp.concatenate([query.astype(BF16), key_b], axis=0)
        inner = dot_nt(both, key_b)
        spread = jnp.exp(jnp.minimum(jnp.concatenate([gcol, gcol], axis=1) - grow, 0.0))
        scores = jnp.where(rows >= cols, inner[:CHUNK] * spread, 0.0).astype(BF16)
        strict = jnp.where(rows > cols, inner[CHUNK:] * spread, 0.0)
        strict = (strict * jnp.concatenate([bcol, bcol], axis=1)).astype(BF16)
        grown = jnp.exp(gcol)
        right = jnp.concatenate([value * bcol, key * bcol * grown], axis=1).astype(BF16)
        last = grow[:, CHUNK - 1 : CHUNK]
        key_dec = (key * jnp.exp(last - gcol)).astype(BF16)
        inverse = jnp.where(rows == cols, 1.0, 0.0).astype(BF16) - strict * masks_ref[0]
        work.append([strict, inverse, scores, right, key_dec, query * grown, jnp.exp(last)])
    for level in range(1, masks_ref.shape[0]):
        inner = [dot(w[0] * masks_ref[level], w[1]).astype(BF16) for w in work]
        for w, part in zip(work, inner):
            w[1] = w[1] - dot(w[1], part).astype(BF16)
    for head in range(heads):
        _, inverse, scores, right, key_dec, query_dec, kept = work[head]
        solved = dot(inverse, right).astype(BF16)
        seen = dot(scores, solved)
        moved = dot_tn(key_dec, solved)
        current = map_ref[head]
        current_b = current.astype(BF16)
        asked = (query_dec - seen[:, 128:]).astype(BF16)
        answer = dot(asked, current_b)
        where_rows = pl.ds(pl.multiple_of(start, CHUNK), CHUNK)
        from_state_ref[head, where_rows, :] = answer[:, :128].astype(BF16)
        local_ref[head, where_rows, :] = answer[:, 128:] + seen[:, :128]
        added = jnp.concatenate([jnp.zeros((128, 128), F32), moved[:, :128]], axis=1)
        map_ref[head] = current * kept - dot(moved[:, 128:].astype(BF16), current_b) + added


def local_kernel(heads, chunks, raw_ref, taps_ref, beta_ref, decay_ref, from_state_ref, local_ref,
                 map_out_ref, grow_ref, gcol_ref, bcol_ref, masks_ref, map_ref):
    fill_masks(masks_ref)
    fill_gates(beta_ref[...], decay_ref[...], grow_ref, gcol_ref, bcol_ref)
    rows = lax.broadcasted_iota(jnp.int32, (128, 256), 0)
    cols = lax.broadcasted_iota(jnp.int32, (128, 256), 1)
    for head in range(heads):
        map_ref[head] = jnp.where(rows == cols, 1.0, 0.0)

    @pl.loop(0, chunks)
    def _(chunk):
        delta_chunk(chunk, heads, chunks, raw_ref, taps_ref, grow_ref, gcol_ref, bcol_ref,
                    masks_ref, map_ref, from_state_ref, local_ref)

    map_out_ref[...] = map_ref[...].astype(BF16)


def local_maps(raw, taps, beta, decay, heads):
    tok_rows = raw.shape[0] - HALO
    chunks = tok_rows // CHUNK
    vmem = pl.BlockSpec(memory_space=pltpu.VMEM)
    return pl.pallas_call(
        lambda *refs: local_kernel(heads, chunks, *refs),
        out_shape=(
            jax.ShapeDtypeStruct((heads, tok_rows, 128), BF16),
            jax.ShapeDtypeStruct((heads, tok_rows, 128), F32),
            jax.ShapeDtypeStruct((heads, 128, 256), BF16),
        ),
        in_specs=[vmem] * 4,
        out_specs=(vmem, vmem, vmem),
        scratch_shapes=[
            pltpu.VMEM((heads * chunks, 8, CHUNK), F32),
            pltpu.VMEM((heads * chunks, CHUNK, 128), F32),
            pltpu.VMEM((heads * chunks, CHUNK, 128), F32),
            pltpu.VMEM((8, CHUNK, CHUNK), BF16),
            pltpu.VMEM((heads, 128, 256), F32),
        ],
        compiler_params=pltpu.CompilerParams(vmem_limit_bytes=VMEM_LIMIT),
        name="local_maps",
    )(raw, taps, beta, decay)


def after(later, earlier):
    offset = jnp.concatenate([jnp.zeros((128, 128), F32), later[:, 128:].astype(F32)], axis=1)
    return dot(later[:, :128], earlier.astype(BF16)) + offset


def prefix_kernel(heads, n_z, n_x, own_ref, state_ref, row_ref, total_ref, column_ref, send_x,
                  recv_x, send_z, recv_z):
    z, x = lax.axis_index("sp_0"), lax.axis_index("sp_1")
    barrier = pltpu.get_barrier_semaphore()
    for step in range(1, n_x):
        to = lax.rem(x + step, n_x)
        pl.semaphore_signal(barrier, 1, device_id={"sp_1": to}, device_id_type=MESH_ID)
    for step in range(1, n_z):
        to = lax.rem(z + step, n_z)
        pl.semaphore_signal(barrier, 1, device_id={"sp_0": to}, device_id_type=MESH_ID)
    pl.semaphore_wait(barrier, n_x + n_z - 2)

    copies = []
    for step in range(1, n_x):
        copy = pltpu.make_async_remote_copy(
            src_ref=own_ref, dst_ref=row_ref.at[step], send_sem=send_x.at[step],
            recv_sem=recv_x.at[step], device_id={"sp_1": lax.rem(x + step, n_x)},
            device_id_type=MESH_ID)
        copy.start()
        copies.append(copy)
    row_ref[0] = own_ref[...]
    for copy in copies:
        copy.wait()
    inside, total = [None] * heads, [None] * heads
    rows = lax.broadcasted_iota(jnp.int32, (128, 256), 0)
    cols = lax.broadcasted_iota(jnp.int32, (128, 256), 1)
    identity = jnp.where(rows == cols, 1.0, 0.0)
    for head in range(heads):
        so_far = identity
        before = identity
        for k in range(n_x):
            piece = row_ref[lax.rem(x - k + n_x, n_x), head]
            so_far = piece.astype(F32) if k == 0 else after(piece, so_far)
            before = jnp.where(k < x, so_far, before)
        inside[head] = before
        total_ref[head] = so_far.astype(BF16)
    copies = []
    for step in range(1, n_z):
        copy = pltpu.make_async_remote_copy(
            src_ref=total_ref, dst_ref=column_ref.at[step], send_sem=send_z.at[step],
            recv_sem=recv_z.at[step], device_id={"sp_0": lax.rem(z + step, n_z)},
            device_id_type=MESH_ID)
        copy.start()
        copies.append(copy)
    column_ref[0] = total_ref[...]
    for copy in copies:
        copy.wait()
    for head in range(heads):
        so_far = jnp.zeros((128, 128), F32)
        state = so_far
        for k in range(n_z - 1):
            piece = column_ref[lax.rem(z - k + n_z, n_z), head]
            offset = piece[:, 128:].astype(F32)
            so_far = offset if k == 0 else dot(piece[:, :128], so_far.astype(BF16)) + offset
            state = jnp.where(k < z, so_far, state)
        entering = dot(inside[head][:, :128].astype(BF16), state.astype(BF16))
        state_ref[head] = (entering + inside[head][:, 128:]).astype(BF16)


def incoming_state(own, n_z, n_x):
    heads = own.shape[0]
    vmem = pl.BlockSpec(memory_space=pltpu.VMEM)
    return pl.pallas_call(
        lambda *refs: prefix_kernel(heads, n_z, n_x, *refs),
        out_shape=jax.ShapeDtypeStruct((heads, 128, 128), BF16),
        in_specs=[vmem],
        out_specs=vmem,
        scratch_shapes=[
            pltpu.VMEM((n_x, heads, 128, 256), BF16),
            pltpu.VMEM((heads, 128, 256), BF16),
            pltpu.VMEM((n_z, heads, 128, 256), BF16),
            pltpu.SemaphoreType.DMA((n_x,)),
            pltpu.SemaphoreType.DMA((n_x,)),
            pltpu.SemaphoreType.DMA((n_z,)),
            pltpu.SemaphoreType.DMA((n_z,)),
        ],
        compiler_params=pltpu.CompilerParams(collective_id=0, has_side_effects=True),
        name="incoming_state",
    )(own)


def pooled_rows(pool_ref, position, wide, mix_ref, scale_ref, out_ref, start):
    for group in range(2):
        lanes = slice(group * 128, group * 128 + 128)
        rows = pool_ref[pl.ds(pl.multiple_of(start, 8), CHUNK + HALO), lanes]
        reach = 1
        sums = rows
        for _ in range(group + 1):
            sums = sums + pltpu.roll(sums, reach, 0)
            reach *= 2
        broad = sums
        for _ in range(2):
            broad = broad + pltpu.roll(broad, reach, 0)
            reach *= 2
        short, long = 2 << group, 8 << group
        seen = lax.broadcasted_iota(jnp.int32, (CHUNK, 128), 0) + (position + 1)
        count = jnp.minimum(seen, jnp.where(wide, long, short)).astype(F32)
        window = jnp.where(wide, broad[HALO:], sums[HALO:])
        diff = (window / count - rows[HALO:]).astype(BF16)
        mixed = dot(diff, mix_ref[group]) * scale_ref[0:1, lanes]
        out_ref[pl.ds(pl.multiple_of(start, CHUNK), CHUNK), lanes] = mixed.astype(BF16)


def finish_kernel(heads, chunks, from_state_ref, local_ref, state_ref, gain_ref, pool_ref, mix_ref,
                  scale_ref, out_ref):
    tok_rows = chunks * CHUNK
    token = (lax.axis_index("sp_0") * lax.axis_size("sp_1") + lax.axis_index("sp_1")) * tok_rows
    wide = lax.rem(lax.axis_index("tp"), 2) == 1

    @pl.loop(0, chunks)
    def _(chunk):
        start = chunk * CHUNK
        where_rows = pl.ds(pl.multiple_of(start, CHUNK), CHUNK)
        pooled_rows(pool_ref, token + start, wide, mix_ref, scale_ref, out_ref, start)
        for head in range(heads):
            raw = dot(from_state_ref[head, where_rows, :], state_ref[head])
            raw = raw + local_ref[head, where_rows, :]
            squares = jnp.mean(raw * raw, axis=-1, keepdims=True)
            normed = raw * lax.rsqrt(squares + EPSILON) * gain_ref[...]
            out_ref[where_rows, 256 + head * 128 : 384 + head * 128] = normed.astype(BF16)


def finish(from_state, local, state, gain, pool_raw, mix, scale):
    heads, tok_rows, _ = from_state.shape
    vmem = pl.BlockSpec(memory_space=pltpu.VMEM)
    return pl.pallas_call(
        lambda *refs: finish_kernel(heads, tok_rows // CHUNK, *refs),
        out_shape=jax.ShapeDtypeStruct((tok_rows, 512), BF16),
        in_specs=[vmem] * 7,
        out_specs=vmem,
        compiler_params=pltpu.CompilerParams(vmem_limit_bytes=VMEM_LIMIT),
        name="finish",
    )(from_state, local, state, gain, pool_raw, mix, scale)


def side_by_side(arrays, axis, dim, along):
    widths = [a.shape[along] for a in arrays]
    both = jnp.concatenate(arrays, axis=along)
    result = lax.all_gather(both, axis, axis=dim, tiled=True)
    return tuple(jnp.split(result, [sum(widths[:k]) for k in range(1, len(widths))], axis=along))


def shifted(block, axis, distance):
    devices = range(lax.axis_size(axis))
    route = [(i - distance, i) for i in devices if i - distance in devices]
    return lax.ppermute(block, axis, route)


def scale_rows(values, gain_vec):
    squares = jnp.mean(values * values, axis=-1, keepdims=True)
    return values * lax.rsqrt(squares + EPSILON) * gain_vec.astype(F32)


def per_device(tokens, input_norm_scale, mean_input_weight, query_matrix, key_matrix, value_matrix,
               strength_weight, decay_input_weight, causal_filter_weight, head_decay_logrates,
               decay_input_shift, strength_shift, decay_spike, head_norm_scale,
               group_mixing_weight, mean_channel_scale, mean_output_weight, delta_output_weight):
    tok_rows = tokens.shape[0]
    pool_cols = mean_input_weight.shape[1]
    delta_cols = query_matrix.shape[1]
    heads = strength_weight.shape[1]
    groups = pool_cols // GROUP_DIM
    chunks = tok_rows // CHUNK
    tp = lax.axis_index("tp")
    normed = scale_rows(tokens.astype(F32), input_norm_scale).astype(BF16)
    pieces = side_by_side(
        (mean_input_weight, query_matrix, key_matrix, value_matrix, strength_weight,
         decay_input_weight), SP, 0, 1)
    wide = jnp.dot(normed, jnp.concatenate(pieces[:4], axis=1), preferred_element_type=F32)
    narrow = jnp.dot(normed, jnp.concatenate(pieces[4:], axis=1), preferred_element_type=F32)
    before = shifted(wide[tok_rows - HALO :].astype(BF16), SP, 1)
    extended = jnp.concatenate([before.astype(F32), wide], axis=0)
    taps = lax.dynamic_slice_in_dim(causal_filter_weight, tp * delta_cols, delta_cols, 2)
    taps = taps.reshape(CONV, 3 * delta_cols).astype(F32)

    def own(vector):
        return lax.dynamic_slice_in_dim(vector, tp * heads, heads)

    beta = jax.nn.sigmoid(narrow[:, :heads] + own(strength_shift))
    decay = (-jnp.exp(own(head_decay_logrates))
             * jax.nn.softplus(narrow[:, heads:] + own(decay_input_shift)) + decay_spike)
    from_state, local, own_map = local_maps(
        extended[:, pool_cols:], taps, beta.T.reshape(heads * chunks, CHUNK),
        decay.T.reshape(heads * chunks, CHUNK), heads)
    state = incoming_state(own_map, lax.axis_size("sp_0"), lax.axis_size("sp_1"))
    mix = lax.dynamic_slice_in_dim(group_mixing_weight, tp * groups, groups, 0)
    scale = lax.dynamic_slice_in_dim(mean_channel_scale, tp * pool_cols, pool_cols)
    mixed = finish(from_state, local, state, head_norm_scale.astype(F32).reshape(1, HEAD_DIM),
                   extended[:, :pool_cols], mix, scale.astype(F32).reshape(1, pool_cols))
    out_weight = jnp.concatenate(
        side_by_side((mean_output_weight, delta_output_weight), SP, 1, 0), axis=0)
    return lax.psum_scatter(
        jnp.dot(mixed, out_weight, preferred_element_type=F32).astype(BF16),
        "tp", scatter_dimension=0, tiled=True)


def solution(mesh):
    finer = Mesh(mesh.devices.reshape(4, 4, mesh.shape["tp"]), SP_TP)
    in_specs = (
        P(SP, None), P(), P(SP, "tp"), P(SP, "tp"), P(SP, "tp"), P(SP, "tp"), P(SP, "tp"),
        P(SP, "tp"), P(), P(), P(), P(), P(SP, "tp"), P(), P(), P(), P("tp", SP), P("tp", SP),
    )
    return jax.shard_map(
        per_device, mesh=finer, in_specs=in_specs, out_specs=P(SP_TP, None), check_vma=False
    )
```

time: 379 us -> 238 us (0.63); the launches traced: 374 us -> 238 us
  matrix products: 137 us -> 30.1 us
  Pallas kernels: 0 us -> 49.2 us
  blocking collectives: 39.1 us -> 0 us
  local copies, waits for them, and re-layouts: 25.1 us -> 7.59 us
  other arithmetic: 28.5 us -> 17.4 us
  waiting for transfers between devices: 122 us -> 117 us
    dot_general x125 -> x3, matrix products: 137 us -> 30.1 us  [the longest x1 13.8 us: per_device(): jnp.dot(normed, jnp.concatenate(pieces[:4], axis=1), preferred_element_ty...]
    pallas_call x0 -> x3, Pallas kernels: none -> 49.2 us  [the longest x1 24.1 us: incoming_state(): pl.pallas_call(lambda *refs: prefix_kernel(heads, n_z, n_x, *refs), out_s...]
    all_gather x4 -> x0, blocking collectives: 39.1 us -> none  [prefix_by_axis(): lax.all_gather(part.astype(kind), axis)]
    reduce_scatter x1, waiting for transfers between devices: 61.4 us -> 52.1 us  [per_device(): lax.psum_scatter(jnp.dot(mixed, out_weight, preferred_element_type=F32).a...]
    mul x5 -> x0, other arithmetic: 8.25 us -> none  [the longest x1 2.2 us: unit_rows(): values * values]
    concatenate x0 -> x2, other arithmetic: none -> 6.02 us  [per_device(): extended = jnp.concatenate([before.astype(F32), wide], axis=0)]
    mul x24 -> x0, local copies, waits for them, and re-layouts: 5.82 us -> none  [the longest x2 3.91 us: unit_rows(): values * values]
    gt x8 -> x0, other arithmetic: 4.58 us -> none  [pool_means(): lag_rows < window_size[None, :]]
  transfers between devices with their start and end apart: 5 -> 4, of which waited for: 2 -> 2; matrix products, arithmetic and copies ran while one was open for 47% -> 17% of each run, Pallas kernels for 0% -> 21%
where the time goes in v1:
time: 238 us
  waiting for transfers between devices  117 us (49%)
  Pallas kernels  49.2 us (21%)
  matrix products  30.1 us (13%)
  other arithmetic  17.4 us (7%)
  between operations  13.2 us (6%)
  local copies, waits for them, and re-layouts  7.59 us (3%)
  starting transfers between devices  3.49 us (1%)
    all_gather x2, waiting for transfers between devices, side_by_side(): result = lax.all_gather(both, axis, axis=dim, tiled=True)  64.7 us
    reduce_scatter x1, waiting for transfers between devices, per_device(): lax.psum_scatter(jnp.dot(mixed, out_weight, preferred_element_type=F32).a...  52.1 us
    pallas_call x1, Pallas kernels, incoming_state(): pl.pallas_call(lambda *refs: prefix_kernel(heads, n_z, n_x, *refs), out_s...  24.1 us
    pallas_call x1, Pallas kernels, local_maps(): pl.pallas_call(lambda *refs: local_kernel(heads, chunks, *refs), out_shap...  20.5 us
    dot_general x1, matrix products, per_device(): jnp.dot(normed, jnp.concatenate(pieces[:4], axis=1), preferred_element_ty...  13.8 us
    dot_general x1, matrix products, per_device(): jnp.dot(mixed, out_weight, preferred_element_type=F32).astype(BF16)  10.3 us
    dot_general x1, matrix products, per_device(): jnp.dot(normed, jnp.concatenate(pieces[4:], axis=1), preferred_element_ty...  6.1 us
    concatenate x2, other arithmetic, per_device(): extended = jnp.concatenate([before.astype(F32), wide], axis=0)  6.02 us
  transfers between devices with their start and end apart: 4, of which 2 were waited for; matrix products, arithmetic and copies ran while one was open for 17% of the time, Pallas kernels for 21%

profile of v1, /device:TPU:1, one launch (start us, length us, event | category | flops | bytes accessed | tf_op | source)
XLA Modules:
  0.0 237.9 jit_solution(4789620948091620866)
XLA Ops:
  6.5 0.9 copy.22
  7.4 0.8 copy.23
  8.2 1.9 concatenate.15
  10.2 1.7 pad_maximum_fusion.1
  12.0 0.7 dynamic_slice.19
  12.7 0.7 dynamic_slice.21
  13.4 0.7 convert_element_type.24
  14.1 0.7 constant_dynamic-slice_fusion.1
  15.4 0.7 exponential_negate_fusion
  16.1 1.3 dynamic-slice_convert_fusion
  17.4 0.6 constant_dynamic-slice_fusion.refs_5_
  18.1 1.2 bitcast_convert_fusion.refs_3_
  19.3 5.1 %fusion = f32[1024]{0:T(1024)S(1)} fusion(bf16[1024,4096]{1,0:T(8,128)(2,1)} %param.18), kind=kLoop, calls=%fused_computation.2 | loop fusion | flops 12581888 | bytes 8392704 | tf_op jit(solution)/shard_map/reduce_sum | solution.py:312
  24.4 64.7 %all-gather.3.cloned.1.call-done = bf16[4096,1028]{1,0:T(8,128)(2,1)} async-done(((bf16[256,1028]{1,0:T(8,128)(2,1)}), bf16[4096,1028]{1,0:T(8,128)(2,1)}) %all-gather.3.cloned.1.call-update) | async-done | bytes 8421392 | tf_op jit(solution)/shard_map/all_gather | solution.py:301
  89.0 13.8 %fusion.3 = f32[1024,1024]{1,0:T(8,128)S(1)} fusion(bf16[4096,1028]{1,0:T(8,128)(2,1)} %all-gather.3.cloned.1.call-done, bf16[1024,4096]{1,0:T(8,128)(2,1)} %param.18, f32[4096]{0:T(1024)S(1)} %convert_element_type.24, f32[1024]{0:T(1024)S(1)} %add_rsqrt_fusion), kind=kOutput, calls=%fused_computation.5 | convolution fusion | flops 8606711808 | bytes 20992000 | tf_op jit(solution)/shard_map/dot_general | solution.py:331
  102.8 3.4 %collective-permute-start = (bf16[16,1024]{1,0:T(8,128)(2,1)S(1)}, bf16[16,1024]{1,0:T(8,128)(2,1)S(1)}, u32[]{:S(2)}, u32[]{:S(2)}) collective-permute-start(bf16[16,1024]{1,0:T(8,128)(2,1)S(1)} %slice.50), channel_id=1, source_target_pairs={{0,8},{8,16},{16,24},{24,32},{32,40},{40,48},{48,56},{56,64},{64,7... | collective-permute-start | bytes 98312 | tf_op jit(solution)/shard_map/ppermute | solution.py:308
  106.3 6.1 %fusion.6 = f32[1024,4]{0,1:T(4,128)S(1)} fusion(bf16[1024,4096]{1,0:T(8,128)(2,1)} %param.18, f32[4096]{0:T(1024)S(1)} %convert_element_type.24, f32[1024]{0:T(1024)S(1)} %add_rsqrt_fusion, bf16[4096,1028]{1,0:T(8,128)(2,1)} %all-gather.3.cloned.1.call-done), kind=kOutput, calls=%fused_computation.11 | convolution fusion | flops 50331648 | bytes 9474048 | tf_op jit(solution)/shard_map/dot_general | solution.py:332
  113.7 3.7 %fusion.5.refs_0_ = f32[1040,768]{1,0:T(8,128)} fusion(f32[16,1024]{1,0:T(8,128)S(1)} %convert_element_type.26, f32[1024,1024]{1,0:T(8,128)} %copy-done.1), kind=kLoop, calls=%fused_computation.10 | loop fusion | flops 798720 | bytes 7454720 | tf_op jit(solution)/shard_map/concatenate | solution.py:334
  117.5 20.5 %local_maps.1 = (bf16[2,1024,128]{2,1,0:T(8,128)(2,1)}, f32[2,1024,128]{2,1,0:T(8,128)}, bf16[2,128,256]{2,1,0:T(8,128)(2,1)}) custom-call(f32[1040,768]{1,0:T(8,128)} %fusion.5.refs_0_, f32[4,768]{1,0:T(4,128)} %convert.7.refs_1_, f32[8,256]{1,0:T(8,128)} %reshape.31.refs_2_, f32[8,256]{1,0:T(8,128)} %reshape.32.refs_3_), custom_call_target="tpu_custom_call" | custom-call | tf_op jit(solution)/shard_map/local_maps/pallas_call | solution.py:137
  138.0 24.1 %incoming_state.1.refs_2_ = bf16[2,128,128]{2,1,0:T(8,128)(2,1)} custom-call(bf16[2,128,256]{2,1,0:T(8,128)(2,1)} %get-tuple-element.10.refs_0_), custom_call_target="tpu_custom_call" | custom-call | tf_op jit(solution)/shard_map/incoming_state/pallas_call | solution.py:225
  162.1 2.3 pad_maximum_fusion.refs_4_
  164.4 4.6 %finish.1 = bf16[1024,512]{1,0:T(8,128)(2,1)} custom-call(bf16[2,1024,128]{2,1,0:T(8,128)(2,1)} %get-tuple-element.8.refs_0_, f32[2,1024,128]{2,1,0:T(8,128)} %get-tuple-element.9.refs_1_, bf16[2,128,128]{2,1,0:T(8,128)(2,1)} %incoming_state.1.refs_2_, f32[1,128]{1,0:T(1,128)} %bitcast_convert_fusion.refs_3_, f32[1040,256]{1,0:T(8,128)} %pad_maximum_fusion.refs_4_, ...), custom_call_target="tpu_custom_call" | custom-call | tf_op jit(solution)/shard_map/finish/pallas_call | solution.py:288
  169.0 10.3 %convolution_convert_fusion = bf16[1024,4096]{1,0:T(8,128)(2,1)} fusion(bf16[1024,512]{1,0:T(8,128)(2,1)} %finish.1, bf16[512,4096]{1,0:T(8,128)(2,1)} %all-gather.5.cloned.1.call-done), kind=kOutput, calls=%fused_computation.7 | convolution fusion | flops 4299161600 | bytes 13631488 | tf_op jit(solution)/shard_map/dot_general | solution.py:355
  179.3 52.1 %reduce-scatter.2.cloned.1.call-done = bf16[128,4096]{1,0:T(8,128)(2,1)} async-done(((bf16[1024,4096]{1,0:T(8,128)(2,1)}), bf16[128,4096]{1,0:T(8,128)(2,1)}) %reduce-scatter.2.cloned.1.call-update) | async-done | bytes 1048592 | tf_op jit(solution)/shard_map/reduce_scatter | solution.py:354
  (21 shorter events, 2.1 us)
Async XLA Ops:
  6.5 10.9 %copy-start = (bf16[16,128,128]{2,1,0:T(8,128)(2,1)S(1)}, bf16[16,128,128]{2,1,0:T(8,128)(2,1)}, u32[]{:S(2)}) copy-start(bf16[16,128,128]{2,1,0:T(8,128)(2,1)} %param.32) | copy-start | bytes 1572868
  6.5 82.5 %all-gather.3.cloned.1.call-start = ((), (), s32[]{:S(2)}) async-start(), calls=%async_computation.1 | async-start | bytes 10027008 | tf_op jit(solution)/shard_map/all_gather | solution.py:301
  10.1 158.8 %all-gather.5.cloned.1.call-start = ((), (), s32[]{:S(2)}) async-start(), calls=%async_computation.2 | async-start | bytes 4456448 | tf_op jit(solution)/shard_map/all_gather | solution.py:301
  11.9 219.5 %reduce-scatter.2.cloned.1.call-start = ((), (), s32[]{:S(2)}) async-start(), calls=%async_computation.3 | async-start | bytes 9437184 | tf_op jit(solution)/shard_map/reduce_scatter | solution.py:354
  102.8 9.6 %copy-start.1 = (f32[1024,1024]{1,0:T(8,128)}, f32[1024,1024]{1,0:T(8,128)S(1)}, u32[]{:S(2)}) copy-start(f32[1024,1024]{1,0:T(8,128)S(1)} %fusion.3) | copy-start | bytes 12582916
  102.8 9.5 %copy-start.2 = (f32[1024,2]{0,1:T(2,128)S(1)}, f32[1024,2]{0,1:T(2,128)}, u32[]{:S(2)}) copy-start(f32[1024,2]{0,1:T(2,128)} %param.30) | copy-start | bytes 24580
  102.8 10.9 %collective-permute-start = (bf16[16,1024]{1,0:T(8,128)(2,1)S(1)}, bf16[16,1024]{1,0:T(8,128)(2,1)S(1)}, u32[]{:S(2)}, u32[]{:S(2)}) collective-permute-start(bf16[16,1024]{1,0:T(8,128)(2,1)S(1)} %slice.50), channel_id=1, source_target_pairs={{0,8},{8,16},{16,24},{24,32},{32,40},{40,48},{48,56},{56,64},{64,7... | collective-permute-start | bytes 98312 | tf_op jit(solution)/shard_map/ppermute | solution.py:308
Sparse Core Ops, SparseCore 0:
  10.3 78.7 all-gather.2
  91.1 59.9 all-gather.4
  179.4 51.9 reduce-scatter.1

commit v2 on v1

--- a/solution.py
+++ b/solution.py
@@ -43,19 +43,6 @@
     for level in range(masks_ref.shape[0]):
         inside = (rows > cols) & (apart >= 2**level) & (apart < 2 ** (level + 1))
         masks_ref[level] = jnp.where(inside, 1.0, 0.0).astype(BF16)
-
-
-def fill_gates(beta, decay, grow_ref, gcol_ref, bcol_ref):
-    lane = lax.broadcasted_iota(jnp.int32, decay.shape, 1)
-    total = decay
-    step = 1
-    while step < CHUNK:
-        total = total + jnp.where(lane >= step, pltpu.roll(total, step, 1), 0.0)
-        step *= 2
-    for row in range(decay.shape[0]):
-        grow_ref[row] = jnp.broadcast_to(total[row : row + 1], (8, CHUNK))
-        gcol_ref[row] = jnp.broadcast_to(total[row : row + 1], (128, CHUNK)).T
-        bcol_ref[row] = jnp.broadcast_to(beta[row : row + 1], (128, CHUNK)).T
 
 
 def conv_rows(raw_ref, taps_ref, start, part):
@@ -113,46 +100,329 @@
         map_ref[head] = current * kept - dot(moved[:, 128:].astype(BF16), current_b) + added
 
 
-def local_kernel(heads, chunks, raw_ref, taps_ref, beta_ref, decay_ref, from_state_ref, local_ref,
-                 map_out_ref, grow_ref, gcol_ref, bcol_ref, masks_ref, map_ref):
+ROWS_A = (272, 768)
+SPLIT_A = 128
+ROWS_B = (768, 256)
+SPLIT_B = 384
+ORDER = ((0, 1), (0, -1), (1, 0), (-1, 0), (1, 1), (1, -1), (-1, 1), (-1, -1), (0, 2), (2, 0),
+         (1, 2), (-1, 2), (2, 1), (2, -1), (2, 2))
+
+
+class PlaneGather:
+    def __init__(self, buf, split, send_sems, recv_sems):
+        self.buf, self.split = buf, split
+        self.send_sems, self.recv_sems = send_sems, recv_sems
+        self.z, self.x = lax.axis_index("sp_0"), lax.axis_index("sp_1")
+        self.copies = {}
+
+    def shard(self, dz, dx):
+        return lax.rem(self.z + dz + 4, 4) * 4 + lax.rem(self.x + dx + 4, 4)
+
+    def rows(self, part):
+        split, total = self.split, self.buf.shape[1]
+        quarter = split // 32 * 16
+        rest = split + (total - split) // 32 * 16
+        return {"a": (0, split), "b": (split, total), "a0": (0, quarter), "a1": (quarter, split),
+                "b0": (split, rest), "b1": (rest, total)}[part]
+
+    def region(self, dz, dx, part):
+        low, high = self.rows(part)
+        return self.buf.at[self.shard(dz, dx), pl.ds(low, high - low), :]
+
+    def send(self, name, source, part, way):
+        index = len(self.copies)
+        ref = self.region(source[0], source[1], part)
+        copy = pltpu.make_async_remote_copy(
+            src_ref=ref, dst_ref=ref, send_sem=self.send_sems.at[index],
+            recv_sem=self.recv_sems.at[index],
+            device_id={"sp_0": lax.rem(self.z + way[0] + 4, 4),
+                       "sp_1": lax.rem(self.x + way[1] + 4, 4)},
+            device_id_type=MESH_ID)
+        copy.start()
+        self.copies[name, way] = (copy, index, source, part)
+
+    def got(self, name, way):
+        _, index, source, part = self.copies[name, way]
+        ref = self.region(source[0] - way[0], source[1] - way[1], part)
+        pltpu.make_async_remote_copy(
+            src_ref=ref, dst_ref=ref, send_sem=self.send_sems.at[index],
+            recv_sem=self.recv_sems.at[index],
+            device_id={"sp_0": lax.rem(self.z + way[0] + 4, 4),
+                       "sp_1": lax.rem(self.x + way[1] + 4, 4)},
+            device_id_type=MESH_ID).wait_recv()
+
+    def own(self):
+        for step in (1, -1):
+            self.send("a", (0, 0), "a", (0, step))
+            self.send("b", (0, 0), "b", (step, 0))
+        for step in (1, -1):
+            self.send("b", (0, 0), "b", (0, step))
+            self.send("a", (0, 0), "a", (step, 0))
+
+    def first(self):
+        for step in (1, -1):
+            self.got("a", (0, step))
+            self.got("b", (step, 0))
+        self.send("a2", (0, -1), "a0", (0, 1))
+        self.send("a2", (0, 1), "a1", (0, -1))
+        self.send("b2", (-1, 0), "b0", (1, 0))
+        self.send("b2", (1, 0), "b1", (-1, 0))
+        for at in (1, -1):
+            for step in (1, -1):
+                self.send(("a3", at), (0, at), "a", (step, 0))
+                self.send(("b3", at), (at, 0), "b", (0, step))
+
+    def second(self):
+        for step in (1, -1):
+            self.got("b", (0, step))
+            self.got("a", (step, 0))
+        self.send(("a4", 0), (-1, 0), "a", (1, 0))
+        self.send(("b4", 0), (0, -1), "b", (0, 1))
+
+    def third(self):
+        for step in (1, -1):
+            self.got("a2", (0, step))
+            self.got("b2", (step, 0))
+        for step in (-1, 1):
+            self.send(("a3", 2), (0, 2), "a", (step, 0))
+            self.send(("b3", 2), (2, 0), "b", (0, step))
+
+    def fourth(self):
+        for at in (1, -1):
+            for step in (1, -1):
+                self.got(("a3", at), (step, 0))
+                self.got(("b3", at), (0, step))
+        for at in (1, -1):
+            self.send(("a4", at), (-at, at), "a", (at, 0))
+            self.send(("b4", at), (at, -at), "b", (0, at))
+
+    def fifth(self):
+        for step in (1, -1):
+            self.got(("a3", 2), (step, 0))
+            self.got(("b3", 2), (0, step))
+        self.send(("a4", 2), (1, 2), "a", (-1, 0))
+        self.send(("b4", 2), (2, 1), "b", (0, -1))
+
+    def last(self, dz, dx):
+        side = {0: 1, 1: 1, -1: -1, 2: -1}
+        if dz == 2:
+            self.got(("a4", dx), (side[dx], 0))
+        if dx == 2:
+            self.got(("b4", dz), (0, side[dz]))
+
+    def drain(self):
+        for copy, _, _, _ in self.copies.values():
+            copy.wait_send()
+
+
+def norm_rows(tok_ref, gain_ref, start, count):
+    @pl.loop(0, count // 16)
+    def _(step):
+        rows = pl.ds(pl.multiple_of(start + step * 16, 16), 16)
+        values = tok_ref[rows, :].astype(F32)
+        squares = jnp.mean(values * values, axis=-1, keepdims=True)
+        tok_ref[rows, :] = (values * lax.rsqrt(squares + EPSILON) * gain_ref[...]).astype(BF16)
+
+
+def front_kernel(heads, tok_hbm, pool_hbm, query_hbm, key_hbm, value_hbm, pool_out_hbm,
+                 delta_out_hbm, gain_ref, strength_ref, decay_ref, taps_ref, spike_ref, rate_ref,
+                 decay_shift_ref, strength_shift_ref,
+                 from_state_ref, local_ref, map_out_ref, pool_acc_ref, out_w_hbm,
+                 tok_ref, wide_ref, late_ref, acc_ref, thin_ref, grow_ref, gcol_ref, bcol_ref,
+                 masks_ref, map_ref, tok_sems, load_sems, halo_send, halo_recv,
+                 send_a, recv_a, send_b, recv_b, out_sem):
+    z, x, tp = lax.axis_index("sp_0"), lax.axis_index("sp_1"), lax.axis_index("tp")
+    tok_rows = tok_hbm.shape[0]
+    chunks = tok_rows // CHUNK
+    mine = z * 4 + x
+    loads = []
+    for k, (hbm, ref, rows, lanes) in enumerate((
+            (query_hbm, wide_ref, 0, 0), (key_hbm, wide_ref, 0, 256), (value_hbm, wide_ref, 0, 512),
+            (pool_hbm, late_ref, 0, 0), (pool_out_hbm, late_ref, 256, 0),
+            (delta_out_hbm, late_ref, 512, 0))):
+        load = pltpu.make_async_copy(
+            hbm, ref.at[mine, pl.ds(rows, 256), pl.ds(lanes, 256)], load_sems.at[k])
+        load.start()
+        loads.append(load)
+    tok_loads = []
+    for k in range(chunks):
+        load = pltpu.make_async_copy(
+            tok_hbm.at[pl.ds(k * CHUNK, CHUNK), :],
+            tok_ref.at[pl.ds(HALO + k * CHUNK, CHUNK), :], tok_sems.at[k])
+        load.start()
+        tok_loads.append(load)
+    at = lax.broadcasted_iota(jnp.int32, (16, 256), 0)
+    thin = jnp.zeros((16, 256), F32)
+    for k, (ref, row) in enumerate(((strength_ref, 0), (strength_ref, 1), (decay_ref, 0),
+                                    (decay_ref, 1))):
+        row_values = ref[...].astype(F32)[row : row + 1]
+        thin = jnp.where(at == k, jnp.broadcast_to(row_values, (16, 256)), thin)
+    wide_ref[mine, 256:272, 0:256] = thin.astype(BF16)
+    wide_ref[mine, 256:272, 256:768] = jnp.zeros((16, 512), BF16)
+
+    following = lax.rem(mine + 1, 16)
+    before = lax.rem(mine + 15, 16)
+    barrier = pltpu.get_barrier_semaphore()
+    for dz, dx in ((0, 1), (0, -1), (1, 0), (-1, 0)):
+        pl.semaphore_signal(
+            barrier, 1, device_id={"sp_0": lax.rem(z + dz + 4, 4), "sp_1": lax.rem(x + dx + 4, 4)},
+            device_id_type=MESH_ID)
+    for other in (following, before):
+        pl.semaphore_signal(
+            barrier, 1, device_id={"sp_0": other // 4, "sp_1": lax.rem(other, 4)},
+            device_id_type=MESH_ID)
     fill_masks(masks_ref)
-    fill_gates(beta_ref[...], decay_ref[...], grow_ref, gcol_ref, bcol_ref)
+    for load in loads:
+        load.wait()
+    pl.semaphore_wait(barrier, 6)
+
+    early = PlaneGather(wide_ref, SPLIT_A, send_a, recv_a)
+    early.own()
+    halo = pltpu.make_async_remote_copy(
+        src_ref=tok_hbm.at[pl.ds(tok_rows - HALO, HALO), :], dst_ref=tok_ref.at[pl.ds(0, HALO), :],
+        send_sem=halo_send, recv_sem=halo_recv,
+        device_id={"sp_0": following // 4, "sp_1": lax.rem(following, 4)}, device_id_type=MESH_ID)
+    halo.start()
+    for k in range(chunks):
+        tok_loads[k].wait()
+        norm_rows(tok_ref, gain_ref, HALO + k * CHUNK, CHUNK)
+    halo.wait()
+
+    @pl.when(mine == 0)
+    def _():
+        tok_ref[0:HALO, :] = jnp.zeros((HALO, tok_ref.shape[1]), BF16)
+
+    norm_rows(tok_ref, gain_ref, 0, HALO)
+
+    tile = 208
+
+    def project(gather, dz, dx, into, first=False):
+        shard = gather.shard(dz, dx)
+        lanes = pl.ds(pl.multiple_of(shard * 256, 256), 256)
+
+        @pl.loop(0, acc_ref.shape[0] // tile)
+        def _(step):
+            rows = pl.ds(pl.multiple_of(step * tile, 16), tile)
+            normed = tok_ref[rows, lanes]
+            product = dot(normed, gather.buf[shard, 0:256, :])
+            into[rows, :] = product if first else into[rows, :] + product
+            if gather is early:
+                narrow = dot_nt(normed, gather.buf[shard, 256:272, 0:256])
+                thin_ref[rows, :] = narrow if first else thin_ref[rows, :] + narrow
+
+    project(early, 0, 0, acc_ref, first=True)
+    early.first()
+    early.second()
+    for dz, dx in ORDER[:4]:
+        project(early, dz, dx, acc_ref)
+    early.third()
+    early.fourth()
+    for dz, dx in ORDER[4:8]:
+        project(early, dz, dx, acc_ref)
+    early.fifth()
+    late = PlaneGather(late_ref, SPLIT_B, send_b, recv_b)
+    late.own()
+    for dz, dx in ORDER[8:]:
+        early.last(dz, dx)
+        project(early, dz, dx, acc_ref)
+
+    narrow = thin_ref[HALO:, :].T
+    total = tok_rows
+    heads_at = lax.broadcasted_iota(jnp.int32, (16, total), 0)
+
+    def own_scalar(ref, head):
+        return ref[tp * heads + head]
+
+    for head in range(heads):
+        strength = narrow[head : head + 1] + own_scalar(strength_shift_ref, head)
+        beta = 1.0 / (1.0 + jnp.exp(-strength))
+        level = narrow[heads + head : heads + head + 1] + own_scalar(decay_shift_ref, head)
+        soft = jnp.maximum(level, 0.0) + jnp.log1p(jnp.exp(-jnp.abs(level)))
+        rate = jnp.exp(jnp.full((1, total), own_scalar(rate_ref, head), F32))
+        decay = spike_ref[head : head + 1, :] - rate * soft
+        lane = lax.rem(lax.broadcasted_iota(jnp.int32, (8, total), 1), CHUNK)
+        summed = jnp.broadcast_to(decay, (8, total))
+        step = 1
+        while step < CHUNK:
+            summed = summed + jnp.where(lane >= step, pltpu.roll(summed, step, 1), 0.0)
+            step *= 2
+        for chunk in range(chunks):
+            row = head * chunks + chunk
+            part = slice(chunk * CHUNK, chunk * CHUNK + CHUNK)
+            grow_ref[row] = summed[:, part]
+            gcol_ref[row] = jnp.broadcast_to(summed[0:1, part], (128, CHUNK)).T
+            bcol_ref[row] = jnp.broadcast_to(beta[:, part], (128, CHUNK)).T
     rows = lax.broadcasted_iota(jnp.int32, (128, 256), 0)
     cols = lax.broadcasted_iota(jnp.int32, (128, 256), 1)
     for head in range(heads):
         map_ref[head] = jnp.where(rows == cols, 1.0, 0.0)
 
-    @pl.loop(0, chunks)
-    def _(chunk):
-        delta_chunk(chunk, heads, chunks, raw_ref, taps_ref, grow_ref, gcol_ref, bcol_ref,
-                    masks_ref, map_ref, from_state_ref, local_ref)
-
+    def delta(low, high):
+        @pl.loop(low, high)
+        def _(chunk):
+            delta_chunk(chunk, heads, chunks, acc_ref, taps_ref, grow_ref, gcol_ref, bcol_ref,
+                        masks_ref, map_ref, from_state_ref, local_ref)
+
+    late.first()
+    late.second()
+    delta(0, chunks // 2)
+    late.third()
+    late.fourth()
+    delta(chunks // 2, chunks)
     map_out_ref[...] = map_ref[...].astype(BF16)
-
-
-def local_maps(raw, taps, beta, decay, heads):
-    tok_rows = raw.shape[0] - HALO
+    late.fifth()
+    project(late, 0, 0, pool_acc_ref, first=True)
+    for dz, dx in ORDER[:8]:
+        project(late, dz, dx, pool_acc_ref)
+    for dz, dx in ORDER[8:]:
+        late.last(dz, dx)
+        project(late, dz, dx, pool_acc_ref)
+    result = pltpu.make_async_copy(late_ref.at[:, pl.ds(256, 512), :], out_w_hbm, out_sem)
+    result.start()
+    early.drain()
+    late.drain()
+    result.wait()
+
+
+def front(tokens, weights, out_weights, gain, strength, decay, taps, spike, rate, decay_shift,
+          strength_shift, heads):
+    tok_rows, depth = tokens.shape
     chunks = tok_rows // CHUNK
     vmem = pl.BlockSpec(memory_space=pltpu.VMEM)
+    smem = pl.BlockSpec(memory_space=pltpu.SMEM)
+    hbm = pl.BlockSpec(memory_space=pl.ANY)
+    pairs = heads * chunks
+    dma = pltpu.SemaphoreType.DMA
     return pl.pallas_call(
-        lambda *refs: local_kernel(heads, chunks, *refs),
+        lambda *refs: front_kernel(heads, *refs),
         out_shape=(
             jax.ShapeDtypeStruct((heads, tok_rows, 128), BF16),
             jax.ShapeDtypeStruct((heads, tok_rows, 128), F32),
             jax.ShapeDtypeStruct((heads, 128, 256), BF16),
+            jax.ShapeDtypeStruct((tok_rows + HALO, 256), F32),
+            jax.ShapeDtypeStruct((16, 512, 256), BF16),
         ),
-        in_specs=[vmem] * 4,
-        out_specs=(vmem, vmem, vmem),
+        in_specs=[hbm] * 7 + [vmem] * 5 + [smem] * 3,
+        out_specs=(vmem, vmem, vmem, vmem, hbm),
         scratch_shapes=[
-            pltpu.VMEM((heads * chunks, 8, CHUNK), F32),
-            pltpu.VMEM((heads * chunks, CHUNK, 128), F32),
-            pltpu.VMEM((heads * chunks, CHUNK, 128), F32),
+            pltpu.VMEM((tok_rows + HALO, depth), BF16),
+            pltpu.VMEM((16,) + ROWS_A, BF16),
+            pltpu.VMEM((16,) + ROWS_B, BF16),
+            pltpu.VMEM((tok_rows + HALO, 768), F32),
+            pltpu.VMEM((tok_rows + HALO, 16), F32),
+            pltpu.VMEM((pairs, 8, CHUNK), F32),
+            pltpu.VMEM((pairs, CHUNK, 128), F32),
+            pltpu.VMEM((pairs, CHUNK, 128), F32),
             pltpu.VMEM((8, CHUNK, CHUNK), BF16),
             pltpu.VMEM((heads, 128, 256), F32),
+            dma((chunks,)), dma((6,)), dma(()), dma(()),
+            dma((32,)), dma((32,)), dma((32,)), dma((32,)), dma(()),
         ],
-        compiler_params=pltpu.CompilerParams(vmem_limit_bytes=VMEM_LIMIT),
-        name="local_maps",
-    )(raw, taps, beta, decay)
+        compiler_params=pltpu.CompilerParams(
+            vmem_limit_bytes=VMEM_LIMIT, collective_id=1, has_side_effects=True),
+        name="front",
+    )(tokens, *weights, *out_weights, gain, strength, decay, taps, spike, rate, decay_shift,
+      strength_shift)
 
 
 def after(later, earlier):
@@ -295,62 +565,28 @@
     )(from_state, local, state, gain, pool_raw, mix, scale)
 
 
-def side_by_side(arrays, axis, dim, along):
-    widths = [a.shape[along] for a in arrays]
-    both = jnp.concatenate(arrays, axis=along)
-    result = lax.all_gather(both, axis, axis=dim, tiled=True)
-    return tuple(jnp.split(result, [sum(widths[:k]) for k in range(1, len(widths))], axis=along))
-
-
-def shifted(block, axis, distance):
-    devices = range(lax.axis_size(axis))
-    route = [(i - distance, i) for i in devices if i - distance in devices]
-    return lax.ppermute(block, axis, route)
-
-
-def scale_rows(values, gain_vec):
-    squares = jnp.mean(values * values, axis=-1, keepdims=True)
-    return values * lax.rsqrt(squares + EPSILON) * gain_vec.astype(F32)
-
-
 def per_device(tokens, input_norm_scale, mean_input_weight, query_matrix, key_matrix, value_matrix,
                strength_weight, decay_input_weight, causal_filter_weight, head_decay_logrates,
                decay_input_shift, strength_shift, decay_spike, head_norm_scale,
                group_mixing_weight, mean_channel_scale, mean_output_weight, delta_output_weight):
-    tok_rows = tokens.shape[0]
     pool_cols = mean_input_weight.shape[1]
     delta_cols = query_matrix.shape[1]
     heads = strength_weight.shape[1]
     groups = pool_cols // GROUP_DIM
-    chunks = tok_rows // CHUNK
     tp = lax.axis_index("tp")
-    normed = scale_rows(tokens.astype(F32), input_norm_scale).astype(BF16)
-    pieces = side_by_side(
-        (mean_input_weight, query_matrix, key_matrix, value_matrix, strength_weight,
-         decay_input_weight), SP, 0, 1)
-    wide = jnp.dot(normed, jnp.concatenate(pieces[:4], axis=1), preferred_element_type=F32)
-    narrow = jnp.dot(normed, jnp.concatenate(pieces[4:], axis=1), preferred_element_type=F32)
-    before = shifted(wide[tok_rows - HALO :].astype(BF16), SP, 1)
-    extended = jnp.concatenate([before.astype(F32), wide], axis=0)
     taps = lax.dynamic_slice_in_dim(causal_filter_weight, tp * delta_cols, delta_cols, 2)
     taps = taps.reshape(CONV, 3 * delta_cols).astype(F32)
-
-    def own(vector):
-        return lax.dynamic_slice_in_dim(vector, tp * heads, heads)
-
-    beta = jax.nn.sigmoid(narrow[:, :heads] + own(strength_shift))
-    decay = (-jnp.exp(own(head_decay_logrates))
-             * jax.nn.softplus(narrow[:, heads:] + own(decay_input_shift)) + decay_spike)
-    from_state, local, own_map = local_maps(
-        extended[:, pool_cols:], taps, beta.T.reshape(heads * chunks, CHUNK),
-        decay.T.reshape(heads * chunks, CHUNK), heads)
+    from_state, local, own_map, pool_raw, out_weight = front(
+        tokens, (mean_input_weight, query_matrix, key_matrix, value_matrix),
+        (mean_output_weight, delta_output_weight), input_norm_scale.astype(F32).reshape(1, -1),
+        strength_weight.T, decay_input_weight.T, taps, decay_spike.T, head_decay_logrates,
+        decay_input_shift, strength_shift, heads)
     state = incoming_state(own_map, lax.axis_size("sp_0"), lax.axis_size("sp_1"))
     mix = lax.dynamic_slice_in_dim(group_mixing_weight, tp * groups, groups, 0)
     scale = lax.dynamic_slice_in_dim(mean_channel_scale, tp * pool_cols, pool_cols)
     mixed = finish(from_state, local, state, head_norm_scale.astype(F32).reshape(1, HEAD_DIM),
-                   extended[:, :pool_cols], mix, scale.astype(F32).reshape(1, pool_cols))
-    out_weight = jnp.concatenate(
-        side_by_side((mean_output_weight, delta_output_weight), SP, 1, 0), axis=0)
+                   pool_raw, mix, scale.astype(F32).reshape(1, pool_cols))
+    out_weight = jnp.transpose(out_weight, (1, 0, 2)).reshape(512, -1)
     return lax.psum_scatter(
         jnp.dot(mixed, out_weight, preferred_element_type=F32).astype(BF16),
         "tp", scatter_dimension=0, tiled=True)

time: 238 us -> 212 us (0.89)
  Pallas kernels: 49.2 us -> 118 us
  waiting for transfers between devices: 117 us -> 58 us
  matrix products: 30.1 us -> 10.3 us
  other arithmetic: 17.4 us -> 4.48 us
  starting transfers between devices: 3.49 us -> 0.01 us
    pallas_call x1, Pallas kernels: 20.5 us -> 96.4 us  [front(): pl.pallas_call(lambda *refs: front_kernel(heads, *refs), out_shape=(jax.S...]
    all_gather x2 -> x0, waiting for transfers between devices: 64.7 us -> none  [side_by_side(): result = lax.all_gather(both, axis, axis=dim, tiled=True)]
    dot_general x2 -> x0, matrix products: 19.9 us -> none  [the longest x1 13.8 us: per_device(): jnp.dot(normed, jnp.concatenate(pieces[:4], axis=1), preferred_element_ty...]
    concatenate x3 -> x0, other arithmetic: 7.71 us -> none  [the longest x2 6.02 us: per_device(): extended = jnp.concatenate([before.astype(F32), wide], axis=0)]
    pallas_call x1, Pallas kernels: 24.1 us -> 16.7 us  [incoming_state(): pl.pallas_call(lambda *refs: prefix_kernel(heads, n_z, n_x, *refs), out_s...]
    transpose x0 -> x1, local copies, waits for them, and re-layouts: none -> 6.39 us  [per_device(): out_weight = jnp.transpose(out_weight, (1, 0, 2)).reshape(512, -1)]
    reduce_scatter x1, waiting for transfers between devices: 52.1 us -> 58 us  [per_device(): lax.psum_scatter(jnp.dot(mixed, out_weight, preferred_element_type=F32).a...]
    reduce_sum x1 -> x0, other arithmetic: 5.07 us -> none  [scale_rows(): squares = jnp.mean(values * values, axis=-1, keepdims=True)]
  transfers between devices with their start and end apart: 4 -> 1, of which waited for: 2 -> 1; matrix products, arithmetic and copies ran while one was open for 17% -> 0% of each run, Pallas kernels for 21% -> 0%
where the time goes in v2:
time: 212 us
  Pallas kernels  118 us (56%)
  waiting for transfers between devices  58 us (27%)
  between operations  13.4 us (6%)
  matrix products  10.3 us (5%)
  local copies, waits for them, and re-layouts  7.72 us (4%)
  other arithmetic  4.48 us (2%)
    pallas_call x1, Pallas kernels, front(): pl.pallas_call(lambda *refs: front_kernel(heads, *refs), out_shape=(jax.S...  96.4 us
    reduce_scatter x1, waiting for transfers between devices, per_device(): lax.psum_scatter(jnp.dot(mixed, out_weight, preferred_element_type=F32).a...  58 us
    pallas_call x1, Pallas kernels, incoming_state(): pl.pallas_call(lambda *refs: prefix_kernel(heads, n_z, n_x, *refs), out_s...  16.7 us
    dot_general x1, matrix products, per_device(): jnp.dot(mixed, out_weight, preferred_element_type=F32).astype(BF16)  10.3 us
    transpose x1, local copies, waits for them, and re-layouts, per_device(): out_weight = jnp.transpose(out_weight, (1, 0, 2)).reshape(512, -1)  6.39 us
    pallas_call x1, Pallas kernels, finish(): pl.pallas_call(lambda *refs: finish_kernel(heads, tok_rows // CHUNK, *ref...  4.52 us
  transfers between devices with their start and end apart: 1, of which 1 were waited for; matrix products, arithmetic and copies ran while one was open for 0% of the time, Pallas kernels for 0%

profile of v2, /device:TPU:1, one launch (start us, length us, event | category | flops | bytes accessed | tf_op | source)
XLA Modules:
  0.0 211.5 jit_solution(3023831997109164969)
XLA Ops:
  6.5 0.0 copy-start
  6.5 0.0 reduce-scatter.2.cloned.1.call-start
  6.5 1.3 bitcast_convert_fusion.refs_3_
  7.8 1.3 dynamic-slice_convert_fusion
  9.1 0.7 constant_dynamic-slice_fusion.1
  9.8 0.6 convert.4.refs_10_
  10.4 1.3 reshape.28
  11.7 96.4 %front.1 = (bf16[2,1024,128]{2,1,0:T(8,128)(2,1)}, f32[2,1024,128]{2,1,0:T(8,128)}, bf16[2,128,256]{2,1,0:T(8,128)(2,1)}, f32[1040,256]{1,0:T(8,128)}, bf16[16,512,256]{2,1,0:T(8,128)(2,1)}) custom-call(bf16[1024,4096]{1,0:T(8,128)(2,1)} %refs_0_.1, bf16[256,256]{1,0:T(8,128)(2,1)} %refs_1_.1, bf16[256,256]{1,0:T(8,128)(2,1)} %refs_2_.1, ...), custom_call_target="tpu_custom_call" | custom-call | tf_op jit(solution)/shard_map/front/pallas_call | solution.py:396
  108.1 16.7 %incoming_state.1.refs_2_ = bf16[2,128,128]{2,1,0:T(8,128)(2,1)} custom-call(bf16[2,128,256]{2,1,0:T(8,128)(2,1)} %get-tuple-element.12.refs_0_), custom_call_target="tpu_custom_call" | custom-call | tf_op jit(solution)/shard_map/incoming_state/pallas_call | solution.py:495
  124.8 6.4 %copy.20 = bf16[512,16,256]{0,2,1:T(8,128)(2,1)} copy(bf16[512,16,256]{2,0,1:T(8,128)(2,1)} %bitcast.15) | data formatting | bytes 8388608 | tf_op jit(solution)/shard_map/transpose | solution.py:589
  131.2 0.0 copy-done
  131.2 0.6 constant_dynamic-slice_fusion.refs_5_
  131.8 4.5 %finish.1 = bf16[1024,512]{1,0:T(8,128)(2,1)} custom-call(bf16[2,1024,128]{2,1,0:T(8,128)(2,1)} %get-tuple-element.10.refs_0_, f32[2,1024,128]{2,1,0:T(8,128)} %get-tuple-element.11.refs_1_, bf16[2,128,128]{2,1,0:T(8,128)(2,1)} %incoming_state.1.refs_2_, f32[1,128]{1,0:T(1,128)} %bitcast_convert_fusion.refs_3_, f32[1040,256]{1,0:T(8,128)} %get-tuple-element.13.refs_4_, ...), custom_call_target="tpu_custom_call" | custom-call | tf_op jit(solution)/shard_map/finish/pallas_call | solution.py:558
  136.3 10.3 %convolution_convert_fusion = bf16[1024,4096]{1,0:T(8,128)(2,1)} fusion(bf16[1024,512]{1,0:T(8,128)(2,1)} %finish.1, bf16[512,4096]{0,1:T(8,128)(2,1)} %bitcast.14), kind=kOutput, calls=%fused_computation | convolution fusion | flops 4299161600 | bytes 13631488 | tf_op jit(solution)/shard_map/dot_general | solution.py:591
  146.6 0.0 reduce-scatter.2.cloned.1.call-update
  146.6 58.0 %reduce-scatter.2.cloned.1.call-done = bf16[128,4096]{1,0:T(8,128)(2,1)} async-done(((bf16[1024,4096]{1,0:T(8,128)(2,1)}), bf16[128,4096]{1,0:T(8,128)(2,1)}) %reduce-scatter.2.cloned.1.call-update) | async-done | bytes 1048592 | tf_op jit(solution)/shard_map/reduce_scatter | solution.py:590
Async XLA Ops:
  6.5 124.7 %copy-start = (bf16[16,128,128]{2,1,0:T(8,128)(2,1)S(1)}, bf16[16,128,128]{2,1,0:T(8,128)(2,1)}, u32[]{:S(2)}) copy-start(bf16[16,128,128]{2,1,0:T(8,128)(2,1)} %param.32) | copy-start | bytes 1572868
  6.5 198.1 %reduce-scatter.2.cloned.1.call-start = ((), (), s32[]{:S(2)}) async-start(), calls=%async_computation.1 | async-start | bytes 9437184 | tf_op jit(solution)/shard_map/reduce_scatter | solution.py:590
Sparse Core Ops, SparseCore 0:
  146.8 57.8 reduce-scatter.1

commit v3 on v2

--- a/solution.py
+++ b/solution.py
@@ -430,91 +430,29 @@
     return dot(later[:, :128], earlier.astype(BF16)) + offset
 
 
-def prefix_kernel(heads, n_z, n_x, own_ref, state_ref, row_ref, total_ref, column_ref, send_x,
-                  recv_x, send_z, recv_z):
-    z, x = lax.axis_index("sp_0"), lax.axis_index("sp_1")
-    barrier = pltpu.get_barrier_semaphore()
-    for step in range(1, n_x):
-        to = lax.rem(x + step, n_x)
-        pl.semaphore_signal(barrier, 1, device_id={"sp_1": to}, device_id_type=MESH_ID)
-    for step in range(1, n_z):
-        to = lax.rem(z + step, n_z)
-        pl.semaphore_signal(barrier, 1, device_id={"sp_0": to}, device_id_type=MESH_ID)
-    pl.semaphore_wait(barrier, n_x + n_z - 2)
-
-    copies = []
-    for step in range(1, n_x):
-        copy = pltpu.make_async_remote_copy(
-            src_ref=own_ref, dst_ref=row_ref.at[step], send_sem=send_x.at[step],
-            recv_sem=recv_x.at[step], device_id={"sp_1": lax.rem(x + step, n_x)},
-            device_id_type=MESH_ID)
-        copy.start()
-        copies.append(copy)
-    row_ref[0] = own_ref[...]
-    for copy in copies:
-        copy.wait()
-    inside, total = [None] * heads, [None] * heads
-    rows = lax.broadcasted_iota(jnp.int32, (128, 256), 0)
-    cols = lax.broadcasted_iota(jnp.int32, (128, 256), 1)
-    identity = jnp.where(rows == cols, 1.0, 0.0)
-    for head in range(heads):
-        so_far = identity
-        before = identity
-        for k in range(n_x):
-            piece = row_ref[lax.rem(x - k + n_x, n_x), head]
-            so_far = piece.astype(F32) if k == 0 else after(piece, so_far)
-            before = jnp.where(k < x, so_far, before)
-        inside[head] = before
-        total_ref[head] = so_far.astype(BF16)
-    copies = []
-    for step in range(1, n_z):
-        copy = pltpu.make_async_remote_copy(
-            src_ref=total_ref, dst_ref=column_ref.at[step], send_sem=send_z.at[step],
-            recv_sem=recv_z.at[step], device_id={"sp_0": lax.rem(z + step, n_z)},
-            device_id_type=MESH_ID)
-        copy.start()
-        copies.append(copy)
-    column_ref[0] = total_ref[...]
-    for copy in copies:
-        copy.wait()
-    for head in range(heads):
-        so_far = jnp.zeros((128, 128), F32)
-        state = so_far
-        for k in range(n_z - 1):
-            piece = column_ref[lax.rem(z - k + n_z, n_z), head]
-            offset = piece[:, 128:].astype(F32)
-            so_far = offset if k == 0 else dot(piece[:, :128], so_far.astype(BF16)) + offset
-            state = jnp.where(k < z, so_far, state)
-        entering = dot(inside[head][:, :128].astype(BF16), state.astype(BF16))
-        state_ref[head] = (entering + inside[head][:, 128:]).astype(BF16)
-
-
-def incoming_state(own, n_z, n_x):
-    heads = own.shape[0]
-    vmem = pl.BlockSpec(memory_space=pltpu.VMEM)
-    return pl.pallas_call(
-        lambda *refs: prefix_kernel(heads, n_z, n_x, *refs),
-        out_shape=jax.ShapeDtypeStruct((heads, 128, 128), BF16),
-        in_specs=[vmem],
-        out_specs=vmem,
-        scratch_shapes=[
-            pltpu.VMEM((n_x, heads, 128, 256), BF16),
-            pltpu.VMEM((heads, 128, 256), BF16),
-            pltpu.VMEM((n_z, heads, 128, 256), BF16),
-            pltpu.SemaphoreType.DMA((n_x,)),
-            pltpu.SemaphoreType.DMA((n_x,)),
-            pltpu.SemaphoreType.DMA((n_z,)),
-            pltpu.SemaphoreType.DMA((n_z,)),
-        ],
-        compiler_params=pltpu.CompilerParams(collective_id=0, has_side_effects=True),
-        name="incoming_state",
-    )(own)
-
-
-def pooled_rows(pool_ref, position, wide, mix_ref, scale_ref, out_ref, start):
+PIECE = 1024
+
+
+def device_at(z=0, x=0, tp=0):
+    place = {}
+    for name, step in (("sp_0", z), ("sp_1", x), ("tp", tp)):
+        if step:
+            size = lax.axis_size(name)
+            place[name] = lax.rem(lax.axis_index(name) + step + size, size)
+    return place
+
+
+def remote(src, dst, send_sem, recv_sem, place):
+    return pltpu.make_async_remote_copy(
+        src_ref=src, dst_ref=dst, send_sem=send_sem, recv_sem=recv_sem, device_id=place,
+        device_id_type=MESH_ID)
+
+
+def pooled_rows(pool_ref, chunk, position, wide, mix_ref, scale_ref):
+    parts = []
     for group in range(2):
         lanes = slice(group * 128, group * 128 + 128)
-        rows = pool_ref[pl.ds(pl.multiple_of(start, 8), CHUNK + HALO), lanes]
+        rows = pool_ref[pl.ds(pl.multiple_of(chunk * CHUNK, CHUNK), CHUNK + HALO), lanes]
         reach = 1
         sums = rows
         for _ in range(group + 1):
@@ -525,44 +463,202 @@
             broad = broad + pltpu.roll(broad, reach, 0)
             reach *= 2
         short, long = 2 << group, 8 << group
-        seen = lax.broadcasted_iota(jnp.int32, (CHUNK, 128), 0) + (position + 1)
+        seen = lax.broadcasted_iota(jnp.int32, (CHUNK, 128), 0) + (position + chunk * CHUNK + 1)
         count = jnp.minimum(seen, jnp.where(wide, long, short)).astype(F32)
         window = jnp.where(wide, broad[HALO:], sums[HALO:])
         diff = (window / count - rows[HALO:]).astype(BF16)
-        mixed = dot(diff, mix_ref[group]) * scale_ref[0:1, lanes]
-        out_ref[pl.ds(pl.multiple_of(start, CHUNK), CHUNK), lanes] = mixed.astype(BF16)
-
-
-def finish_kernel(heads, chunks, from_state_ref, local_ref, state_ref, gain_ref, pool_ref, mix_ref,
-                  scale_ref, out_ref):
-    tok_rows = chunks * CHUNK
-    token = (lax.axis_index("sp_0") * lax.axis_size("sp_1") + lax.axis_index("sp_1")) * tok_rows
-    wide = lax.rem(lax.axis_index("tp"), 2) == 1
+        parts.append((dot(diff, mix_ref[group]) * scale_ref[0:1, lanes]).astype(BF16))
+    return parts
+
+
+def back_kernel(heads, own_ref, gain_ref, mix_ref, scale_ref, from_state_hbm, local_hbm, pool_hbm,
+                out_w_hbm, out_ref,
+                from_state_ref, local_ref, pool_ref, out_w_ref, row_ref, total_ref, column_ref,
+                state_ref, mixed_ref, part_ref, pair_out_ref, pair_in_ref, ring_out_ref,
+                half_ref, final_ref, load_sems, send_x, recv_x, send_z, recv_z, pair_send,
+                pair_recv, ring_send, ring_recv):
+    z, x, tp = lax.axis_index("sp_0"), lax.axis_index("sp_1"), lax.axis_index("tp")
+    n_z, n_x = lax.axis_size("sp_0"), lax.axis_size("sp_1")
+    y, core = tp // 2, lax.rem(tp, 2)
+    n_y = lax.axis_size("tp") // 2
+    chunks = pool_ref.shape[0] // CHUNK
+    position = (z * n_x + x) * (chunks * CHUNK)
+    loads = []
+    for k, (hbm, ref) in enumerate(((pool_hbm, pool_ref), (from_state_hbm, from_state_ref),
+                                    (local_hbm, local_ref), (out_w_hbm, out_w_ref))):
+        load = pltpu.make_async_copy(hbm, ref, load_sems.at[k])
+        load.start()
+        loads.append(load)
+    other = {"tp": y * 2 + (1 - core)}
+    peers = [device_at(x=step) for step in range(1, n_x)]
+    peers += [device_at(z=step) for step in range(1, n_z)]
+    peers += [other, device_at(tp=2), device_at(tp=-2)]
+    barrier = pltpu.get_barrier_semaphore()
+    for peer in peers:
+        pl.semaphore_signal(barrier, 1, device_id=peer, device_id_type=MESH_ID)
+    pl.semaphore_wait(barrier, len(peers))
+
+    along_x = [remote(own_ref, row_ref.at[step], send_x.at[step], recv_x.at[step],
+                      device_at(x=step)) for step in range(1, n_x)]
+    for copy in along_x:
+        copy.start()
+    row_ref[0] = own_ref[...]
+    loads[0].wait()
+    wide = core == 1
+
+    def store_halves(chunk, lanes, values):
+        for half in range(2):
+            slot = lax.rem(half + core, 2)
+            mixed_ref[chunk, pl.ds(pl.multiple_of(slot * 128, 128), 128), lanes] = (
+                values[half * 128 : half * 128 + 128])
 
     @pl.loop(0, chunks)
     def _(chunk):
-        start = chunk * CHUNK
-        where_rows = pl.ds(pl.multiple_of(start, CHUNK), CHUNK)
-        pooled_rows(pool_ref, token + start, wide, mix_ref, scale_ref, out_ref, start)
+        for group, values in enumerate(
+                pooled_rows(pool_ref, chunk, position, wide, mix_ref, scale_ref)):
+            store_halves(chunk, slice(group * 128, group * 128 + 128), values)
+
+    for copy in along_x:
+        copy.wait_recv()
+    inside = []
+    rows = lax.broadcasted_iota(jnp.int32, (128, 256), 0)
+    cols = lax.broadcasted_iota(jnp.int32, (128, 256), 1)
+    for head in range(heads):
+        so_far = before = jnp.where(rows == cols, 1.0, 0.0)
+        for k in range(n_x):
+            piece = row_ref[lax.rem(x - k + n_x, n_x), head]
+            so_far = piece.astype(F32) if k == 0 else after(piece, so_far)
+            before = jnp.where(k < x, so_far, before)
+        inside.append(before)
+        total_ref[head] = so_far.astype(BF16)
+    along_z = [remote(total_ref, column_ref.at[step], send_z.at[step], recv_z.at[step],
+                      device_at(z=step)) for step in range(1, n_z)]
+    for copy in along_z:
+        copy.start()
+    column_ref[0] = total_ref[...]
+    for load in loads[1:]:
+        load.wait()
+    for copy in along_z:
+        copy.wait_recv()
+    for head in range(heads):
+        so_far = state = jnp.zeros((128, 128), F32)
+        for k in range(n_z - 1):
+            piece = column_ref[lax.rem(z - k + n_z, n_z), head]
+            offset = piece[:, 128:].astype(F32)
+            so_far = offset if k == 0 else dot(piece[:, :128], so_far.astype(BF16)) + offset
+            state = jnp.where(k < z, so_far, state)
+        entering = dot(inside[head][:, :128].astype(BF16), state.astype(BF16))
+        state_ref[head] = (entering + inside[head][:, 128:]).astype(BF16)
+
+    pairs, rings = {}, []
+
+    def produce(ahead, order):
+        chunk = lax.rem(y + ahead, n_y)
+        where_rows = pl.ds(pl.multiple_of(chunk * CHUNK, CHUNK), CHUNK)
         for head in range(heads):
             raw = dot(from_state_ref[head, where_rows, :], state_ref[head])
             raw = raw + local_ref[head, where_rows, :]
             squares = jnp.mean(raw * raw, axis=-1, keepdims=True)
-            normed = raw * lax.rsqrt(squares + EPSILON) * gain_ref[...]
-            out_ref[where_rows, 256 + head * 128 : 384 + head * 128] = normed.astype(BF16)
-
-
-def finish(from_state, local, state, gain, pool_raw, mix, scale):
+            normed = (raw * lax.rsqrt(squares + EPSILON) * gain_ref[...]).astype(BF16)
+            store_halves(chunk, slice(256 + head * 128, 384 + head * 128), normed)
+        for piece in order:
+            @pl.loop(0, PIECE // 256)
+            def _(block):
+                lanes = pl.ds(pl.multiple_of(block * 256, 256), 256)
+                product = dot(mixed_ref[chunk], out_w_ref[piece * (PIECE // 256) + block])
+                part_ref[ahead, piece, :, lanes] = product[:128]
+                pair_out_ref[ahead, piece, :, lanes] = product[128:].astype(BF16)
+
+            index = ahead * 4 + piece
+            copy = remote(pair_out_ref.at[ahead, piece], pair_in_ref.at[ahead, piece],
+                          pair_send.at[index], pair_recv.at[index], other)
+            copy.start()
+            pairs[ahead, piece] = copy
+
+    def chip_sum(ahead, piece):
+        pairs[ahead, piece].wait_recv()
+        return part_ref[ahead, piece] + pair_in_ref[ahead, piece].astype(F32)
+
+    def pass_on(ahead, piece, value, place, target):
+        slot = ahead - 1
+        ring_out_ref[slot, piece] = value.astype(BF16)
+        index = len(rings)
+        copy = remote(ring_out_ref.at[slot, piece], target, ring_send.at[index],
+                      ring_recv.at[index], place)
+        copy.start()
+        rings.append(copy)
+        return copy
+
+    up, down = device_at(tp=2), device_at(tp=-2)
+    produce(2, (0, 2, 1, 3))
+    halves = {}
+    for piece in (0, 2, 1, 3):
+        halves[piece] = pass_on(2, piece, chip_sum(2, piece), up if piece < 2 else down,
+                                half_ref.at[piece])
+    finals = {}
+    produce(1, (2, 3, 0, 1))
+    produce(3, (0, 1, 2, 3))
+    for k in range(2):
+        piece = 2 + k
+        finals[1, piece] = pass_on(1, piece, chip_sum(1, piece), up, final_ref.at[0, piece])
+        piece = k
+        finals[3, piece] = pass_on(3, piece, chip_sum(3, piece), down, final_ref.at[1, piece])
+    produce(0, (0, 1, 2, 3))
+    for k in range(2):
+        for ahead, piece, place, side in ((1, k, up, 0), (3, 2 + k, down, 1)):
+            value = chip_sum(ahead, piece)
+            halves[piece].wait_recv()
+            value = value + half_ref[piece].astype(F32)
+            finals[ahead, piece] = pass_on(ahead, piece, value, place, final_ref.at[side, piece])
+    for piece in range(4):
+        part_ref[0, piece] = chip_sum(0, piece)
+    for first, second in ((2, 0), (3, 1), (0, 2), (1, 3)):
+        for side, ahead, piece in ((0, 1, first), (1, 3, second)):
+            finals[ahead, piece].wait_recv()
+            part_ref[0, piece] = part_ref[0, piece] + final_ref[side, piece].astype(F32)
+    for piece in range(4):
+        out_ref[:, piece * PIECE : piece * PIECE + PIECE] = part_ref[0, piece].astype(BF16)
+    for copy in along_x + along_z + list(pairs.values()) + rings:
+        copy.wait_send()
+
+
+def back(own_map, gain, mix, scale, from_state, local, pool_raw, out_weight):
     heads, tok_rows, _ = from_state.shape
+    n_z, n_x = lax.axis_size("sp_0"), lax.axis_size("sp_1")
+    width = out_weight.shape[0] * 256
+    chunks = tok_rows // CHUNK
+    pieces = width // PIECE
     vmem = pl.BlockSpec(memory_space=pltpu.VMEM)
+    hbm = pl.BlockSpec(memory_space=pl.ANY)
+    dma = pltpu.SemaphoreType.DMA
     return pl.pallas_call(
-        lambda *refs: finish_kernel(heads, tok_rows // CHUNK, *refs),
-        out_shape=jax.ShapeDtypeStruct((tok_rows, 512), BF16),
-        in_specs=[vmem] * 7,
+        lambda *refs: back_kernel(heads, *refs),
+        out_shape=jax.ShapeDtypeStruct((128, width), BF16),
+        in_specs=[vmem] * 4 + [hbm] * 4,
         out_specs=vmem,
-        compiler_params=pltpu.CompilerParams(vmem_limit_bytes=VMEM_LIMIT),
-        name="finish",
-    )(from_state, local, state, gain, pool_raw, mix, scale)
+        scratch_shapes=[
+            pltpu.VMEM(from_state.shape, BF16),
+            pltpu.VMEM(local.shape, F32),
+            pltpu.VMEM(pool_raw.shape, F32),
+            pltpu.VMEM(out_weight.shape, BF16),
+            pltpu.VMEM((n_x, heads, 128, 256), BF16),
+            pltpu.VMEM((heads, 128, 256), BF16),
+            pltpu.VMEM((n_z, heads, 128, 256), BF16),
+            pltpu.VMEM((heads, 128, 128), BF16),
+            pltpu.VMEM((chunks, CHUNK, 512), BF16),
+            pltpu.VMEM((4, pieces, 128, PIECE), F32),
+            pltpu.VMEM((4, pieces, 128, PIECE), BF16),
+            pltpu.VMEM((4, pieces, 128, PIECE), BF16),
+            pltpu.VMEM((3, pieces, 128, PIECE), BF16),
+            pltpu.VMEM((pieces, 128, PIECE), BF16),
+            pltpu.VMEM((2, pieces, 128, PIECE), BF16),
+            dma((4,)), dma((n_x,)), dma((n_x,)), dma((n_z,)), dma((n_z,)),
+            dma((16,)), dma((16,)), dma((12,)), dma((12,)),
+        ],
+        compiler_params=pltpu.CompilerParams(
+            vmem_limit_bytes=VMEM_LIMIT, collective_id=0, has_side_effects=True),
+        name="back",
+    )(own_map, gain, mix, scale, from_state, local, pool_raw, out_weight)
 
 
 def per_device(tokens, input_norm_scale, mean_input_weight, query_matrix, key_matrix, value_matrix,
@@ -581,15 +677,10 @@
         (mean_output_weight, delta_output_weight), input_norm_scale.astype(F32).reshape(1, -1),
         strength_weight.T, decay_input_weight.T, taps, decay_spike.T, head_decay_logrates,
         decay_input_shift, strength_shift, heads)
-    state = incoming_state(own_map, lax.axis_size("sp_0"), lax.axis_size("sp_1"))
     mix = lax.dynamic_slice_in_dim(group_mixing_weight, tp * groups, groups, 0)
     scale = lax.dynamic_slice_in_dim(mean_channel_scale, tp * pool_cols, pool_cols)
-    mixed = finish(from_state, local, state, head_norm_scale.astype(F32).reshape(1, HEAD_DIM),
-                   pool_raw, mix, scale.astype(F32).reshape(1, pool_cols))
-    out_weight = jnp.transpose(out_weight, (1, 0, 2)).reshape(512, -1)
-    return lax.psum_scatter(
-        jnp.dot(mixed, out_weight, preferred_element_type=F32).astype(BF16),
-        "tp", scatter_dimension=0, tiled=True)
+    return back(own_map, head_norm_scale.astype(F32).reshape(1, HEAD_DIM), mix,
+                scale.astype(F32).reshape(1, pool_cols), from_state, local, pool_raw, out_weight)
 
 
 def solution(mesh):

time: 212 us -> 170 us (0.80)
  waiting for transfers between devices: 58 us -> 0 us
  Pallas kernels: 118 us -> 162 us
  between operations: 13.4 us -> 0.02 us
  matrix products: 10.3 us -> 0 us
  local copies, waits for them, and re-layouts: 7.72 us -> 3.62 us
    reduce_scatter x1 -> x0, waiting for transfers between devices: 58 us -> none  [per_device(): lax.psum_scatter(jnp.dot(mixed, out_weight, preferred_element_type=F32).a...]
    pallas_call x2 -> x1, Pallas kernels: 21.2 us -> 65.4 us  [back(): pl.pallas_call(lambda *refs: back_kernel(heads, *refs), out_shape=jax.Sha...]
    dot_general x1 -> x0, matrix products: 10.3 us -> none  [per_device(): jnp.dot(mixed, out_weight, preferred_element_type=F32).astype(BF16)]
    transpose x1 -> x0, local copies, waits for them, and re-layouts: 6.39 us -> none  [per_device(): out_weight = jnp.transpose(out_weight, (1, 0, 2)).reshape(512, -1)]
    unnamed x2 -> x3, local copies, waits for them, and re-layouts: 0.01 us -> 2.29 us
  transfers between devices with their start and end apart: 1 -> 0, of which waited for: 1 -> 0; matrix products, arithmetic and copies ran while one was open for 0% -> 0% of each run, Pallas kernels for 0% -> 0%
where the time goes in v3:
time: 170 us
  Pallas kernels  162 us (95%)
  other arithmetic  4.51 us (3%)
  local copies, waits for them, and re-layouts  3.62 us (2%)
    pallas_call x1, Pallas kernels, front(): pl.pallas_call(lambda *refs: front_kernel(heads, *refs), out_shape=(jax.S...  96.3 us
    pallas_call x1, Pallas kernels, back(): pl.pallas_call(lambda *refs: back_kernel(heads, *refs), out_shape=jax.Sha...  65.4 us

profile of v3, /device:TPU:1, one launch (start us, length us, event | category | flops | bytes accessed | tf_op | source)
XLA Modules:
  0.0 169.9 jit_solution(6386282233158061195)
XLA Ops:
  0.0 0.0 copy-start
  0.0 1.3 bitcast_convert_fusion.refs_1_
  1.3 1.3 dynamic-slice_convert_fusion
  2.6 0.7 constant_dynamic-slice_fusion.1
  3.3 0.6 convert.4.refs_10_
  3.9 1.3 reshape.24
  5.2 0.0 copy-done
  5.2 0.6 constant_dynamic-slice_fusion.refs_2_
  5.8 96.3 %front.1 = (bf16[2,1024,128]{2,1,0:T(8,128)(2,1)}, f32[2,1024,128]{2,1,0:T(8,128)}, bf16[2,128,256]{2,1,0:T(8,128)(2,1)}, f32[1040,256]{1,0:T(8,128)}, bf16[16,512,256]{2,1,0:T(8,128)(2,1)}) custom-call(bf16[1024,4096]{1,0:T(8,128)(2,1)} %refs_0_.1, bf16[256,256]{1,0:T(8,128)(2,1)} %refs_1_.1, bf16[256,256]{1,0:T(8,128)(2,1)} %refs_2_.1, ...), custom_call_target="tpu_custom_call" | custom-call | tf_op jit(solution)/shard_map/front/pallas_call | solution.py:396
  102.2 65.4 %back.1 = bf16[128,4096]{1,0:T(8,128)(2,1)} custom-call(bf16[2,128,256]{2,1,0:T(8,128)(2,1)} %get-tuple-element.10.refs_0_, f32[1,128]{1,0:T(1,128)} %bitcast_convert_fusion.refs_1_, bf16[2,128,128]{2,1,0:T(8,128)(2,1)} %constant_dynamic-slice_fusion.refs_2_, f32[1,256]{1,0:T(1,128)} %bitcast.13, bf16[2,1024,128]{2,1,0:T(8,128)(2,1)} %get-tuple-element.11.refs_4_, ...), custom_call_target="tpu_custom_call" | custom-call | tf_op jit(solution)/shard_map/back/pallas_call | solution.py:634
  167.6 2.3 %copy.21 = bf16[128,4096]{1,0:T(8,128)(2,1)} copy(bf16[128,4096]{1,0:T(8,128)(2,1)} %back.1) | data formatting | bytes 2097152
Async XLA Ops:
  0.0 5.2 %copy-start = (bf16[16,128,128]{2,1,0:T(8,128)(2,1)S(1)}, bf16[16,128,128]{2,1,0:T(8,128)(2,1)}, u32[]{:S(2)}) copy-start(bf16[16,128,128]{2,1,0:T(8,128)(2,1)} %param.32) | copy-start | bytes 1572868

commit v4 on v2

v4 whole, which is shorter than its diff:
```python
import jax
import jax.numpy as jnp
from jax import lax
from jax.experimental import pallas as pl
from jax.experimental.pallas import tpu as pltpu
from jax.sharding import Mesh
from jax.sharding import PartitionSpec as P

HEAD_DIM = 128
CONV = 4
CHUNK = 256
HALO = 16
EPSILON = 1e-06
SP = ("sp_0", "sp_1")
SP_TP = ("sp_0", "sp_1", "tp")
MESH_ID = pl.DeviceIdType.MESH
F32 = jnp.float32
BF16 = jnp.bfloat16
VMEM_LIMIT = 63 * 1000 * 1000


def dot(a, b):
    return jnp.dot(a, b, preferred_element_type=F32)


def dot_nt(a, b):
    return lax.dot_general(a, b, (((1,), (1,)), ((), ())), preferred_element_type=F32)


def dot_tn(a, b):
    return lax.dot_general(a, b, (((0,), (0,)), ((), ())), preferred_element_type=F32)


def unit_rows(values):
    return values * lax.rsqrt(jnp.sum(values * values, axis=-1, keepdims=True) + EPSILON)


def fill_masks(masks_ref):
    rows = lax.broadcasted_iota(jnp.int32, (CHUNK, CHUNK), 0)
    cols = lax.broadcasted_iota(jnp.int32, (CHUNK, CHUNK), 1)
    apart = jnp.bitwise_xor(rows, cols)
    for level in range(masks_ref.shape[0]):
        inside = (rows > cols) & (apart >= 2**level) & (apart < 2 ** (level + 1))
        masks_ref[level] = jnp.where(inside, 1.0, 0.0).astype(BF16)


def conv_rows(raw_ref, taps_ref, start, part):
    lanes = slice(part * 128, part * 128 + 128)
    tap_lanes = slice(part % 2 * 128, part % 2 * 128 + 128)
    rows = raw_ref[pl.ds(pl.multiple_of(start + HALO - 8, 8), CHUNK + 8), lanes]
    mixed = taps_ref[part // 2, CONV - 1 : CONV, tap_lanes] * rows[8:]
    for back in range(1, CONV):
        tap = taps_ref[part // 2, CONV - 1 - back : CONV - back, tap_lanes]
        mixed = mixed + tap * pltpu.roll(rows, back, 0)[8:]
    return mixed / (1.0 + jnp.exp(-mixed))


def delta_chunk(chunk, heads, chunks, raw_ref, taps_ref, grow_ref, gcol_ref, bcol_ref, masks_ref,
                map_ref, from_state_ref, local_ref):
    start = chunk * CHUNK
    rows = lax.broadcasted_iota(jnp.int32, (CHUNK, CHUNK), 0)
    cols = lax.broadcasted_iota(jnp.int32, (CHUNK, CHUNK), 1)
    work = []
    for head in range(heads):
        row = head * chunks + chunk
        query = unit_rows(conv_rows(raw_ref, taps_ref, start, head)) * HEAD_DIM ** (-0.5)
        key = unit_rows(conv_rows(raw_ref, taps_ref, start, heads + head))
        value = conv_rows(raw_ref, taps_ref, start, 2 * heads + head)
        gcol, bcol, grow = gcol_ref[row], bcol_ref[row], grow_ref[row][0:1]
        key_b = key.astype(BF16)
        both = jnp.concatenate([query.astype(BF16), key_b], axis=0)
        inner = dot_nt(both, key_b)
        spread = jnp.exp(jnp.minimum(jnp.concatenate([gcol, gcol], axis=1) - grow, 0.0))
        scores = jnp.where(rows >= cols, inner[:CHUNK] * spread, 0.0).astype(BF16)
        strict = jnp.where(rows > cols, inner[CHUNK:] * spread, 0.0)
        strict = (strict * jnp.concatenate([bcol, bcol], axis=1)).astype(BF16)
        grown = jnp.exp(gcol)
        right = jnp.concatenate([value * bcol, key * bcol * grown], axis=1).astype(BF16)
        last = grow[:, CHUNK - 1 : CHUNK]
        key_dec = (key * jnp.exp(last - gcol)).astype(BF16)
        inverse = jnp.where(rows == cols, 1.0, 0.0).astype(BF16) - strict * masks_ref[0]
        work.append([strict, inverse, scores, right, key_dec, query * grown, jnp.exp(last)])
    for level in range(1, masks_ref.shape[0]):
        inner = [dot(w[0] * masks_ref[level], w[1]).astype(BF16) for w in work]
        for w, part in zip(work, inner):
            w[1] = w[1] - dot(w[1], part).astype(BF16)
    for head in range(heads):
        _, inverse, scores, right, key_dec, query_dec, kept = work[head]
        solved = dot(inverse, right).astype(BF16)
        seen = dot(scores, solved)
        moved = dot_tn(key_dec, solved)
        current = map_ref[head]
        current_b = current.astype(BF16)
        asked = (query_dec - seen[:, 128:]).astype(BF16)
        answer = dot(asked, current_b)
        where_rows = pl.ds(pl.multiple_of(start, CHUNK), CHUNK)
        from_state_ref[head, where_rows, :] = answer[:, :128].astype(BF16)
        local_ref[head, where_rows, :] = answer[:, 128:] + seen[:, :128]
        added = jnp.concatenate([jnp.zeros((128, 128), F32), moved[:, :128]], axis=1)
        map_ref[head] = current * kept - dot(moved[:, 128:].astype(BF16), current_b) + added


SPLIT_A = 128
PIECE = 1024
ORDER = ((0, 0), (0, 1), (0, -1), (1, 0), (-1, 0), (1, 1), (1, -1), (-1, 1), (-1, -1), (0, 2), (2, 0),
         (1, 2), (-1, 2), (2, 1), (2, -1), (2, 2))


class PlaneGather:
    def __init__(self, buf, split, send_sems, recv_sems):
        self.buf, self.split = buf, split
        self.send_sems, self.recv_sems = send_sems, recv_sems
        self.z, self.x = lax.axis_index("sp_0"), lax.axis_index("sp_1")
        self.copies = {}

    def shard(self, dz, dx):
        return lax.rem(self.z + dz + 4, 4) * 4 + lax.rem(self.x + dx + 4, 4)

    def rows(self, part):
        split, total = self.split, self.buf.shape[1]
        quarter = split // 32 * 16
        rest = split + (total - split) // 32 * 16
        return {"a": (0, split), "b": (split, total), "a0": (0, quarter), "a1": (quarter, split),
                "b0": (split, rest), "b1": (rest, total)}[part]

    def region(self, dz, dx, part):
        low, high = self.rows(part)
        return self.buf.at[self.shard(dz, dx), pl.ds(low, high - low), :]

    def copy(self, name, way, source):
        index, _, part = self.copies[name, way]
        ref = self.region(source[0], source[1], part)
        return remote(ref, ref, self.send_sems.at[index], self.recv_sems.at[index],
                      {"sp_0": lax.rem(self.z + way[0] + 4, 4),
                       "sp_1": lax.rem(self.x + way[1] + 4, 4)})

    def send(self, name, source, part, way):
        self.copies[name, way] = (len(self.copies), source, part)
        self.copy(name, way, source).start()

    def got(self, name, way):
        source = self.copies[name, way][1]
        self.copy(name, way, (source[0] - way[0], source[1] - way[1])).wait_recv()

    def own(self):
        for step in (1, -1):
            self.send("a", (0, 0), "a", (0, step))
            self.send("b", (0, 0), "b", (step, 0))
        for step in (1, -1):
            self.send("b", (0, 0), "b", (0, step))
            self.send("a", (0, 0), "a", (step, 0))

    def first(self):
        for step in (1, -1):
            self.got("a", (0, step))
            self.got("b", (step, 0))
        self.send("a2", (0, -1), "a0", (0, 1))
        self.send("a2", (0, 1), "a1", (0, -1))
        self.send("b2", (-1, 0), "b0", (1, 0))
        self.send("b2", (1, 0), "b1", (-1, 0))
        for at in (1, -1):
            for step in (1, -1):
                self.send(("a3", at), (0, at), "a", (step, 0))
                self.send(("b3", at), (at, 0), "b", (0, step))

    def second(self):
        for step in (1, -1):
            self.got("b", (0, step))
            self.got("a", (step, 0))
        self.send(("a4", 0), (-1, 0), "a", (1, 0))
        self.send(("b4", 0), (0, -1), "b", (0, 1))

    def third(self, along="xz"):
        for step in (1, -1):
            self.got("a2", (0, step)) if "z" in along else None
            self.got("b2", (step, 0)) if "x" in along else None
        for step in (-1, 1):
            if "z" in along:
                self.send(("a3", 2), (0, 2), "a", (step, 0))
            if "x" in along:
                self.send(("b3", 2), (2, 0), "b", (0, step))

    def fourth(self):
        for at in (1, -1):
            for step in (1, -1):
                self.got(("a3", at), (step, 0))
                self.got(("b3", at), (0, step))
        for at in (1, -1):
            self.send(("a4", at), (-at, at), "a", (at, 0))
            self.send(("b4", at), (at, -at), "b", (0, at))

    def fifth(self):
        for step in (1, -1):
            self.got(("a3", 2), (step, 0))
            self.got(("b3", 2), (0, step))
        self.send(("a4", 2), (1, 2), "a", (-1, 0))
        self.send(("b4", 2), (2, 1), "b", (0, -1))

    def last(self, dz, dx):
        side = {0: 1, 1: 1, -1: -1, 2: -1}
        if dz == 2:
            self.got(("a4", dx), (side[dx], 0))
        if dx == 2:
            self.got(("b4", dz), (0, side[dz]))

    def drain(self):
        for (name, way), (_, source, _) in self.copies.items():
            self.copy(name, way, source).wait_send()


def after(later, earlier):
    offset = jnp.concatenate([jnp.zeros((128, 128), F32), later[:, 128:].astype(F32)], axis=1)
    return dot(later[:, :128], earlier.astype(BF16)) + offset


def device_at(z=0, x=0, tp=0):
    place = {}
    for name, step in (("sp_0", z), ("sp_1", x), ("tp", tp)):
        if step:
            size = lax.axis_size(name)
            place[name] = lax.rem(lax.axis_index(name) + step + size, size)
    return place


def remote(src, dst, send_sem, recv_sem, place):
    return pltpu.make_async_remote_copy(
        src_ref=src, dst_ref=dst, send_sem=send_sem, recv_sem=recv_sem, device_id=place,
        device_id_type=MESH_ID)


def pooled_rows(pool_ref, chunk, position, wide, mix_ref, scales):
    parts = []
    for group in range(2):
        lanes = slice(group * 128, group * 128 + 128)
        rows = pool_ref[pl.ds(pl.multiple_of(chunk * CHUNK, CHUNK), CHUNK + HALO), lanes]
        reach = 1
        sums = rows
        for _ in range(group + 1):
            sums = sums + pltpu.roll(sums, reach, 0)
            reach *= 2
        broad = sums
        for _ in range(2):
            broad = broad + pltpu.roll(broad, reach, 0)
            reach *= 2
        short, long = 2 << group, 8 << group
        seen = lax.broadcasted_iota(jnp.int32, (CHUNK, 128), 0) + (position + chunk * CHUNK + 1)
        count = jnp.minimum(seen, jnp.where(wide, long, short)).astype(F32)
        window = jnp.where(wide, broad[HALO:], sums[HALO:])
        diff = (window / count - rows[HALO:]).astype(BF16)
        parts.append((dot(diff, mix_ref[group]) * scales[group]).astype(BF16))
    return parts


def norm_rows(tok_ref, gain_ref, start, count, step_rows):
    @pl.loop(0, count // step_rows)
    def _(step):
        rows = pl.ds(pl.multiple_of(start + step * step_rows, 16), step_rows)
        values = tok_ref[rows, :].astype(F32)
        scale = lax.rsqrt(jnp.mean(values * values, axis=-1, keepdims=True) + EPSILON)
        tok_ref[rows, :] = (tok_ref[rows, :].astype(F32) * scale * gain_ref[0:1, :]).astype(BF16)


def layer_kernel(heads, tok_hbm, pool_hbm, query_hbm, key_hbm, value_hbm, pool_out_hbm,
                 delta_out_hbm, taps_hbm, mix_hbm, gain_in_ref, head_gain_ref, scale_in_ref,
                 strength_ref, decay_ref, spike_ref, rate_ref, decay_shift_ref, strength_shift_ref,
                 out_ref,
                 tok_ref, wide_ref, pool_w_ref, out_w_ref, acc_ref, pool_ref, thin_ref, gain_ref,
                 taps_in_ref, taps_ref, mix_ref, grow_ref, gcol_ref, bcol_ref, masks_ref, map_ref,
                 from_state_ref, local_ref, own_ref, row_ref, total_ref, column_ref, state_ref,
                 mixed_ref, part_ref, pair_out_ref, pair_in_ref, ring_out_ref, half_ref, final_ref,
                 tok_sems, load_sems, halo_send, halo_recv, send_a, recv_a, send_b, recv_b,
                 send_c, recv_c, send_x, recv_x, send_z, recv_z, pair_send, pair_recv, ring_send,
                 ring_recv):
    z, x, tp = lax.axis_index("sp_0"), lax.axis_index("sp_1"), lax.axis_index("tp")
    n_z, n_x, n_tp = lax.axis_size("sp_0"), lax.axis_size("sp_1"), lax.axis_size("tp")
    y, core = tp // 2, lax.rem(tp, 2)
    n_y = n_tp // 2
    tok_rows, depth = tok_hbm.shape
    chunks = tok_rows // CHUNK
    mine = z * n_x + x
    position = mine * tok_rows
    loads = []
    for k, (hbm, ref) in enumerate((
            (query_hbm, wide_ref.at[mine, pl.ds(0, 256), pl.ds(0, 256)]),
            (key_hbm, wide_ref.at[mine, pl.ds(0, 256), pl.ds(256, 256)]),
            (value_hbm, wide_ref.at[mine, pl.ds(0, 256), pl.ds(512, 256)]),
            (pool_hbm, pool_w_ref.at[mine]),
            (pool_out_hbm, out_w_ref.at[mine, pl.ds(0, 256), :]),
            (delta_out_hbm, out_w_ref.at[mine, pl.ds(256, 256), :]),
            (taps_hbm.at[:, :, pl.ds(pl.multiple_of(tp * 256, 256), 256)], taps_in_ref),
            (mix_hbm.at[pl.ds(tp * 2, 2)], mix_ref))):
        load = pltpu.make_async_copy(hbm, ref, load_sems.at[k])
        load.start()
        loads.append(load)
    tok_loads = []
    for k in range(chunks):
        load = pltpu.make_async_copy(
            tok_hbm.at[pl.ds(k * CHUNK, CHUNK), :],
            tok_ref.at[pl.ds(HALO + k * CHUNK, CHUNK), :], tok_sems.at[k])
        load.start()
        tok_loads.append(load)
    following, before = lax.rem(mine + 1, 16), lax.rem(mine + 15, 16)
    next_place = {"sp_0": following // 4, "sp_1": lax.rem(following, 4)}
    last_place = {"sp_0": before // 4, "sp_1": lax.rem(before, 4)}
    peers = [device_at(x=step) for step in range(1, n_x)]
    peers += [device_at(z=step) for step in range(1, n_z)]
    peers += [device_at(tp=step) for step in range(1, n_tp)]
    peers += [next_place, last_place]
    barrier = pltpu.get_barrier_semaphore()
    for peer in peers:
        pl.semaphore_signal(barrier, 1, device_id=peer, device_id_type=MESH_ID)
    at = lax.broadcasted_iota(jnp.int32, (16, 256), 0)
    thin = jnp.zeros((16, 256), F32)
    for k, (ref, row) in enumerate(((strength_ref, 0), (strength_ref, 1), (decay_ref, 0),
                                    (decay_ref, 1))):
        row_values = ref[...].astype(F32)[row : row + 1]
        thin = jnp.where(at == k, jnp.broadcast_to(row_values, (16, 256)), thin)
    wide_ref[mine, 256:272, 0:256] = thin.astype(BF16)
    wide_ref[mine, 256:272, 256:768] = jnp.zeros((16, 512), BF16)
    gains = gain_in_ref[...].astype(F32)
    for k in range(depth // 128):
        gain_ref[:, k * 128 : k * 128 + 128] = jnp.broadcast_to(gains[k : k + 1], (8, 128))
    fill_masks(masks_ref)
    for load in loads[:3]:
        load.wait()
    pl.semaphore_wait(barrier, len(peers))

    early = PlaneGather(wide_ref, SPLIT_A, send_a, recv_a)
    slices = depth // n_tp

    def halo_part(owner):
        return tok_ref.at[pl.ds(0, HALO), pl.ds(pl.multiple_of(owner * slices, 128), slices)]

    halos = [remote(
        tok_hbm.at[pl.ds(tok_rows - HALO, HALO), pl.ds(pl.multiple_of(tp * slices, 128), slices)],
        halo_part(tp), halo_send.at[0], halo_recv.at[0], next_place)]
    halos[0].start()
    early.own()
    tok_loads[0].wait()
    norm_rows(tok_ref, gain_ref, HALO, CHUNK, 64)
    halos[0].wait_recv()
    for step in range(1, n_tp):
        copy = remote(halo_part(tp), halo_part(tp), halo_send.at[step], halo_recv.at[step],
                      device_at(tp=step))
        copy.start()
        halos.append(copy)
    tok_loads[1].wait()
    norm_rows(tok_ref, gain_ref, HALO + CHUNK, CHUNK, 64)
    early.first()
    for k in range(2, chunks):
        tok_loads[k].wait()
        norm_rows(tok_ref, gain_ref, HALO + k * CHUNK, CHUNK, 64)
    for step in range(1, n_tp):
        owner = lax.rem(tp - step + n_tp, n_tp)
        remote(halo_part(owner), halo_part(owner), halo_send.at[step], halo_recv.at[step],
               device_at(tp=step)).wait_recv()
    for copy in halos:
        copy.wait_send()

    @pl.when(mine == 0)
    def _():
        tok_ref[0:HALO, :] = jnp.zeros((HALO, depth), BF16)

    norm_rows(tok_ref, gain_ref, 0, HALO, HALO)
    early.second()
    tile = 208

    def project(gather, places, into, first=False):
        @pl.loop(0, acc_ref.shape[0] // tile)
        def _(step):
            rows = pl.ds(pl.multiple_of(step * tile, 16), tile)
            total = None if first else into[rows, :]
            narrow = None if first or gather is not early else thin_ref[rows, :]
            for dz, dx in places:
                shard = gather.shard(dz, dx)
                normed = tok_ref[rows, pl.ds(pl.multiple_of(shard * 256, 256), 256)]
                term = dot(normed, gather.buf[shard, 0:256, :])
                total = term if total is None else total + term
                if gather is early:
                    term = dot_nt(normed, gather.buf[shard, 256:272, 0:256])
                    narrow = term if narrow is None else narrow + term
            into[rows, :] = total
            if gather is early:
                thin_ref[rows, :] = narrow

    project(early, ORDER[:1], acc_ref, first=True)
    project(early, ORDER[1:5], acc_ref)
    early.third()
    early.fourth()
    project(early, ORDER[5:9], acc_ref)
    early.fifth()
    for load in loads[3:]:
        load.wait()
    pool = PlaneGather(pool_w_ref, 128, send_b, recv_b)
    pool.own()
    for places in (ORDER[9:13], ORDER[13:]):
        for dz, dx in places:
            early.last(dz, dx)
        project(early, places, acc_ref)

    taps_ref[...] = taps_in_ref[...].astype(F32)
    narrow = thin_ref[HALO:, :].T
    for head in range(heads):
        strength = narrow[head : head + 1] + strength_shift_ref[tp * heads + head]
        beta = 1.0 / (1.0 + jnp.exp(-strength))
        level = narrow[heads + head : heads + head + 1] + decay_shift_ref[tp * heads + head]
        soft = jnp.maximum(level, 0.0) + jnp.log1p(jnp.exp(-jnp.abs(level)))
        rate = jnp.exp(jnp.full((1, tok_rows), rate_ref[tp * heads + head], F32))
        decay = spike_ref[head : head + 1, :] - rate * soft
        lane = lax.rem(lax.broadcasted_iota(jnp.int32, (8, tok_rows), 1), CHUNK)
        summed = jnp.broadcast_to(decay, (8, tok_rows))
        step = 1
        while step < CHUNK:
            summed = summed + jnp.where(lane >= step, pltpu.roll(summed, step, 1), 0.0)
            step *= 2
        for chunk in range(chunks):
            row = head * chunks + chunk
            part = slice(chunk * CHUNK, chunk * CHUNK + CHUNK)
            grow_ref[row] = summed[:, part]
            gcol_ref[row] = jnp.broadcast_to(summed[0:1, part], (128, CHUNK)).T
            bcol_ref[row] = jnp.broadcast_to(beta[:, part], (128, CHUNK)).T
    rows = lax.broadcasted_iota(jnp.int32, (128, 256), 0)
    cols = lax.broadcasted_iota(jnp.int32, (128, 256), 1)
    identity = jnp.where(rows == cols, 1.0, 0.0)
    for head in range(heads):
        map_ref[head] = identity

    out = PlaneGather(out_w_ref, 256, send_c, recv_c)

    @pl.loop(0, chunks)
    def _(chunk):
        @pl.when(chunk == 0)
        def _():
            pool.first()
            pool.second()

        @pl.when(chunk == 1)
        def _():
            pool.third()
            pool.fourth()

        @pl.when(chunk == 2)
        def _():
            pool.fifth()
            out.own()

        delta_chunk(chunk, heads, chunks, acc_ref, taps_ref, grow_ref, gcol_ref, bcol_ref,
                    masks_ref, map_ref, from_state_ref, local_ref)

    own_ref[...] = map_ref[...].astype(BF16)
    row_ref[0] = own_ref[...]
    along_x = [remote(own_ref, row_ref.at[step], send_x.at[step], recv_x.at[step],
                      device_at(x=step)) for step in range(1, n_x)]
    for copy in along_x:
        copy.start()
    out.first()
    for dz, dx in ORDER[9:]:
        pool.last(dz, dx)
    for k in range(4):
        project(pool, ORDER[4 * k : 4 * k + 4], pool_ref, first=k == 0)
    wide = core == 1
    scales_at = lax.broadcasted_iota(jnp.int32, scale_in_ref.shape, 0)
    scales = [jnp.sum(jnp.where(scales_at == tp * 2 + group, scale_in_ref[...].astype(F32), 0.0),
                      axis=0, keepdims=True) for group in range(2)]

    def store_halves(chunk, lanes, values):
        for half in range(2):
            slot = lax.rem(half + core, 2)
            mixed_ref[chunk, pl.ds(pl.multiple_of(slot * 128, 128), 128), lanes] = (
                values[half * 128 : half * 128 + 128])

    for copy in along_x:
        copy.wait_recv()
    inside = []
    for head in range(heads):
        so_far = before_here = identity
        for k in range(n_x):
            piece = row_ref[lax.rem(x - k + n_x, n_x), head]
            so_far = piece.astype(F32) if k == 0 else after(piece, so_far)
            before_here = jnp.where(k < x, so_far, before_here)
        inside.append(before_here)
        total_ref[head] = so_far.astype(BF16)
    along_z = [remote(total_ref, column_ref.at[step], send_z.at[step], recv_z.at[step],
                      device_at(z=step)) for step in range(1, n_z)]
    for copy in along_z:
        copy.start()
    column_ref[0] = total_ref[...]
    out.second()
    out.third()

    @pl.loop(0, chunks)
    def _(chunk):
        for group, values in enumerate(
                pooled_rows(pool_ref, chunk, position, wide, mix_ref, scales)):
            store_halves(chunk, slice(group * 128, group * 128 + 128), values)

    for copy in along_z:
        copy.wait_recv()
    for head in range(heads):
        so_far = state = jnp.zeros((128, 128), F32)
        for k in range(n_z - 1):
            piece = column_ref[lax.rem(z - k + n_z, n_z), head]
            offset = piece[:, 128:].astype(F32)
            so_far = offset if k == 0 else dot(piece[:, :128], so_far.astype(BF16)) + offset
            state = jnp.where(k < z, so_far, state)
        entering = dot(inside[head][:, :128].astype(BF16), state.astype(BF16))
        state_ref[head] = (entering + inside[head][:, 128:]).astype(BF16)
    out.fourth()

    head_gain = head_gain_ref[...].astype(F32)
    partner = {"tp": y * 2 + (1 - core)}
    pairs, rings, finals, halves = {}, [], {}, {}
    slots = {2: 0, 1: 1, 3: 2, 0: 0}

    def finish_rows(ahead):
        chunk = lax.rem(y + ahead, n_y)
        where_rows = pl.ds(pl.multiple_of(chunk * CHUNK, CHUNK), CHUNK)
        for head in range(heads):
            raw = dot(from_state_ref[head, where_rows, :], state_ref[head])
            raw = raw + local_ref[head, where_rows, :]
            squares = jnp.mean(raw * raw, axis=-1, keepdims=True)
            normed = (raw * lax.rsqrt(squares + EPSILON) * head_gain).astype(BF16)
            store_halves(chunk, slice(256 + head * 128, 384 + head * 128), normed)

    def produce(ahead, piece):
        chunk = lax.rem(y + ahead, n_y)
        for block, (dz, dx) in enumerate(ORDER[4 * piece : 4 * piece + 4]):
            lanes = slice(block * 256, block * 256 + 256)
            product = dot(mixed_ref[chunk], out_w_ref[out.shard(dz, dx)])
            part_ref[slots[ahead], piece, :, lanes] = product[:128]
            pair_out_ref[ahead, piece, :, lanes] = product[128:].astype(BF16)
        index = ahead * 4 + piece
        copy = remote(pair_out_ref.at[ahead, piece], pair_in_ref.at[ahead, piece],
                      pair_send.at[index], pair_recv.at[index], partner)
        copy.start()
        pairs[ahead, piece] = copy

    def chip_sum(ahead, piece):
        pairs[ahead, piece].wait_recv()
        return part_ref[slots[ahead], piece] + pair_in_ref[ahead, piece].astype(F32)

    def pass_on(ahead, piece, place, target, merge=False):
        value = chip_sum(ahead, piece)
        if merge:
            halves[piece].wait_recv()
            value = value + half_ref[piece].astype(F32)
        ring_out_ref[ahead - 1, piece] = value.astype(BF16)
        index = len(rings)
        copy = remote(ring_out_ref.at[ahead - 1, piece], target, ring_send.at[index],
                      ring_recv.at[index], place)
        copy.start()
        rings.append(copy)
        return copy

    up, down = device_at(tp=2), device_at(tp=-2)

    def far(piece):
        halves[piece] = pass_on(2, piece, down if piece % 2 else up, half_ref.at[piece])

    def near(ahead, piece, merge=False):
        side = 0 if ahead == 1 else 1
        finals[side, piece] = pass_on(ahead, piece, down if side else up,
                                      final_ref.at[side, piece], merge)

    finish_rows(2)
    produce(2, 0)
    produce(2, 1)
    far(0)
    far(1)
    out.fifth()
    finish_rows(1)
    finish_rows(3)
    produce(1, 1)
    produce(3, 0)
    near(1, 1)
    near(3, 0)
    for dz, dx in ORDER[9:]:
        out.last(dz, dx)
    produce(2, 2)
    produce(2, 3)
    far(2)
    far(3)
    produce(1, 3)
    produce(3, 2)
    near(1, 3)
    near(3, 2)
    for piece in (0, 2):
        produce(1, piece)
        produce(3, piece + 1)
    finish_rows(0)
    for piece in range(4):
        produce(0, piece)
    for piece in (0, 2):
        near(1, piece, merge=True)
        near(3, piece + 1, merge=True)
    for piece in range(4):
        part_ref[0, piece] = chip_sum(0, piece)
    arrived = set()
    for key in ((0, 1), (1, 0), (0, 3), (1, 2), (0, 0), (1, 1), (0, 2), (1, 3)):
        side, piece = key
        finals[key].wait_recv()
        value = part_ref[0, piece] + final_ref[side, piece].astype(F32)
        if (1 - side, piece) not in arrived:
            part_ref[0, piece] = value
        else:
            for block, (dz, dx) in enumerate(ORDER[4 * piece : 4 * piece + 4]):
                lanes = pl.ds(pl.multiple_of(out.shard(dz, dx) * 256, 256), 256)
                out_ref[:, lanes] = value[:, block * 256 : block * 256 + 256].astype(BF16)
        arrived.add(key)
    for copy in along_x + along_z + list(pairs.values()) + rings:
        copy.wait_send()
    for gather in (early, pool, out):
        gather.drain()


def per_device(tokens, input_norm_scale, mean_input_weight, query_matrix, key_matrix, value_matrix,
               strength_weight, decay_input_weight, causal_filter_weight, head_decay_logrates,
               decay_input_shift, strength_shift, decay_spike, head_norm_scale,
               group_mixing_weight, mean_channel_scale, mean_output_weight, delta_output_weight):
    tok_rows, depth = tokens.shape
    heads = strength_weight.shape[1]
    n_z, n_x = lax.axis_size("sp_0"), lax.axis_size("sp_1")
    chunks = tok_rows // CHUNK
    pairs = heads * chunks
    width = n_z * n_x * 256
    pieces = width // PIECE
    vmem = pl.BlockSpec(memory_space=pltpu.VMEM)
    smem = pl.BlockSpec(memory_space=pltpu.SMEM)
    hbm = pl.BlockSpec(memory_space=pl.ANY)
    dma = pltpu.SemaphoreType.DMA
    return pl.pallas_call(
        lambda *refs: layer_kernel(heads, *refs),
        out_shape=jax.ShapeDtypeStruct((128, width), BF16),
        in_specs=[hbm] * 9 + [vmem] * 6 + [smem] * 3,
        out_specs=vmem,
        scratch_shapes=[
            pltpu.VMEM((tok_rows + HALO, depth), BF16),
            pltpu.VMEM((16, 272, 768), BF16),
            pltpu.VMEM((16, 256, 256), BF16),
            pltpu.VMEM((16, 512, 256), BF16),
            pltpu.VMEM((tok_rows + HALO, 768), F32),
            pltpu.VMEM((tok_rows + HALO, 256), F32),
            pltpu.VMEM((tok_rows + HALO, 16), F32),
            pltpu.VMEM((8, depth), F32),
            pltpu.VMEM((3, CONV, 256), BF16),
            pltpu.VMEM((3, CONV, 256), F32),
            pltpu.VMEM((2, 128, 128), BF16),
            pltpu.VMEM((pairs, 8, CHUNK), F32),
            pltpu.VMEM((pairs, CHUNK, 128), F32),
            pltpu.VMEM((pairs, CHUNK, 128), F32),
            pltpu.VMEM((8, CHUNK, CHUNK), BF16),
            pltpu.VMEM((heads, 128, 256), F32),
            pltpu.VMEM((heads, tok_rows, 128), BF16),
            pltpu.VMEM((heads, tok_rows, 128), F32),
            pltpu.VMEM((heads, 128, 256), BF16),
            pltpu.VMEM((n_x, heads, 128, 256), BF16),
            pltpu.VMEM((heads, 128, 256), BF16),
            pltpu.VMEM((n_z, heads, 128, 256), BF16),
            pltpu.VMEM((heads, 128, 128), BF16),
            pltpu.VMEM((chunks, CHUNK, 512), BF16),
            pltpu.VMEM((3, pieces, 128, PIECE), F32),
            pltpu.VMEM((4, pieces, 128, PIECE), BF16),
            pltpu.VMEM((4, pieces, 128, PIECE), BF16),
            pltpu.VMEM((3, pieces, 128, PIECE), BF16),
            pltpu.VMEM((pieces, 128, PIECE), BF16),
            pltpu.VMEM((2, pieces, 128, PIECE), BF16),
            dma((chunks,)), dma((8,)), dma((8,)), dma((8,)),
            dma((32,)), dma((32,)), dma((32,)), dma((32,)), dma((32,)), dma((32,)),
            dma((n_x,)), dma((n_x,)), dma((n_z,)), dma((n_z,)),
            dma((16,)), dma((16,)), dma((12,)), dma((12,)),
        ],
        compiler_params=pltpu.CompilerParams(
            vmem_limit_bytes=VMEM_LIMIT, collective_id=0, has_side_effects=True),
        name="layer",
    )(tokens, mean_input_weight, query_matrix, key_matrix, value_matrix, mean_output_weight,
      delta_output_weight, jnp.transpose(causal_filter_weight, (1, 0, 2)), group_mixing_weight,
      input_norm_scale.reshape(-1, 128), head_norm_scale.reshape(1, HEAD_DIM),
      mean_channel_scale.reshape(-1, 128), strength_weight.T, decay_input_weight.T, decay_spike.T,
      head_decay_logrates, decay_input_shift, strength_shift)


def solution(mesh):
    finer = Mesh(mesh.devices.reshape(4, 4, mesh.shape["tp"]), SP_TP)
    in_specs = (
        P(SP, None), P(), P(SP, "tp"), P(SP, "tp"), P(SP, "tp"), P(SP, "tp"), P(SP, "tp"),
        P(SP, "tp"), P(), P(), P(), P(), P(SP, "tp"), P(), P(), P(), P("tp", SP), P("tp", SP),
    )
    return jax.shard_map(
        per_device, mesh=finer, in_specs=in_specs, out_specs=P(SP_TP, None), check_vma=False
    )
```

time: 212 us -> 134 us (0.63)
  waiting for transfers between devices: 58 us -> 0 us
  between operations: 13.4 us -> 0.01 us
  Pallas kernels: 118 us -> 131 us
  matrix products: 10.3 us -> 0 us
  local copies, waits for them, and re-layouts: 7.72 us -> 2.29 us
  other arithmetic: 4.48 us -> 0 us
    reduce_scatter x1 -> x0, waiting for transfers between devices: 58 us -> none  [per_device(): lax.psum_scatter(jnp.dot(mixed, out_weight, preferred_element_type=F32).a...]
    pallas_call x3 -> x1, Pallas kernels: 118 us -> 131 us  [per_device(): pl.pallas_call(lambda *refs: layer_kernel(heads, *refs), out_shape=jax.Sh...]
    dot_general x1 -> x0, matrix products: 10.3 us -> none  [per_device(): jnp.dot(mixed, out_weight, preferred_element_type=F32).astype(BF16)]
    transpose x1 -> x0, local copies, waits for them, and re-layouts: 6.39 us -> none  [per_device(): out_weight = jnp.transpose(out_weight, (1, 0, 2)).reshape(512, -1)]
    reshape x3 -> x0, other arithmetic: 3.88 us -> none  [the longest x1 1.32 us: per_device(): scale.astype(F32).reshape(1, pool_cols)]
    unnamed x2 -> x1, local copies, waits for them, and re-layouts: 0.01 us -> 2.29 us
  transfers between devices with their start and end apart: 1 -> 0, of which waited for: 1 -> 0; matrix products, arithmetic and copies ran while one was open for 0% -> 0% of each run, Pallas kernels for 0% -> 0%
where the time goes in v4:
time: 134 us; the launch traced here: 133 us
  Pallas kernels  131 us (98%)
  local copies, waits for them, and re-layouts  2.29 us (2%)
    pallas_call x1, Pallas kernels, per_device(): pl.pallas_call(lambda *refs: layer_kernel(heads, *refs), out_shape=jax.Sh...  131 us

profile of v4, /device:TPU:1, one launch (start us, length us, event | category | flops | bytes accessed | tf_op | source)
XLA Modules:
  0.0 133.4 jit_solution(15294726193457867726)
XLA Ops:
  0.0 131.1 %layer.1 = bf16[128,4096]{1,0:T(8,128)(2,1)} custom-call(bf16[1024,4096]{1,0:T(8,128)(2,1)} %refs_0_.1, bf16[256,256]{1,0:T(8,128)(2,1)} %refs_1_.1, bf16[256,256]{1,0:T(8,128)(2,1)} %refs_2_.1, bf16[256,256]{1,0:T(8,128)(2,1)} %refs_3_.1, bf16[256,256]{1,0:T(8,128)(2,1)} %refs_4_.1, bf16[256,256]{1,0:T(8,128)(2,1)} %refs_5_.1, bf16[256,256]{1,0:T(8,128)(2,1)} %refs_6_.1, ...), custom_call_target="tpu_custom_call" | custom-call | tf_op jit(solution)/shard_map/layer/pallas_call | solution.py:631
  131.2 2.3 %copy.20 = bf16[128,4096]{1,0:T(8,128)(2,1)} copy(bf16[128,4096]{1,0:T(8,128)(2,1)} %layer.1) | data formatting | bytes 2097152

commit v5 on v4

--- a/solution.py
+++ b/solution.py
@@ -44,28 +44,28 @@
         masks_ref[level] = jnp.where(inside, 1.0, 0.0).astype(BF16)
 
 
-def conv_rows(raw_ref, taps_ref, start, part):
+def conv_rows(raw_ref, taps_ref, head, start, part):
     lanes = slice(part * 128, part * 128 + 128)
-    tap_lanes = slice(part % 2 * 128, part % 2 * 128 + 128)
-    rows = raw_ref[pl.ds(pl.multiple_of(start + HALO - 8, 8), CHUNK + 8), lanes]
-    mixed = taps_ref[part // 2, CONV - 1 : CONV, tap_lanes] * rows[8:]
+    tap_lanes = slice(head * 128, head * 128 + 128)
+    rows = raw_ref[head, start + HALO - 8 : start + HALO + CHUNK, lanes]
+    mixed = taps_ref[part, CONV - 1 : CONV, tap_lanes] * rows[8:]
     for back in range(1, CONV):
-        tap = taps_ref[part // 2, CONV - 1 - back : CONV - back, tap_lanes]
+        tap = taps_ref[part, CONV - 1 - back : CONV - back, tap_lanes]
         mixed = mixed + tap * pltpu.roll(rows, back, 0)[8:]
     return mixed / (1.0 + jnp.exp(-mixed))
 
 
-def delta_chunk(chunk, heads, chunks, raw_ref, taps_ref, grow_ref, gcol_ref, bcol_ref, masks_ref,
-                map_ref, from_state_ref, local_ref):
-    start = chunk * CHUNK
+def delta_head(head, chunks, raw_ref, taps_ref, grow_ref, gcol_ref, bcol_ref, masks_ref, map_ref,
+               from_state_ref, local_ref, events):
     rows = lax.broadcasted_iota(jnp.int32, (CHUNK, CHUNK), 0)
     cols = lax.broadcasted_iota(jnp.int32, (CHUNK, CHUNK), 1)
     work = []
-    for head in range(heads):
+    for chunk in range(chunks):
         row = head * chunks + chunk
-        query = unit_rows(conv_rows(raw_ref, taps_ref, start, head)) * HEAD_DIM ** (-0.5)
-        key = unit_rows(conv_rows(raw_ref, taps_ref, start, heads + head))
-        value = conv_rows(raw_ref, taps_ref, start, 2 * heads + head)
+        start = chunk * CHUNK
+        query = unit_rows(conv_rows(raw_ref, taps_ref, head, start, 0)) * HEAD_DIM ** (-0.5)
+        key = unit_rows(conv_rows(raw_ref, taps_ref, head, start, 1))
+        value = conv_rows(raw_ref, taps_ref, head, start, 2)
         gcol, bcol, grow = gcol_ref[row], bcol_ref[row], grow_ref[row][0:1]
         key_b = key.astype(BF16)
         both = jnp.concatenate([query.astype(BF16), key_b], axis=0)
@@ -80,24 +80,27 @@
         key_dec = (key * jnp.exp(last - gcol)).astype(BF16)
         inverse = jnp.where(rows == cols, 1.0, 0.0).astype(BF16) - strict * masks_ref[0]
         work.append([strict, inverse, scores, right, key_dec, query * grown, jnp.exp(last)])
+        events.get(("chunk", chunk), lambda: None)()
     for level in range(1, masks_ref.shape[0]):
         inner = [dot(w[0] * masks_ref[level], w[1]).astype(BF16) for w in work]
         for w, part in zip(work, inner):
             w[1] = w[1] - dot(w[1], part).astype(BF16)
-    for head in range(heads):
-        _, inverse, scores, right, key_dec, query_dec, kept = work[head]
-        solved = dot(inverse, right).astype(BF16)
-        seen = dot(scores, solved)
-        moved = dot_tn(key_dec, solved)
-        current = map_ref[head]
+        events.get(("level", level), lambda: None)()
+    solved = [dot(w[1], w[3]).astype(BF16) for w in work]
+    seen = [dot(w[2], s) for w, s in zip(work, solved)]
+    moved = [dot_tn(w[4], s) for w, s in zip(work, solved)]
+    current = map_ref[head]
+    for chunk in range(chunks):
+        where_rows = slice(chunk * CHUNK, chunk * CHUNK + CHUNK)
         current_b = current.astype(BF16)
-        asked = (query_dec - seen[:, 128:]).astype(BF16)
+        asked = (work[chunk][5] - seen[chunk][:, 128:]).astype(BF16)
         answer = dot(asked, current_b)
-        where_rows = pl.ds(pl.multiple_of(start, CHUNK), CHUNK)
         from_state_ref[head, where_rows, :] = answer[:, :128].astype(BF16)
-        local_ref[head, where_rows, :] = answer[:, 128:] + seen[:, :128]
-        added = jnp.concatenate([jnp.zeros((128, 128), F32), moved[:, :128]], axis=1)
-        map_ref[head] = current * kept - dot(moved[:, 128:].astype(BF16), current_b) + added
+        local_ref[head, where_rows, :] = answer[:, 128:] + seen[chunk][:, :128]
+        added = jnp.concatenate([jnp.zeros((128, 128), F32), moved[chunk][:, :128]], axis=1)
+        current = (current * work[chunk][6] - dot(moved[chunk][:, 128:].astype(BF16), current_b)
+                   + added)
+    map_ref[head] = current
 
 
 SPLIT_A = 128
@@ -142,13 +145,13 @@
         source = self.copies[name, way][1]
         self.copy(name, way, (source[0] - way[0], source[1] - way[1])).wait_recv()
 
-    def own(self):
-        for step in (1, -1):
-            self.send("a", (0, 0), "a", (0, step))
-            self.send("b", (0, 0), "b", (step, 0))
-        for step in (1, -1):
-            self.send("b", (0, 0), "b", (0, step))
-            self.send("a", (0, 0), "a", (step, 0))
+    def own(self, along="xz"):
+        for part in range(2):
+            for step in (1, -1):
+                if "x" in along:
+                    self.send("ab"[part], (0, 0), "ab"[part], (0, step))
+                if "z" in along:
+                    self.send("ba"[part], (0, 0), "ba"[part], (step, 0))
 
     def first(self):
         for step in (1, -1):
@@ -264,11 +267,11 @@
                  delta_out_hbm, taps_hbm, mix_hbm, gain_in_ref, head_gain_ref, scale_in_ref,
                  strength_ref, decay_ref, spike_ref, rate_ref, decay_shift_ref, strength_shift_ref,
                  out_ref,
-                 tok_ref, wide_ref, pool_w_ref, out_w_ref, acc_ref, pool_ref, thin_ref, gain_ref,
+                 tok_ref, wide_ref, next_ref, pool_w_ref, out_w_ref, acc_ref, pool_ref, thin_ref, gain_ref,
                  taps_in_ref, taps_ref, mix_ref, grow_ref, gcol_ref, bcol_ref, masks_ref, map_ref,
                  from_state_ref, local_ref, own_ref, row_ref, total_ref, column_ref, state_ref,
                  mixed_ref, part_ref, pair_out_ref, pair_in_ref, ring_out_ref, half_ref, final_ref,
-                 tok_sems, load_sems, halo_send, halo_recv, send_a, recv_a, send_b, recv_b,
+                 tok_sems, load_sems, halo_send, halo_recv, send_a, recv_a, send_d, recv_d, send_b, recv_b,
                  send_c, recv_c, send_x, recv_x, send_z, recv_z, pair_send, pair_recv, ring_send,
                  ring_recv):
     z, x, tp = lax.axis_index("sp_0"), lax.axis_index("sp_1"), lax.axis_index("tp")
@@ -281,9 +284,12 @@
     position = mine * tok_rows
     loads = []
     for k, (hbm, ref) in enumerate((
-            (query_hbm, wide_ref.at[mine, pl.ds(0, 256), pl.ds(0, 256)]),
-            (key_hbm, wide_ref.at[mine, pl.ds(0, 256), pl.ds(256, 256)]),
-            (value_hbm, wide_ref.at[mine, pl.ds(0, 256), pl.ds(512, 256)]),
+            (query_hbm.at[:, pl.ds(0, 128)], wide_ref.at[mine, pl.ds(0, 256), pl.ds(0, 128)]),
+            (key_hbm.at[:, pl.ds(0, 128)], wide_ref.at[mine, pl.ds(0, 256), pl.ds(128, 128)]),
+            (value_hbm.at[:, pl.ds(0, 128)], wide_ref.at[mine, pl.ds(0, 256), pl.ds(256, 128)]),
+            (query_hbm.at[:, pl.ds(128, 128)], next_ref.at[mine, :, pl.ds(0, 128)]),
+            (key_hbm.at[:, pl.ds(128, 128)], next_ref.at[mine, :, pl.ds(128, 128)]),
+            (value_hbm.at[:, pl.ds(128, 128)], next_ref.at[mine, :, pl.ds(256, 128)]),
             (pool_hbm, pool_w_ref.at[mine]),
             (pool_out_hbm, out_w_ref.at[mine, pl.ds(0, 256), :]),
             (delta_out_hbm, out_w_ref.at[mine, pl.ds(256, 256), :]),
@@ -316,7 +322,7 @@
         row_values = ref[...].astype(F32)[row : row + 1]
         thin = jnp.where(at == k, jnp.broadcast_to(row_values, (16, 256)), thin)
     wide_ref[mine, 256:272, 0:256] = thin.astype(BF16)
-    wide_ref[mine, 256:272, 256:768] = jnp.zeros((16, 512), BF16)
+    wide_ref[mine, 256:272, 256:384] = jnp.zeros((16, 128), BF16)
     gains = gain_in_ref[...].astype(F32)
     for k in range(depth // 128):
         gain_ref[:, k * 128 : k * 128 + 128] = jnp.broadcast_to(gains[k : k + 1], (8, 128))
@@ -336,20 +342,16 @@
         halo_part(tp), halo_send.at[0], halo_recv.at[0], next_place)]
     halos[0].start()
     early.own()
-    tok_loads[0].wait()
-    norm_rows(tok_ref, gain_ref, HALO, CHUNK, 64)
-    halos[0].wait_recv()
-    for step in range(1, n_tp):
-        copy = remote(halo_part(tp), halo_part(tp), halo_send.at[step], halo_recv.at[step],
-                      device_at(tp=step))
-        copy.start()
-        halos.append(copy)
-    tok_loads[1].wait()
-    norm_rows(tok_ref, gain_ref, HALO + CHUNK, CHUNK, 64)
-    early.first()
-    for k in range(2, chunks):
+    for k in range(chunks):
         tok_loads[k].wait()
         norm_rows(tok_ref, gain_ref, HALO + k * CHUNK, CHUNK, 64)
+        if k == 1:
+            halos[0].wait_recv()
+            for step in range(1, n_tp):
+                copy = remote(halo_part(tp), halo_part(tp), halo_send.at[step],
+                              halo_recv.at[step], device_at(tp=step))
+                copy.start()
+                halos.append(copy)
     for step in range(1, n_tp):
         owner = lax.rem(tp - step + n_tp, n_tp)
         remote(halo_part(owner), halo_part(owner), halo_send.at[step], halo_recv.at[step],
@@ -362,11 +364,10 @@
         tok_ref[0:HALO, :] = jnp.zeros((HALO, depth), BF16)
 
     norm_rows(tok_ref, gain_ref, 0, HALO, HALO)
-    early.second()
     tile = 208
 
     def project(gather, places, into, first=False):
-        @pl.loop(0, acc_ref.shape[0] // tile)
+        @pl.loop(0, tok_ref.shape[0] // tile)
         def _(step):
             rows = pl.ds(pl.multiple_of(step * tile, 16), tile)
             total = None if first else into[rows, :]
@@ -383,20 +384,27 @@
             if gather is early:
                 thin_ref[rows, :] = narrow
 
-    project(early, ORDER[:1], acc_ref, first=True)
-    project(early, ORDER[1:5], acc_ref)
+    first_acc, second_acc = acc_ref.at[0], acc_ref.at[1]
+    early.first()
+    project(early, ORDER[:1], first_acc, first=True)
+    early.second()
+    project(early, ORDER[1:5], first_acc)
     early.third()
-    early.fourth()
-    project(early, ORDER[5:9], acc_ref)
-    early.fifth()
     for load in loads[3:]:
         load.wait()
-    pool = PlaneGather(pool_w_ref, 128, send_b, recv_b)
-    pool.own()
-    for places in (ORDER[9:13], ORDER[13:]):
-        for dz, dx in places:
-            early.last(dz, dx)
-        project(early, places, acc_ref)
+    early.fourth()
+    later = PlaneGather(next_ref, SPLIT_A, send_d, recv_d)
+    later.own()
+    project(early, ORDER[5:9], first_acc)
+    early.fifth()
+    for dz, dx in ORDER[9:13]:
+        early.last(dz, dx)
+    project(early, ORDER[9:13], first_acc)
+    later.first()
+    for dz, dx in ORDER[13:]:
+        early.last(dz, dx)
+    project(early, ORDER[13:], first_acc)
+    later.second()
 
     taps_ref[...] = taps_in_ref[...].astype(F32)
     narrow = thin_ref[HALO:, :].T
@@ -425,87 +433,104 @@
     for head in range(heads):
         map_ref[head] = identity
 
+    pool = PlaneGather(pool_w_ref, 128, send_b, recv_b)
     out = PlaneGather(out_w_ref, 256, send_c, recv_c)
-
-    @pl.loop(0, chunks)
-    def _(chunk):
-        @pl.when(chunk == 0)
-        def _():
-            pool.first()
-            pool.second()
-
-        @pl.when(chunk == 1)
-        def _():
-            pool.third()
-            pool.fourth()
-
-        @pl.when(chunk == 2)
-        def _():
-            pool.fifth()
-            out.own()
-
-        delta_chunk(chunk, heads, chunks, acc_ref, taps_ref, grow_ref, gcol_ref, bcol_ref,
-                    masks_ref, map_ref, from_state_ref, local_ref)
-
-    own_ref[...] = map_ref[...].astype(BF16)
-    row_ref[0] = own_ref[...]
-    along_x = [remote(own_ref, row_ref.at[step], send_x.at[step], recv_x.at[step],
-                      device_at(x=step)) for step in range(1, n_x)]
-    for copy in along_x:
-        copy.start()
-    out.first()
-    for dz, dx in ORDER[9:]:
-        pool.last(dz, dx)
-    for k in range(4):
-        project(pool, ORDER[4 * k : 4 * k + 4], pool_ref, first=k == 0)
-    wide = core == 1
-    scales_at = lax.broadcasted_iota(jnp.int32, scale_in_ref.shape, 0)
-    scales = [jnp.sum(jnp.where(scales_at == tp * 2 + group, scale_in_ref[...].astype(F32), 0.0),
-                      axis=0, keepdims=True) for group in range(2)]
-
-    def store_halves(chunk, lanes, values):
-        for half in range(2):
-            slot = lax.rem(half + core, 2)
-            mixed_ref[chunk, pl.ds(pl.multiple_of(slot * 128, 128), 128), lanes] = (
-                values[half * 128 : half * 128 + 128])
-
-    for copy in along_x:
-        copy.wait_recv()
-    inside = []
-    for head in range(heads):
+    along_x, along_z = {}, {}
+
+    def delta(head, events):
+        delta_head(head, chunks, acc_ref, taps_ref, grow_ref, gcol_ref, bcol_ref, masks_ref,
+                   map_ref, from_state_ref, local_ref, events)
+
+    def send_x_maps(head):
+        own_ref[head] = map_ref[head].astype(BF16)
+        row_ref[0, head] = own_ref[head]
+        along_x[head] = [
+            remote(own_ref.at[head], row_ref.at[step, head], send_x.at[head, step],
+                   recv_x.at[head, step], device_at(x=step)) for step in range(1, n_x)]
+        for copy in along_x[head]:
+            copy.start()
+
+    def send_z_maps(head):
+        for copy in along_x[head]:
+            copy.wait_recv()
         so_far = before_here = identity
         for k in range(n_x):
             piece = row_ref[lax.rem(x - k + n_x, n_x), head]
             so_far = piece.astype(F32) if k == 0 else after(piece, so_far)
             before_here = jnp.where(k < x, so_far, before_here)
-        inside.append(before_here)
+        map_ref[head] = before_here
         total_ref[head] = so_far.astype(BF16)
-    along_z = [remote(total_ref, column_ref.at[step], send_z.at[step], recv_z.at[step],
-                      device_at(z=step)) for step in range(1, n_z)]
-    for copy in along_z:
-        copy.start()
-    column_ref[0] = total_ref[...]
-    out.second()
-    out.third()
-
-    @pl.loop(0, chunks)
-    def _(chunk):
-        for group, values in enumerate(
-                pooled_rows(pool_ref, chunk, position, wide, mix_ref, scales)):
-            store_halves(chunk, slice(group * 128, group * 128 + 128), values)
-
-    for copy in along_z:
-        copy.wait_recv()
-    for head in range(heads):
+        column_ref[0, head] = total_ref[head]
+        along_z[head] = [
+            remote(total_ref.at[head], column_ref.at[step, head], send_z.at[head, step],
+                   recv_z.at[head, step], device_at(z=step)) for step in range(1, n_z)]
+        for copy in along_z[head]:
+            copy.start()
+
+    def enter(head):
+        for copy in along_z[head]:
+            copy.wait_recv()
         so_far = state = jnp.zeros((128, 128), F32)
         for k in range(n_z - 1):
             piece = column_ref[lax.rem(z - k + n_z, n_z), head]
             offset = piece[:, 128:].astype(F32)
             so_far = offset if k == 0 else dot(piece[:, :128], so_far.astype(BF16)) + offset
             state = jnp.where(k < z, so_far, state)
-        entering = dot(inside[head][:, :128].astype(BF16), state.astype(BF16))
-        state_ref[head] = (entering + inside[head][:, 128:]).astype(BF16)
-    out.fourth()
+        entering = dot(map_ref[head, :, 0:128].astype(BF16), state.astype(BF16))
+        state_ref[head] = (entering + map_ref[head, :, 128:256]).astype(BF16)
+
+    delta(0, {("chunk", 3): later.third, ("level", 3): later.fourth})
+    later.fifth()
+    pool.own()
+    send_x_maps(0)
+    project(later, ORDER[:5], second_acc, first=True)
+    project(later, ORDER[5:9], second_acc)
+    for places in (ORDER[9:13], ORDER[13:]):
+        for dz, dx in places:
+            later.last(dz, dx)
+        project(later, places, second_acc)
+
+    def pool_early():
+        pool.first()
+        pool.second()
+
+    def pool_middle():
+        pool.third()
+        pool.fourth()
+
+    pool_early()
+    delta(1, {("chunk", 1): lambda: send_z_maps(0), ("chunk", 3): pool_middle,
+              ("level", 4): pool.fifth})
+    send_x_maps(1)
+    out.own("x")
+    enter(0)
+    wide = core == 1
+    scales_at = lax.broadcasted_iota(jnp.int32, scale_in_ref.shape, 0)
+    scales = [jnp.sum(jnp.where(scales_at == tp * 2 + group, scale_in_ref[...].astype(F32), 0.0),
+                      axis=0, keepdims=True) for group in range(2)]
+
+    def store_halves(chunk, lanes, values):
+        for half in range(2):
+            slot = lax.rem(half + core, 2)
+            mixed_ref[chunk, pl.ds(pl.multiple_of(slot * 128, 128), 128), lanes] = (
+                values[half * 128 : half * 128 + 128])
+
+    project(pool, ORDER[:8], pool_ref, first=True)
+    send_z_maps(1)
+    out.own("z")
+    for dz, dx in ORDER[9:]:
+        pool.last(dz, dx)
+    project(pool, ORDER[8:], pool_ref)
+    out.first()
+
+    @pl.loop(0, chunks)
+    def _(chunk):
+        for group, values in enumerate(
+                pooled_rows(pool_ref, chunk, position, wide, mix_ref, scales)):
+            store_halves(chunk, slice(group * 128, group * 128 + 128), values)
+
+    enter(1)
+    out.second()
 
     head_gain = head_gain_ref[...].astype(F32)
     partner = {"tp": y * 2 + (1 - core)}
@@ -564,39 +589,53 @@
 
     finish_rows(2)
     produce(2, 0)
-    produce(2, 1)
     far(0)
-    far(1)
-    out.fifth()
+    out.third()
     finish_rows(1)
     finish_rows(3)
+    out.fourth()
+    produce(2, 1)
+    far(1)
     produce(1, 1)
     produce(3, 0)
     near(1, 1)
     near(3, 0)
+    out.fifth()
+    produce(1, 0)
+    produce(3, 1)
+    early.drain()
+    later.drain()
+    near(1, 0, merge=True)
+    near(3, 1, merge=True)
     for dz, dx in ORDER[9:]:
         out.last(dz, dx)
-    produce(2, 2)
-    produce(2, 3)
-    far(2)
-    far(3)
+    for piece in (2, 3):
+        produce(2, piece)
+        far(piece)
     produce(1, 3)
+    near(1, 3)
     produce(3, 2)
-    near(1, 3)
     near(3, 2)
-    for piece in (0, 2):
-        produce(1, piece)
-        produce(3, piece + 1)
+    produce(1, 2)
+    produce(3, 3)
     finish_rows(0)
     for piece in range(4):
         produce(0, piece)
-    for piece in (0, 2):
-        near(1, piece, merge=True)
-        near(3, piece + 1, merge=True)
+    pool.drain()
+    out.drain()
+    near(1, 2, merge=True)
+    near(3, 3, merge=True)
     for piece in range(4):
         part_ref[0, piece] = chip_sum(0, piece)
+    for head in range(heads):
+        for copy in along_x[head] + along_z[head]:
+            copy.wait_send()
+    for copy in pairs.values():
+        copy.wait_send()
+    for copy in rings[:8]:
+        copy.wait_send()
     arrived = set()
-    for key in ((0, 1), (1, 0), (0, 3), (1, 2), (0, 0), (1, 1), (0, 2), (1, 3)):
+    for key in ((0, 1), (1, 0), (0, 0), (1, 1), (0, 3), (1, 2), (0, 2), (1, 3)):
         side, piece = key
         finals[key].wait_recv()
         value = part_ref[0, piece] + final_ref[side, piece].astype(F32)
@@ -607,10 +646,8 @@
                 lanes = pl.ds(pl.multiple_of(out.shard(dz, dx) * 256, 256), 256)
                 out_ref[:, lanes] = value[:, block * 256 : block * 256 + 256].astype(BF16)
         arrived.add(key)
-    for copy in along_x + along_z + list(pairs.values()) + rings:
+    for copy in rings[8:]:
         copy.wait_send()
-    for gather in (early, pool, out):
-        gather.drain()
 
 
 def per_device(tokens, input_norm_scale, mean_input_weight, query_matrix, key_matrix, value_matrix,
@@ -635,10 +672,11 @@
         out_specs=vmem,
         scratch_shapes=[
             pltpu.VMEM((tok_rows + HALO, depth), BF16),
-            pltpu.VMEM((16, 272, 768), BF16),
+            pltpu.VMEM((16, 272, 384), BF16),
+            pltpu.VMEM((16, 256, 384), BF16),
             pltpu.VMEM((16, 256, 256), BF16),
             pltpu.VMEM((16, 512, 256), BF16),
-            pltpu.VMEM((tok_rows + HALO, 768), F32),
+            pltpu.VMEM((heads, tok_rows + HALO, 384), F32),
             pltpu.VMEM((tok_rows + HALO, 256), F32),
             pltpu.VMEM((tok_rows + HALO, 16), F32),
             pltpu.VMEM((8, depth), F32),
@@ -664,9 +702,9 @@
             pltpu.VMEM((3, pieces, 128, PIECE), BF16),
             pltpu.VMEM((pieces, 128, PIECE), BF16),
             pltpu.VMEM((2, pieces, 128, PIECE), BF16),
-            dma((chunks,)), dma((8,)), dma((8,)), dma((8,)),
-            dma((32,)), dma((32,)), dma((32,)), dma((32,)), dma((32,)), dma((32,)),
-            dma((n_x,)), dma((n_x,)), dma((n_z,)), dma((n_z,)),
+            dma((chunks,)), dma((11,)), dma((8,)), dma((8,)),
+            dma((32,)), dma((32,)), dma((32,)), dma((32,)), dma((32,)), dma((32,)), dma((32,)), dma((32,)),
+            dma((heads, n_x)), dma((heads, n_x)), dma((heads, n_z)), dma((heads, n_z)),
             dma((16,)), dma((16,)), dma((12,)), dma((12,)),
         ],
         compiler_params=pltpu.CompilerParams(

time: 134 us -> 132 us (0.985)
  Pallas kernels: 131 us -> 128 us
    pallas_call x1, Pallas kernels: 131 us -> 128 us  [per_device(): pl.pallas_call(lambda *refs: layer_kernel(heads, *refs), out_shape=jax.Sh...]
where the time goes in v5:
time: 132 us; the launch traced here: 130 us
  Pallas kernels  128 us (97%)
  local copies, waits for them, and re-layouts  2.29 us (2%)
    pallas_call x1, Pallas kernels, per_device(): pl.pallas_call(lambda *refs: layer_kernel(heads, *refs), out_shape=jax.Sh...  128 us

profile of v5, /device:TPU:1, one launch (start us, length us, event | category | flops | bytes accessed | tf_op | source)
XLA Modules:
  0.0 130.3 jit_solution(2635177224786827329)
XLA Ops:
  0.0 128.0 %layer.1 = bf16[128,4096]{1,0:T(8,128)(2,1)} custom-call(bf16[1024,4096]{1,0:T(8,128)(2,1)} %refs_0_.1, bf16[256,256]{1,0:T(8,128)(2,1)} %refs_1_.1, bf16[256,256]{1,0:T(8,128)(2,1)} %refs_2_.1, bf16[256,256]{1,0:T(8,128)(2,1)} %refs_3_.1, bf16[256,256]{1,0:T(8,128)(2,1)} %refs_4_.1, bf16[256,256]{1,0:T(8,128)(2,1)} %refs_5_.1, bf16[256,256]{1,0:T(8,128)(2,1)} %refs_6_.1, ...), custom_call_target="tpu_custom_call" | custom-call | tf_op jit(solution)/shard_map/layer/pallas_call | solution.py:668
  128.0 2.3 %copy.20 = bf16[128,4096]{1,0:T(8,128)(2,1)} copy(bf16[128,4096]{1,0:T(8,128)(2,1)} %layer.1) | data formatting | bytes 2097152

commit v6 on v5

--- a/solution.py
+++ b/solution.py
@@ -87,20 +87,24 @@
             w[1] = w[1] - dot(w[1], part).astype(BF16)
         events.get(("level", level), lambda: None)()
     solved = [dot(w[1], w[3]).astype(BF16) for w in work]
-    seen = [dot(w[2], s) for w, s in zip(work, solved)]
     moved = [dot_tn(w[4], s) for w, s in zip(work, solved)]
     current = map_ref[head]
+    starts = []
     for chunk in range(chunks):
-        where_rows = slice(chunk * CHUNK, chunk * CHUNK + CHUNK)
         current_b = current.astype(BF16)
-        asked = (work[chunk][5] - seen[chunk][:, 128:]).astype(BF16)
-        answer = dot(asked, current_b)
-        from_state_ref[head, where_rows, :] = answer[:, :128].astype(BF16)
-        local_ref[head, where_rows, :] = answer[:, 128:] + seen[chunk][:, :128]
+        starts.append(current_b)
         added = jnp.concatenate([jnp.zeros((128, 128), F32), moved[chunk][:, :128]], axis=1)
         current = (current * work[chunk][6] - dot(moved[chunk][:, 128:].astype(BF16), current_b)
                    + added)
     map_ref[head] = current
+    events.get(("maps", 0), lambda: None)()
+    seen = [dot(w[2], s) for w, s in zip(work, solved)]
+    for chunk in range(chunks):
+        where_rows = slice(chunk * CHUNK, chunk * CHUNK + CHUNK)
+        asked = (work[chunk][5] - seen[chunk][:, 128:]).astype(BF16)
+        answer = dot(asked, starts[chunk])
+        from_state_ref[head, where_rows, :] = answer[:, :128].astype(BF16)
+        local_ref[head, where_rows, :] = answer[:, 128:] + seen[chunk][:, :128]
 
 
 SPLIT_A = 128
@@ -110,11 +114,10 @@
 
 
 class PlaneGather:
-    def __init__(self, buf, split, send_sems, recv_sems):
+    def __init__(self, buf, split, send_sem, recv_sems):
         self.buf, self.split = buf, split
-        self.send_sems, self.recv_sems = send_sems, recv_sems
+        self.send_sem, self.recv_sems = send_sem, recv_sems
         self.z, self.x = lax.axis_index("sp_0"), lax.axis_index("sp_1")
-        self.copies = {}
 
     def shard(self, dz, dx):
         return lax.rem(self.z + dz + 4, 4) * 4 + lax.rem(self.x + dx + 4, 4)
@@ -126,89 +129,70 @@
         return {"a": (0, split), "b": (split, total), "a0": (0, quarter), "a1": (quarter, split),
                 "b0": (split, rest), "b1": (rest, total)}[part]
 
-    def region(self, dz, dx, part):
+    def send(self, group, source, part, way):
         low, high = self.rows(part)
-        return self.buf.at[self.shard(dz, dx), pl.ds(low, high - low), :]
-
-    def copy(self, name, way, source):
-        index, _, part = self.copies[name, way]
-        ref = self.region(source[0], source[1], part)
-        return remote(ref, ref, self.send_sems.at[index], self.recv_sems.at[index],
-                      {"sp_0": lax.rem(self.z + way[0] + 4, 4),
-                       "sp_1": lax.rem(self.x + way[1] + 4, 4)})
-
-    def send(self, name, source, part, way):
-        self.copies[name, way] = (len(self.copies), source, part)
-        self.copy(name, way, source).start()
-
-    def got(self, name, way):
-        source = self.copies[name, way][1]
-        self.copy(name, way, (source[0] - way[0], source[1] - way[1])).wait_recv()
-
-    def own(self, along="xz"):
-        for part in range(2):
+        ref = self.buf.at[self.shard(*source), pl.ds(low, high - low), :]
+        remote(ref, ref, self.send_sem, self.recv_sems.at[group],
+               {"sp_0": lax.rem(self.z + way[0] + 4, 4),
+                "sp_1": lax.rem(self.x + way[1] + 4, 4)}).start()
+
+    def got(self, group, blocks):
+        ref = self.buf.at[pl.ds(0, blocks)]
+        pltpu.make_async_copy(ref, ref, self.recv_sems.at[group]).wait()
+
+    def own(self, along="xz", parts=(0, 1)):
+        for part in parts:
             for step in (1, -1):
                 if "x" in along:
-                    self.send("ab"[part], (0, 0), "ab"[part], (0, step))
+                    self.send(part, (0, 0), "ab"[part], (0, step))
                 if "z" in along:
-                    self.send("ba"[part], (0, 0), "ba"[part], (step, 0))
+                    self.send(part, (0, 0), "ba"[part], (step, 0))
 
     def first(self):
-        for step in (1, -1):
-            self.got("a", (0, step))
-            self.got("b", (step, 0))
-        self.send("a2", (0, -1), "a0", (0, 1))
-        self.send("a2", (0, 1), "a1", (0, -1))
-        self.send("b2", (-1, 0), "b0", (1, 0))
-        self.send("b2", (1, 0), "b1", (-1, 0))
+        self.got(0, 2)
+        self.send(2, (0, -1), "a0", (0, 1))
+        self.send(2, (0, 1), "a1", (0, -1))
+        self.send(2, (-1, 0), "b0", (1, 0))
+        self.send(2, (1, 0), "b1", (-1, 0))
+        for side, group in ((1, 3), (-1, 4)):
+            for step in (1, -1):
+                self.send(group, (0, side * step), "a", (step, 0))
+                self.send(group, (side * step, 0), "b", (0, step))
+
+    def second(self):
+        self.got(1, 2)
+        self.send(6, (-1, 0), "a", (1, 0))
+        self.send(6, (0, -1), "b", (0, 1))
+
+    def third(self):
+        self.got(2, 1)
+        for step, group in ((-1, 5), (1, 7)):
+            self.send(group, (0, 2), "a", (step, 0))
+            self.send(group, (2, 0), "b", (0, step))
+
+    def fourth(self):
+        self.got(3, 2)
         for at in (1, -1):
-            for step in (1, -1):
-                self.send(("a3", at), (0, at), "a", (step, 0))
-                self.send(("b3", at), (at, 0), "b", (0, step))
-
-    def second(self):
-        for step in (1, -1):
-            self.got("b", (0, step))
-            self.got("a", (step, 0))
-        self.send(("a4", 0), (-1, 0), "a", (1, 0))
-        self.send(("b4", 0), (0, -1), "b", (0, 1))
-
-    def third(self, along="xz"):
-        for step in (1, -1):
-            self.got("a2", (0, step)) if "z" in along else None
-            self.got("b2", (step, 0)) if "x" in along else None
-        for step in (-1, 1):
-            if "z" in along:
-                self.send(("a3", 2), (0, 2), "a", (step, 0))
-            if "x" in along:
-                self.send(("b3", 2), (2, 0), "b", (0, step))
-
-    def fourth(self):
-        for at in (1, -1):
-            for step in (1, -1):
-                self.got(("a3", at), (step, 0))
-                self.got(("b3", at), (0, step))
-        for at in (1, -1):
-            self.send(("a4", at), (-at, at), "a", (at, 0))
-            self.send(("b4", at), (at, -at), "b", (0, at))
+            self.send(7, (-at, at), "a", (at, 0))
+            self.send(7, (at, -at), "b", (0, at))
+
+    def corners(self):
+        self.got(4, 2)
 
     def fifth(self):
-        for step in (1, -1):
-            self.got(("a3", 2), (step, 0))
-            self.got(("b3", 2), (0, step))
-        self.send(("a4", 2), (1, 2), "a", (-1, 0))
-        self.send(("b4", 2), (2, 1), "b", (0, -1))
-
-    def last(self, dz, dx):
-        side = {0: 1, 1: 1, -1: -1, 2: -1}
-        if dz == 2:
-            self.got(("a4", dx), (side[dx], 0))
-        if dx == 2:
-            self.got(("b4", dz), (0, side[dz]))
+        self.got(5, 1)
+        self.send(7, (1, 2), "a", (-1, 0))
+        self.send(7, (2, 1), "b", (0, -1))
+
+    def straight(self):
+        self.got(6, 1)
+
+    def last(self):
+        self.got(7, 4)
 
     def drain(self):
-        for (name, way), (_, source, _) in self.copies.items():
-            self.copy(name, way, source).wait_send()
+        ref = self.buf.at[pl.ds(0, 15)]
+        pltpu.make_async_copy(ref, ref, self.send_sem).wait()
 
 
 def after(later, earlier):
@@ -273,7 +257,7 @@
                  mixed_ref, part_ref, pair_out_ref, pair_in_ref, ring_out_ref, half_ref, final_ref,
                  tok_sems, load_sems, halo_send, halo_recv, send_a, recv_a, send_d, recv_d, send_b, recv_b,
                  send_c, recv_c, send_x, recv_x, send_z, recv_z, pair_send, pair_recv, ring_send,
-                 ring_recv):
+                 ring_recv, gate):
     z, x, tp = lax.axis_index("sp_0"), lax.axis_index("sp_1"), lax.axis_index("tp")
     n_z, n_x, n_tp = lax.axis_size("sp_0"), lax.axis_size("sp_1"), lax.axis_size("tp")
     y, core = tp // 2, lax.rem(tp, 2)
@@ -295,9 +279,10 @@
             (delta_out_hbm, out_w_ref.at[mine, pl.ds(256, 256), :]),
             (taps_hbm.at[:, :, pl.ds(pl.multiple_of(tp * 256, 256), 256)], taps_in_ref),
             (mix_hbm.at[pl.ds(tp * 2, 2)], mix_ref))):
-        load = pltpu.make_async_copy(hbm, ref, load_sems.at[k])
+        load = pltpu.make_async_copy(hbm, ref, load_sems.at[max(k - 2, 0)])
         load.start()
         loads.append(load)
+    own_block = wide_ref.at[mine, pl.ds(0, 256), :]
     tok_loads = []
     for k in range(chunks):
         load = pltpu.make_async_copy(
@@ -327,8 +312,7 @@
     for k in range(depth // 128):
         gain_ref[:, k * 128 : k * 128 + 128] = jnp.broadcast_to(gains[k : k + 1], (8, 128))
     fill_masks(masks_ref)
-    for load in loads[:3]:
-        load.wait()
+    pltpu.make_async_copy(own_block, own_block, load_sems.at[0]).wait()
     pl.semaphore_wait(barrier, len(peers))
 
     early = PlaneGather(wide_ref, SPLIT_A, send_a, recv_a)
@@ -339,25 +323,22 @@
 
     halos = [remote(
         tok_hbm.at[pl.ds(tok_rows - HALO, HALO), pl.ds(pl.multiple_of(tp * slices, 128), slices)],
-        halo_part(tp), halo_send.at[0], halo_recv.at[0], next_place)]
+        halo_part(tp), halo_send, halo_recv.at[0], next_place)]
     halos[0].start()
     early.own()
     for k in range(chunks):
         tok_loads[k].wait()
         norm_rows(tok_ref, gain_ref, HALO + k * CHUNK, CHUNK, 64)
-        if k == 1:
+        if k == 2:
             halos[0].wait_recv()
             for step in range(1, n_tp):
-                copy = remote(halo_part(tp), halo_part(tp), halo_send.at[step],
-                              halo_recv.at[step], device_at(tp=step))
-                copy.start()
-                halos.append(copy)
-    for step in range(1, n_tp):
-        owner = lax.rem(tp - step + n_tp, n_tp)
-        remote(halo_part(owner), halo_part(owner), halo_send.at[step], halo_recv.at[step],
-               device_at(tp=step)).wait_recv()
-    for copy in halos:
-        copy.wait_send()
+                remote(halo_part(tp), halo_part(tp), halo_send, halo_recv.at[1],
+                       device_at(tp=step)).start()
+    early.first()
+    others = tok_ref.at[pl.ds(0, HALO), pl.ds(0, depth - slices)]
+    pltpu.make_async_copy(others, others, halo_recv.at[1]).wait()
+    sent = tok_ref.at[pl.ds(0, HALO), :]
+    pltpu.make_async_copy(sent, sent, halo_send).wait()
 
     @pl.when(mine == 0)
     def _():
@@ -385,7 +366,12 @@
                 thin_ref[rows, :] = narrow
 
     first_acc, second_acc = acc_ref.at[0], acc_ref.at[1]
-    early.first()
+    partner = {"tp": y * 2 + (1 - core)}
+
+    def meet():
+        pl.semaphore_signal(gate, 1, device_id=partner, device_id_type=MESH_ID)
+        pl.semaphore_wait(gate, 1)
+
     project(early, ORDER[:1], first_acc, first=True)
     early.second()
     project(early, ORDER[1:5], first_acc)
@@ -393,18 +379,17 @@
     for load in loads[3:]:
         load.wait()
     early.fourth()
-    later = PlaneGather(next_ref, SPLIT_A, send_d, recv_d)
-    later.own()
+    early.corners()
     project(early, ORDER[5:9], first_acc)
     early.fifth()
-    for dz, dx in ORDER[9:13]:
-        early.last(dz, dx)
-    project(early, ORDER[9:13], first_acc)
+    later = PlaneGather(next_ref, SPLIT_A, send_d, recv_d)
+    meet()
+    later.own()
+    early.straight()
+    project(early, ORDER[9:11], first_acc)
+    early.last()
+    project(early, ORDER[11:], first_acc)
     later.first()
-    for dz, dx in ORDER[13:]:
-        early.last(dz, dx)
-    project(early, ORDER[13:], first_acc)
-    later.second()
 
     taps_ref[...] = taps_in_ref[...].astype(F32)
     narrow = thin_ref[HALO:, :].T
@@ -445,14 +430,14 @@
         own_ref[head] = map_ref[head].astype(BF16)
         row_ref[0, head] = own_ref[head]
         along_x[head] = [
-            remote(own_ref.at[head], row_ref.at[step, head], send_x.at[head, step],
-                   recv_x.at[head, step], device_at(x=step)) for step in range(1, n_x)]
+            remote(own_ref.at[head], row_ref.at[step, head], send_x.at[head], recv_x.at[head],
+                   device_at(x=step)) for step in range(1, n_x)]
         for copy in along_x[head]:
             copy.start()
 
     def send_z_maps(head):
-        for copy in along_x[head]:
-            copy.wait_recv()
+        moved = row_ref.at[pl.ds(1, n_x - 1), head]
+        pltpu.make_async_copy(moved, moved, recv_x.at[head]).wait()
         so_far = before_here = identity
         for k in range(n_x):
             piece = row_ref[lax.rem(x - k + n_x, n_x), head]
@@ -462,14 +447,14 @@
         total_ref[head] = so_far.astype(BF16)
         column_ref[0, head] = total_ref[head]
         along_z[head] = [
-            remote(total_ref.at[head], column_ref.at[step, head], send_z.at[head, step],
-                   recv_z.at[head, step], device_at(z=step)) for step in range(1, n_z)]
+            remote(total_ref.at[head], column_ref.at[step, head], send_z.at[head],
+                   recv_z.at[head], device_at(z=step)) for step in range(1, n_z)]
         for copy in along_z[head]:
             copy.start()
 
     def enter(head):
-        for copy in along_z[head]:
-            copy.wait_recv()
+        moved = column_ref.at[pl.ds(1, n_z - 1), head]
+        pltpu.make_async_copy(moved, moved, recv_z.at[head]).wait()
         so_far = state = jnp.zeros((128, 128), F32)
         for k in range(n_z - 1):
             piece = column_ref[lax.rem(z - k + n_z, n_z), head]
@@ -479,29 +464,24 @@
         entering = dot(map_ref[head, :, 0:128].astype(BF16), state.astype(BF16))
         state_ref[head] = (entering + map_ref[head, :, 128:256]).astype(BF16)
 
+    later.second()
     delta(0, {("chunk", 3): later.third, ("level", 3): later.fourth})
+    project(later, ORDER[:5], second_acc, first=True)
     later.fifth()
+    send_x_maps(0)
+    meet()
     pool.own()
-    send_x_maps(0)
-    project(later, ORDER[:5], second_acc, first=True)
+    later.corners()
     project(later, ORDER[5:9], second_acc)
-    for places in (ORDER[9:13], ORDER[13:]):
-        for dz, dx in places:
-            later.last(dz, dx)
-        project(later, places, second_acc)
-
-    def pool_early():
-        pool.first()
-        pool.second()
-
-    def pool_middle():
-        pool.third()
-        pool.fourth()
-
-    pool_early()
-    delta(1, {("chunk", 1): lambda: send_z_maps(0), ("chunk", 3): pool_middle,
-              ("level", 4): pool.fifth})
-    send_x_maps(1)
+    later.straight()
+    later.last()
+    project(later, ORDER[9:], second_acc)
+    pool.first()
+    pool.second()
+    delta(1, {("chunk", 0): lambda: send_z_maps(0), ("chunk", 3): pool.third,
+              ("level", 4): pool.fourth, ("maps", 0): lambda: send_x_maps(1)})
+    pool.fifth()
+    meet()
     out.own("x")
     enter(0)
     wide = core == 1
@@ -515,13 +495,13 @@
             mixed_ref[chunk, pl.ds(pl.multiple_of(slot * 128, 128), 128), lanes] = (
                 values[half * 128 : half * 128 + 128])
 
-    project(pool, ORDER[:8], pool_ref, first=True)
+    pool.corners()
+    project(pool, ORDER[:9], pool_ref, first=True)
     send_z_maps(1)
     out.own("z")
-    for dz, dx in ORDER[9:]:
-        pool.last(dz, dx)
-    project(pool, ORDER[8:], pool_ref)
-    out.first()
+    pool.straight()
+    pool.last()
+    project(pool, ORDER[9:], pool_ref)
 
     @pl.loop(0, chunks)
     def _(chunk):
@@ -530,11 +510,9 @@
             store_halves(chunk, slice(group * 128, group * 128 + 128), values)
 
     enter(1)
-    out.second()
 
     head_gain = head_gain_ref[...].astype(F32)
-    partner = {"tp": y * 2 + (1 - core)}
-    pairs, rings, finals, halves = {}, [], {}, {}
+    pairs = {}
     slots = {2: 0, 1: 1, 3: 2, 0: 0}
 
     def finish_rows(ahead):
@@ -554,9 +532,9 @@
             product = dot(mixed_ref[chunk], out_w_ref[out.shard(dz, dx)])
             part_ref[slots[ahead], piece, :, lanes] = product[:128]
             pair_out_ref[ahead, piece, :, lanes] = product[128:].astype(BF16)
-        index = ahead * 4 + piece
+        index = ahead * 4 + piece if ahead else 0
         copy = remote(pair_out_ref.at[ahead, piece], pair_in_ref.at[ahead, piece],
-                      pair_send.at[index], pair_recv.at[index], partner)
+                      pair_send, pair_recv.at[index], partner)
         copy.start()
         pairs[ahead, piece] = copy
 
@@ -564,90 +542,84 @@
         pairs[ahead, piece].wait_recv()
         return part_ref[slots[ahead], piece] + pair_in_ref[ahead, piece].astype(F32)
 
-    def pass_on(ahead, piece, place, target, merge=False):
-        value = chip_sum(ahead, piece)
-        if merge:
-            halves[piece].wait_recv()
-            value = value + half_ref[piece].astype(F32)
-        ring_out_ref[ahead - 1, piece] = value.astype(BF16)
-        index = len(rings)
-        copy = remote(ring_out_ref.at[ahead - 1, piece], target, ring_send.at[index],
-                      ring_recv.at[index], place)
+    up, down = device_at(tp=2), device_at(tp=-2)
+    half = 64
+    top, bottom = slice(0, half), slice(half, 2 * half)
+
+    def pass_on(group, ahead, piece, rows, value, place, target):
+        ring_out_ref[ahead - 1, piece, rows, :] = value.astype(BF16)
+        where_rows = pl.ds(rows.start, half)
+        copy = remote(ring_out_ref.at[ahead - 1, piece, where_rows],
+                      target.at[piece, where_rows], ring_send, ring_recv.at[group], place)
         copy.start()
-        rings.append(copy)
-        return copy
-
-    up, down = device_at(tp=2), device_at(tp=-2)
 
     def far(piece):
-        halves[piece] = pass_on(2, piece, down if piece % 2 else up, half_ref.at[piece])
-
-    def near(ahead, piece, merge=False):
-        side = 0 if ahead == 1 else 1
-        finals[side, piece] = pass_on(ahead, piece, down if side else up,
-                                      final_ref.at[side, piece], merge)
+        value = chip_sum(2, piece)
+        pass_on(piece, 2, piece, top, value[top], up, half_ref)
+        pass_on(piece, 2, piece, bottom, value[bottom], down, half_ref)
+
+    def near(piece):
+        for ahead, rows, place, side in ((1, bottom, up, 0), (3, top, down, 1)):
+            value = chip_sum(ahead, piece)
+            part_ref[slots[ahead], piece] = value
+            pass_on(4 + piece, ahead, piece, rows, value[rows], place, final_ref.at[side])
+
+    def merged(piece):
+        pltpu.make_async_copy(half_ref.at[piece], half_ref.at[piece], ring_recv.at[piece]).wait()
+        for ahead, rows, place, side in ((1, top, up, 0), (3, bottom, down, 1)):
+            value = part_ref[slots[ahead], piece, rows, :] + half_ref[piece, rows, :].astype(F32)
+            pass_on(4 + piece, ahead, piece, rows, value, place, final_ref.at[side])
+
+    def send_piece(piece):
+        produce(2, piece)
+        produce(1, piece)
+        produce(3, piece)
+        far(piece)
+        near(piece)
 
     finish_rows(2)
-    produce(2, 0)
-    far(0)
-    out.third()
     finish_rows(1)
     finish_rows(3)
+    out.first()
+    out.second()
+    send_piece(0)
+    finish_rows(0)
+    out.third()
+    merged(0)
     out.fourth()
-    produce(2, 1)
-    far(1)
-    produce(1, 1)
-    produce(3, 0)
-    near(1, 1)
-    near(3, 0)
+    out.corners()
+    send_piece(1)
     out.fifth()
-    produce(1, 0)
-    produce(3, 1)
-    early.drain()
-    later.drain()
-    near(1, 0, merge=True)
-    near(3, 1, merge=True)
-    for dz, dx in ORDER[9:]:
-        out.last(dz, dx)
-    for piece in (2, 3):
-        produce(2, piece)
-        far(piece)
-    produce(1, 3)
-    near(1, 3)
-    produce(3, 2)
-    near(3, 2)
-    produce(1, 2)
-    produce(3, 3)
-    finish_rows(0)
+    for piece in range(2):
+        produce(0, piece)
+    merged(1)
+    out.straight()
+    out.last()
+    send_piece(2)
+    merged(2)
+    send_piece(3)
+    for piece in range(2, 4):
+        produce(0, piece)
+    for gather in (early, later, pool, out):
+        gather.drain()
+    for head in range(heads):
+        for ref, sem in ((row_ref, send_x), (column_ref, send_z)):
+            moved = ref.at[pl.ds(1, n_x - 1), head]
+            pltpu.make_async_copy(moved, moved, sem.at[head]).wait()
+    merged(3)
+    pltpu.make_async_copy(pair_in_ref.at[0], pair_in_ref.at[0], pair_recv.at[0]).wait()
     for piece in range(4):
-        produce(0, piece)
-    pool.drain()
-    out.drain()
-    near(1, 2, merge=True)
-    near(3, 3, merge=True)
+        part_ref[0, piece] = part_ref[0, piece] + pair_in_ref[0, piece].astype(F32)
+    pltpu.make_async_copy(pair_out_ref, pair_out_ref, pair_send).wait()
     for piece in range(4):
-        part_ref[0, piece] = chip_sum(0, piece)
-    for head in range(heads):
-        for copy in along_x[head] + along_z[head]:
-            copy.wait_send()
-    for copy in pairs.values():
-        copy.wait_send()
-    for copy in rings[:8]:
-        copy.wait_send()
-    arrived = set()
-    for key in ((0, 1), (1, 0), (0, 0), (1, 1), (0, 3), (1, 2), (0, 2), (1, 3)):
-        side, piece = key
-        finals[key].wait_recv()
-        value = part_ref[0, piece] + final_ref[side, piece].astype(F32)
-        if (1 - side, piece) not in arrived:
-            part_ref[0, piece] = value
-        else:
-            for block, (dz, dx) in enumerate(ORDER[4 * piece : 4 * piece + 4]):
-                lanes = pl.ds(pl.multiple_of(out.shard(dz, dx) * 256, 256), 256)
-                out_ref[:, lanes] = value[:, block * 256 : block * 256 + 256].astype(BF16)
-        arrived.add(key)
-    for copy in rings[8:]:
-        copy.wait_send()
+        arrived = final_ref.at[:, piece]
+        pltpu.make_async_copy(arrived, arrived, ring_recv.at[4 + piece]).wait()
+        value = part_ref[0, piece] + final_ref[0, piece].astype(F32)
+        value = value + final_ref[1, piece].astype(F32)
+        for block, (dz, dx) in enumerate(ORDER[4 * piece : 4 * piece + 4]):
+            lanes = pl.ds(pl.multiple_of(out.shard(dz, dx) * 256, 256), 256)
+            out_ref[:, lanes] = value[:, block * 256 : block * 256 + 256].astype(BF16)
+    pltpu.make_async_copy(ring_out_ref, ring_out_ref, ring_send).wait()
 
 
 def per_device(tokens, input_norm_scale, mean_input_weight, query_matrix, key_matrix, value_matrix,
@@ -702,10 +674,11 @@
             pltpu.VMEM((3, pieces, 128, PIECE), BF16),
             pltpu.VMEM((pieces, 128, PIECE), BF16),
             pltpu.VMEM((2, pieces, 128, PIECE), BF16),
-            dma((chunks,)), dma((11,)), dma((8,)), dma((8,)),
-            dma((32,)), dma((32,)), dma((32,)), dma((32,)), dma((32,)), dma((32,)), dma((32,)), dma((32,)),
-            dma((heads, n_x)), dma((heads, n_x)), dma((heads, n_z)), dma((heads, n_z)),
-            dma((16,)), dma((16,)), dma((12,)), dma((12,)),
+            dma((chunks,)), dma((9,)), dma(()), dma((2,)),
+            dma(()), dma((8,)), dma(()), dma((8,)), dma(()), dma((8,)), dma(()), dma((8,)),
+            dma((heads,)), dma((heads,)), dma((heads,)), dma((heads,)),
+            dma(()), dma((16,)), dma(()), dma((8,)),
+            pltpu.SemaphoreType.REGULAR,
         ],
         compiler_params=pltpu.CompilerParams(
             vmem_limit_bytes=VMEM_LIMIT, collective_id=0, has_side_effects=True),

time: 132 us -> 121 us (0.917)
  Pallas kernels: 128 us -> 118 us
    pallas_call x1, Pallas kernels: 128 us -> 118 us  [per_device(): pl.pallas_call(lambda *refs: layer_kernel(heads, *refs), out_shape=jax.Sh...]
where the time goes in v6:
time: 121 us; the launch traced here: 120 us
  Pallas kernels  118 us (98%)
  local copies, waits for them, and re-layouts  2.29 us (2%)
    pallas_call x1, Pallas kernels, per_device(): pl.pallas_call(lambda *refs: layer_kernel(heads, *refs), out_shape=jax.Sh...  118 us

profile of v6, /device:TPU:1, one launch (start us, length us, event | category | flops | bytes accessed | tf_op | source)
XLA Modules:
  0.0 120.4 jit_solution(1577110325741096615)
XLA Ops:
  0.0 118.1 %layer.1 = bf16[128,4096]{1,0:T(8,128)(2,1)} custom-call(bf16[1024,4096]{1,0:T(8,128)(2,1)} %refs_0_.1, bf16[256,256]{1,0:T(8,128)(2,1)} %refs_1_.1, bf16[256,256]{1,0:T(8,128)(2,1)} %refs_2_.1, bf16[256,256]{1,0:T(8,128)(2,1)} %refs_3_.1, bf16[256,256]{1,0:T(8,128)(2,1)} %refs_4_.1, bf16[256,256]{1,0:T(8,128)(2,1)} %refs_5_.1, bf16[256,256]{1,0:T(8,128)(2,1)} %refs_6_.1, ...), custom_call_target="tpu_custom_call" | custom-call | tf_op jit(solution)/shard_map/layer/pallas_call | solution.py:640
  118.1 2.3 %copy.20 = bf16[128,4096]{1,0:T(8,128)(2,1)} copy(bf16[128,4096]{1,0:T(8,128)(2,1)} %layer.1) | data formatting | bytes 2097152

commit v7 on v6

--- a/solution.py
+++ b/solution.py
@@ -108,7 +108,7 @@
 
 
 SPLIT_A = 128
-PIECE = 1024
+PIECE = 512
 ORDER = ((0, 0), (0, 1), (0, -1), (1, 0), (-1, 0), (1, 1), (1, -1), (-1, 1), (-1, -1), (0, 2), (2, 0),
          (1, 2), (-1, 2), (2, 1), (2, -1), (2, 2))
 
@@ -136,9 +136,16 @@
                {"sp_0": lax.rem(self.z + way[0] + 4, 4),
                 "sp_1": lax.rem(self.x + way[1] + 4, 4)}).start()
 
-    def got(self, group, blocks):
+    def got(self, group, blocks, part=None):
         ref = self.buf.at[pl.ds(0, blocks)]
+        if part is not None:
+            low, high = self.rows(part)
+            ref = self.buf.at[pl.ds(0, blocks), pl.ds(low, high - low), :]
         pltpu.make_async_copy(ref, ref, self.recv_sems.at[group]).wait()
+
+    def got_own(self, along, part):
+        name = "ab"[part] if along == "x" else "ba"[part]
+        self.got(part if along == "x" else 8 + part, 2, name)
 
     def own(self, along="xz", parts=(0, 1)):
         for part in parts:
@@ -146,49 +153,58 @@
                 if "x" in along:
                     self.send(part, (0, 0), "ab"[part], (0, step))
                 if "z" in along:
-                    self.send(part, (0, 0), "ba"[part], (step, 0))
-
-    def first(self):
-        self.got(0, 2)
+                    self.send(8 + part, (0, 0), "ba"[part], (step, 0))
+
+    def quarters(self):
         self.send(2, (0, -1), "a0", (0, 1))
         self.send(2, (0, 1), "a1", (0, -1))
         self.send(2, (-1, 0), "b0", (1, 0))
         self.send(2, (1, 0), "b1", (-1, 0))
+
+    def first(self, waits="xz", quarters_last=False):
+        for along in waits:
+            self.got_own(along, 0)
+        if not quarters_last:
+            self.quarters()
         for side, group in ((1, 3), (-1, 4)):
             for step in (1, -1):
                 self.send(group, (0, side * step), "a", (step, 0))
                 self.send(group, (side * step, 0), "b", (0, step))
-
-    def second(self):
-        self.got(1, 2)
+        if quarters_last:
+            self.quarters()
+
+    def second(self, waits="xz"):
+        for along in waits:
+            self.got_own(along, 1)
         self.send(6, (-1, 0), "a", (1, 0))
         self.send(6, (0, -1), "b", (0, 1))
 
     def third(self):
         self.got(2, 1)
-        for step, group in ((-1, 5), (1, 7)):
+        for step, group in ((-1, 5), (1, 10)):
             self.send(group, (0, 2), "a", (step, 0))
             self.send(group, (2, 0), "b", (0, step))
 
     def fourth(self):
         self.got(3, 2)
-        for at in (1, -1):
-            self.send(7, (-at, at), "a", (at, 0))
-            self.send(7, (at, -at), "b", (0, at))
+        for at, group in ((1, 7), (-1, 10)):
+            self.send(group, (-at, at), "a", (at, 0))
+            self.send(group, (at, -at), "b", (0, at))
 
     def corners(self):
         self.got(4, 2)
 
     def fifth(self):
         self.got(5, 1)
-        self.send(7, (1, 2), "a", (-1, 0))
-        self.send(7, (2, 1), "b", (0, -1))
+        self.send(11, (1, 2), "a", (-1, 0))
+        self.send(11, (2, 1), "b", (0, -1))
 
     def straight(self):
         self.got(6, 1)
 
-    def last(self):
-        self.got(7, 4)
+    def last(self, stages=(0, 1, 2)):
+        for stage in stages:
+            self.got((7, 10, 11)[stage], (1, 2, 1)[stage])
 
     def drain(self):
         ref = self.buf.at[pl.ds(0, 15)]
@@ -308,10 +324,6 @@
         thin = jnp.where(at == k, jnp.broadcast_to(row_values, (16, 256)), thin)
     wide_ref[mine, 256:272, 0:256] = thin.astype(BF16)
     wide_ref[mine, 256:272, 256:384] = jnp.zeros((16, 128), BF16)
-    gains = gain_in_ref[...].astype(F32)
-    for k in range(depth // 128):
-        gain_ref[:, k * 128 : k * 128 + 128] = jnp.broadcast_to(gains[k : k + 1], (8, 128))
-    fill_masks(masks_ref)
     pltpu.make_async_copy(own_block, own_block, load_sems.at[0]).wait()
     pl.semaphore_wait(barrier, len(peers))
 
@@ -326,15 +338,18 @@
         halo_part(tp), halo_send, halo_recv.at[0], next_place)]
     halos[0].start()
     early.own()
+    gains = gain_in_ref[...].astype(F32)
+    for k in range(depth // 128):
+        gain_ref[:, k * 128 : k * 128 + 128] = jnp.broadcast_to(gains[k : k + 1], (8, 128))
     for k in range(chunks):
         tok_loads[k].wait()
         norm_rows(tok_ref, gain_ref, HALO + k * CHUNK, CHUNK, 64)
-        if k == 2:
-            halos[0].wait_recv()
-            for step in range(1, n_tp):
-                remote(halo_part(tp), halo_part(tp), halo_send, halo_recv.at[1],
-                       device_at(tp=step)).start()
     early.first()
+    halos[0].wait_recv()
+    for step in range(1, n_tp):
+        remote(halo_part(tp), halo_part(tp), halo_send, halo_recv.at[1],
+               device_at(tp=step)).start()
+    early.second()
     others = tok_ref.at[pl.ds(0, HALO), pl.ds(0, depth - slices)]
     pltpu.make_async_copy(others, others, halo_recv.at[1]).wait()
     sent = tok_ref.at[pl.ds(0, HALO), :]
@@ -345,6 +360,7 @@
         tok_ref[0:HALO, :] = jnp.zeros((HALO, depth), BF16)
 
     norm_rows(tok_ref, gain_ref, 0, HALO, HALO)
+    fill_masks(masks_ref)
     tile = 208
 
     def project(gather, places, into, first=False):
@@ -373,23 +389,23 @@
         pl.semaphore_wait(gate, 1)
 
     project(early, ORDER[:1], first_acc, first=True)
-    early.second()
-    project(early, ORDER[1:5], first_acc)
     early.third()
     for load in loads[3:]:
         load.wait()
     early.fourth()
+    project(early, ORDER[1:5], first_acc)
     early.corners()
-    project(early, ORDER[5:9], first_acc)
     early.fifth()
     later = PlaneGather(next_ref, SPLIT_A, send_d, recv_d)
     meet()
     later.own()
+    project(early, ORDER[5:9], first_acc)
     early.straight()
     project(early, ORDER[9:11], first_acc)
     early.last()
+    later.first()
     project(early, ORDER[11:], first_acc)
-    later.first()
+    later.second()
 
     taps_ref[...] = taps_in_ref[...].astype(F32)
     narrow = thin_ref[HALO:, :].T
@@ -464,26 +480,31 @@
         entering = dot(map_ref[head, :, 0:128].astype(BF16), state.astype(BF16))
         state_ref[head] = (entering + map_ref[head, :, 128:256]).astype(BF16)
 
-    later.second()
-    delta(0, {("chunk", 3): later.third, ("level", 3): later.fourth})
-    project(later, ORDER[:5], second_acc, first=True)
+    delta(0, {("chunk", 2): later.third, ("level", 2): later.fourth})
     later.fifth()
     send_x_maps(0)
     meet()
     pool.own()
+    project(later, ORDER[:5], second_acc, first=True)
     later.corners()
     project(later, ORDER[5:9], second_acc)
     later.straight()
+    project(later, ORDER[9:11], second_acc)
     later.last()
-    project(later, ORDER[9:], second_acc)
-    pool.first()
-    pool.second()
-    delta(1, {("chunk", 0): lambda: send_z_maps(0), ("chunk", 3): pool.third,
-              ("level", 4): pool.fourth, ("maps", 0): lambda: send_x_maps(1)})
+    project(later, ORDER[11:], second_acc)
+    delta(1, {("chunk", 0): lambda: send_z_maps(0), ("chunk", 2): pool.first,
+              ("level", 2): pool.second, ("maps", 0): lambda: send_x_maps(1)})
+    pool.third()
+    project(pool, ORDER[:5], pool_ref, first=True)
+    pool.fourth()
+    enter(0)
+    pool.corners()
+    project(pool, ORDER[5:9], pool_ref)
     pool.fifth()
     meet()
     out.own("x")
-    enter(0)
+    send_z_maps(1)
+    out.own("z")
     wide = core == 1
     scales_at = lax.broadcasted_iota(jnp.int32, scale_in_ref.shape, 0)
     scales = [jnp.sum(jnp.where(scales_at == tp * 2 + group, scale_in_ref[...].astype(F32), 0.0),
@@ -495,10 +516,6 @@
             mixed_ref[chunk, pl.ds(pl.multiple_of(slot * 128, 128), 128), lanes] = (
                 values[half * 128 : half * 128 + 128])
 
-    pool.corners()
-    project(pool, ORDER[:9], pool_ref, first=True)
-    send_z_maps(1)
-    out.own("z")
     pool.straight()
     pool.last()
     project(pool, ORDER[9:], pool_ref)
@@ -527,12 +544,12 @@
 
     def produce(ahead, piece):
         chunk = lax.rem(y + ahead, n_y)
-        for block, (dz, dx) in enumerate(ORDER[4 * piece : 4 * piece + 4]):
+        for block, (dz, dx) in enumerate(ORDER[2 * piece : 2 * piece + 2]):
             lanes = slice(block * 256, block * 256 + 256)
             product = dot(mixed_ref[chunk], out_w_ref[out.shard(dz, dx)])
             part_ref[slots[ahead], piece, :, lanes] = product[:128]
             pair_out_ref[ahead, piece, :, lanes] = product[128:].astype(BF16)
-        index = ahead * 4 + piece if ahead else 0
+        index = ahead * 8 + piece if ahead else 0
         copy = remote(pair_out_ref.at[ahead, piece], pair_in_ref.at[ahead, piece],
                       pair_send, pair_recv.at[index], partner)
         copy.start()
@@ -562,13 +579,13 @@
         for ahead, rows, place, side in ((1, bottom, up, 0), (3, top, down, 1)):
             value = chip_sum(ahead, piece)
             part_ref[slots[ahead], piece] = value
-            pass_on(4 + piece, ahead, piece, rows, value[rows], place, final_ref.at[side])
+            pass_on(8 + piece, ahead, piece, rows, value[rows], place, final_ref.at[side])
 
     def merged(piece):
         pltpu.make_async_copy(half_ref.at[piece], half_ref.at[piece], ring_recv.at[piece]).wait()
         for ahead, rows, place, side in ((1, top, up, 0), (3, bottom, down, 1)):
             value = part_ref[slots[ahead], piece, rows, :] + half_ref[piece, rows, :].astype(F32)
-            pass_on(4 + piece, ahead, piece, rows, value, place, final_ref.at[side])
+            pass_on(8 + piece, ahead, piece, rows, value, place, final_ref.at[side])
 
     def send_piece(piece):
         produce(2, piece)
@@ -580,25 +597,46 @@
     finish_rows(2)
     finish_rows(1)
     finish_rows(3)
-    out.first()
-    out.second()
+    out.first(quarters_last=True)
+    out.got_own("x", 1)
     send_piece(0)
+    out.second(waits="z")
+    send_piece(1)
     finish_rows(0)
-    out.third()
     merged(0)
     out.fourth()
     out.corners()
-    send_piece(1)
+    send_piece(2)
+    out.third()
+    merged(1)
+    send_piece(3)
     out.fifth()
-    for piece in range(2):
+    for piece in range(4):
         produce(0, piece)
-    merged(1)
+    merged(2)
     out.straight()
-    out.last()
-    send_piece(2)
-    merged(2)
-    send_piece(3)
-    for piece in range(2, 4):
+    send_piece(4)
+    merged(3)
+    out.last((0,))
+    produce(2, 5)
+    far(5)
+    merged(4)
+    out.last((1,))
+    produce(2, 6)
+    far(6)
+    produce(1, 5)
+    produce(3, 5)
+    near(5)
+    merged(5)
+    out.last((2,))
+    produce(2, 7)
+    far(7)
+    for piece in (6, 7):
+        produce(1, piece)
+        produce(3, piece)
+        near(piece)
+        merged(piece)
+    for piece in range(4, 8):
         produce(0, piece)
     for gather in (early, later, pool, out):
         gather.drain()
@@ -606,17 +644,16 @@
         for ref, sem in ((row_ref, send_x), (column_ref, send_z)):
             moved = ref.at[pl.ds(1, n_x - 1), head]
             pltpu.make_async_copy(moved, moved, sem.at[head]).wait()
-    merged(3)
     pltpu.make_async_copy(pair_in_ref.at[0], pair_in_ref.at[0], pair_recv.at[0]).wait()
-    for piece in range(4):
+    for piece in range(8):
         part_ref[0, piece] = part_ref[0, piece] + pair_in_ref[0, piece].astype(F32)
     pltpu.make_async_copy(pair_out_ref, pair_out_ref, pair_send).wait()
-    for piece in range(4):
+    for piece in range(8):
         arrived = final_ref.at[:, piece]
-        pltpu.make_async_copy(arrived, arrived, ring_recv.at[4 + piece]).wait()
+        pltpu.make_async_copy(arrived, arrived, ring_recv.at[8 + piece]).wait()
         value = part_ref[0, piece] + final_ref[0, piece].astype(F32)
         value = value + final_ref[1, piece].astype(F32)
-        for block, (dz, dx) in enumerate(ORDER[4 * piece : 4 * piece + 4]):
+        for block, (dz, dx) in enumerate(ORDER[2 * piece : 2 * piece + 2]):
             lanes = pl.ds(pl.multiple_of(out.shard(dz, dx) * 256, 256), 256)
             out_ref[:, lanes] = value[:, block * 256 : block * 256 + 256].astype(BF16)
     pltpu.make_async_copy(ring_out_ref, ring_out_ref, ring_send).wait()
@@ -675,9 +712,9 @@
             pltpu.VMEM((pieces, 128, PIECE), BF16),
             pltpu.VMEM((2, pieces, 128, PIECE), BF16),
             dma((chunks,)), dma((9,)), dma(()), dma((2,)),
-            dma(()), dma((8,)), dma(()), dma((8,)), dma(()), dma((8,)), dma(()), dma((8,)),
+            dma(()), dma((12,)), dma(()), dma((12,)), dma(()), dma((12,)), dma(()), dma((12,)),
             dma((heads,)), dma((heads,)), dma((heads,)), dma((heads,)),
-            dma(()), dma((16,)), dma(()), dma((8,)),
+            dma(()), dma((32,)), dma(()), dma((16,)),
             pltpu.SemaphoreType.REGULAR,
         ],
         compiler_params=pltpu.CompilerParams(

time: 121 us -> 117 us (0.967)
  Pallas kernels: 118 us -> 115 us
    pallas_call x1, Pallas kernels: 118 us -> 115 us  [per_device(): pl.pallas_call(lambda *refs: layer_kernel(heads, *refs), out_shape=jax.Sh...]
where the time goes in v7:
time: 117 us
  Pallas kernels  115 us (98%)
  local copies, waits for them, and re-layouts  2.29 us (2%)
    pallas_call x1, Pallas kernels, per_device(): pl.pallas_call(lambda *refs: layer_kernel(heads, *refs), out_shape=jax.Sh...  115 us

profile of v7, /device:TPU:1, one launch (start us, length us, event | category | flops | bytes accessed | tf_op | source)
XLA Modules:
  0.0 116.9 jit_solution(9376229463116838643)
XLA Ops:
  0.0 114.6 %layer.1 = bf16[128,4096]{1,0:T(8,128)(2,1)} custom-call(bf16[1024,4096]{1,0:T(8,128)(2,1)} %refs_0_.1, bf16[256,256]{1,0:T(8,128)(2,1)} %refs_1_.1, bf16[256,256]{1,0:T(8,128)(2,1)} %refs_2_.1, bf16[256,256]{1,0:T(8,128)(2,1)} %refs_3_.1, bf16[256,256]{1,0:T(8,128)(2,1)} %refs_4_.1, bf16[256,256]{1,0:T(8,128)(2,1)} %refs_5_.1, bf16[256,256]{1,0:T(8,128)(2,1)} %refs_6_.1, ...), custom_call_target="tpu_custom_call" | custom-call | tf_op jit(solution)/shard_map/layer/pallas_call | solution.py:677
  114.6 2.3 %copy.20 = bf16[128,4096]{1,0:T(8,128)(2,1)} copy(bf16[128,4096]{1,0:T(8,128)(2,1)} %layer.1) | data formatting | bytes 2097152

commit v8 on v7

--- a/solution.py
+++ b/solution.py
@@ -492,8 +492,9 @@
     project(later, ORDER[9:11], second_acc)
     later.last()
     project(later, ORDER[11:], second_acc)
-    delta(1, {("chunk", 0): lambda: send_z_maps(0), ("chunk", 2): pool.first,
-              ("level", 2): pool.second, ("maps", 0): lambda: send_x_maps(1)})
+    delta(1, {("chunk", 2): pool.first, ("chunk", 3): lambda: send_z_maps(0),
+              ("maps", 0): lambda: send_x_maps(1)})
+    pool.second()
     pool.third()
     project(pool, ORDER[:5], pool_ref, first=True)
     pool.fourth()
@@ -595,11 +596,15 @@
         near(piece)
 
     finish_rows(2)
+    out.first(quarters_last=True)
+    out.got_own("x", 1)
+    produce(2, 0)
     finish_rows(1)
     finish_rows(3)
-    out.first(quarters_last=True)
-    out.got_own("x", 1)
-    send_piece(0)
+    produce(1, 0)
+    far(0)
+    produce(3, 0)
+    near(0)
     out.second(waits="z")
     send_piece(1)
     finish_rows(0)

time: 117 us -> 117 us (level)
  no operation moved by 1% of the time
where the time goes in v8:
time: 117 us
  Pallas kernels  115 us (98%)
  local copies, waits for them, and re-layouts  2.29 us (2%)
    pallas_call x1, Pallas kernels, per_device(): pl.pallas_call(lambda *refs: layer_kernel(heads, *refs), out_shape=jax.Sh...  115 us

profile of v8, /device:TPU:1, one launch (start us, length us, event | category | flops | bytes accessed | tf_op | source)
XLA Modules:
  0.0 116.8 jit_solution(10818570154275725226)
XLA Ops:
  0.0 114.5 %layer.1 = bf16[128,4096]{1,0:T(8,128)(2,1)} custom-call(bf16[1024,4096]{1,0:T(8,128)(2,1)} %refs_0_.1, bf16[256,256]{1,0:T(8,128)(2,1)} %refs_1_.1, bf16[256,256]{1,0:T(8,128)(2,1)} %refs_2_.1, bf16[256,256]{1,0:T(8,128)(2,1)} %refs_3_.1, bf16[256,256]{1,0:T(8,128)(2,1)} %refs_4_.1, bf16[256,256]{1,0:T(8,128)(2,1)} %refs_5_.1, bf16[256,256]{1,0:T(8,128)(2,1)} %refs_6_.1, ...), custom_call_target="tpu_custom_call" | custom-call | tf_op jit(solution)/shard_map/layer/pallas_call | solution.py:682
  114.5 2.3 %copy.20 = bf16[128,4096]{1,0:T(8,128)(2,1)} copy(bf16[128,4096]{1,0:T(8,128)(2,1)} %layer.1) | data formatting | bytes 2097152

commit v9 on v8

--- a/solution.py
+++ b/solution.py
@@ -271,9 +271,10 @@
                  taps_in_ref, taps_ref, mix_ref, grow_ref, gcol_ref, bcol_ref, masks_ref, map_ref,
                  from_state_ref, local_ref, own_ref, row_ref, total_ref, column_ref, state_ref,
                  mixed_ref, part_ref, pair_out_ref, pair_in_ref, ring_out_ref, half_ref, final_ref,
+                 result_ref,
                  tok_sems, load_sems, halo_send, halo_recv, send_a, recv_a, send_d, recv_d, send_b, recv_b,
                  send_c, recv_c, send_x, recv_x, send_z, recv_z, pair_send, pair_recv, ring_send,
-                 ring_recv, gate):
+                 ring_recv, out_sem, gate):
     z, x, tp = lax.axis_index("sp_0"), lax.axis_index("sp_1"), lax.axis_index("tp")
     n_z, n_x, n_tp = lax.axis_size("sp_0"), lax.axis_size("sp_1"), lax.axis_size("tp")
     y, core = tp // 2, lax.rem(tp, 2)
@@ -502,7 +503,6 @@
     pool.corners()
     project(pool, ORDER[5:9], pool_ref)
     pool.fifth()
-    meet()
     out.own("x")
     send_z_maps(1)
     out.own("z")
@@ -660,7 +660,10 @@
         value = value + final_ref[1, piece].astype(F32)
         for block, (dz, dx) in enumerate(ORDER[2 * piece : 2 * piece + 2]):
             lanes = pl.ds(pl.multiple_of(out.shard(dz, dx) * 256, 256), 256)
-            out_ref[:, lanes] = value[:, block * 256 : block * 256 + 256].astype(BF16)
+            index = 2 * piece + block
+            result_ref[index] = value[:, block * 256 : block * 256 + 256].astype(BF16)
+            pltpu.make_async_copy(result_ref.at[index], out_ref.at[:, lanes], out_sem).start()
+    pltpu.make_async_copy(result_ref, result_ref, out_sem).wait()
     pltpu.make_async_copy(ring_out_ref, ring_out_ref, ring_send).wait()
 
 
@@ -683,7 +686,7 @@
         lambda *refs: layer_kernel(heads, *refs),
         out_shape=jax.ShapeDtypeStruct((128, width), BF16),
         in_specs=[hbm] * 9 + [vmem] * 6 + [smem] * 3,
-        out_specs=vmem,
+        out_specs=hbm,
         scratch_shapes=[
             pltpu.VMEM((tok_rows + HALO, depth), BF16),
             pltpu.VMEM((16, 272, 384), BF16),
@@ -716,11 +719,12 @@
             pltpu.VMEM((3, pieces, 128, PIECE), BF16),
             pltpu.VMEM((pieces, 128, PIECE), BF16),
             pltpu.VMEM((2, pieces, 128, PIECE), BF16),
+            pltpu.VMEM((width // 256, 128, 256), BF16),
             dma((chunks,)), dma((9,)), dma(()), dma((2,)),
             dma(()), dma((12,)), dma(()), dma((12,)), dma(()), dma((12,)), dma(()), dma((12,)),
             dma((heads,)), dma((heads,)), dma((heads,)), dma((heads,)),
             dma(()), dma((32,)), dma(()), dma((16,)),
-            pltpu.SemaphoreType.REGULAR,
+            dma(()), pltpu.SemaphoreType.REGULAR,
         ],
         compiler_params=pltpu.CompilerParams(
             vmem_limit_bytes=VMEM_LIMIT, collective_id=0, has_side_effects=True),

time: 117 us -> 116 us (level)
  no operation moved by 1% of the time
where the time goes in v9:
time: 116 us
  Pallas kernels  114 us (98%)
  local copies, waits for them, and re-layouts  2.29 us (2%)
    pallas_call x1, Pallas kernels, per_device(): pl.pallas_call(lambda *refs: layer_kernel(heads, *refs), out_shape=jax.Sh...  114 us

profile of v9, /device:TPU:1, one launch (start us, length us, event | category | flops | bytes accessed | tf_op | source)
XLA Modules:
  0.0 116.2 jit_solution(13730040950350790245)
XLA Ops:
  0.0 113.9 %layer.1 = bf16[128,4096]{1,0:T(8,128)(2,1)} custom-call(bf16[1024,4096]{1,0:T(8,128)(2,1)} %refs_0_.1, bf16[256,256]{1,0:T(8,128)(2,1)} %refs_1_.1, bf16[256,256]{1,0:T(8,128)(2,1)} %refs_2_.1, bf16[256,256]{1,0:T(8,128)(2,1)} %refs_3_.1, bf16[256,256]{1,0:T(8,128)(2,1)} %refs_4_.1, bf16[256,256]{1,0:T(8,128)(2,1)} %refs_5_.1, bf16[256,256]{1,0:T(8,128)(2,1)} %refs_6_.1, ...), custom_call_target="tpu_custom_call" | custom-call | tf_op jit(solution)/shard_map/layer/pallas_call | solution.py:685
  113.9 2.3 %copy.20 = bf16[128,4096]{1,0:T(8,128)(2,1)} copy(bf16[128,4096]{1,0:T(8,128)(2,1)} %layer.1) | data formatting | bytes 2097152
